TPU v7x, 32 devices: a whole 2x2x4 slice. The times are simulated.
32 devices in a mesh: sp: 8 (over z, x), tp: 4 (over y, core).
Axes of the slice: x: 2, y: 2, z: 4, core: 2. Of those that a mesh axis runs over, the one named last changes fastest.
Arguments:
- out_gate: bfloat16 [4096, 1536], P('sp', 'tp'), may hold values from -6 to 6
- in_gate: bfloat16 [4096, 1536], P('sp', 'tp'), may hold values from -6 to 6
- conv_values: bfloat16 [4096, 1536], P('sp', 'tp'), may hold values from -6 to 6
- conv_taps: float32 [3, 1536], P(None, 'tp'), may hold values from -3 to 3
- mix_gain: float32 [1536], replicated, may hold values from 0.1 to 1.9
- out_proj: bfloat16 [1536, 2048], replicated, may hold values from -0.15625 to 0.15625
- residual: bfloat16 [4096, 2048], P(('sp', 'tp')), may hold values from -6 to 6
- ffn_gain: float32 [2048], replicated, may hold values from 0.1 to 1.9
- routes: int32 [4096, 6], P(('sp', 'tp')), may hold values from 0 to 31, all different within a row; in each aligned block of 128 rows (0 to 127, 128 to 255, ...) at most 32 rows name the same one
- route_weights: float32 [4096, 6], P(('sp', 'tp')), may hold values from 0.05 to 1
- shared_gate: bfloat16 [2048, 512], replicated, may hold values from -0.125 to 0.125
- shared_up: bfloat16 [2048, 512], replicated, may hold values from -0.125 to 0.125
- shared_down: bfloat16 [512, 2048], replicated, may hold values from -0.25 to 0.25
- expert_gate: bfloat16 [32, 2048, 512], P(('sp', 'tp')), may hold values from -0.125 to 0.125
- expert_up: bfloat16 [32, 2048, 512], P(('sp', 'tp')), may hold values from -0.125 to 0.125
- expert_down: bfloat16 [32, 512, 2048], P(('sp', 'tp')), may hold values from -0.25 to 0.25
Outputs:
- layer_out: bfloat16 [4096, 2048], P(('sp', 'tp'))
Inputs may be any that keep to these rules, and one draw needn't show every extreme that they name: `routes`: each row names 6 different experts. Within the rows of one device (aligned blocks of 128 rows) no expert is named more than 32 times, a bound that some block reaches.
All inputs are finite; a program needn't handle non-finite values.
Results may differ from a plain program's by a relative error of at most 0.0065.
Values may be sent and summed in bfloat16 or wider, within the bound.
No kernel may reach another device: no remote copies, remote signals or barrier semaphores. Data moves between devices by JAX's collectives and lax.ppermute only.
A program may use at most 128 MiB of HBM per device.

v0:
```python
import functools

import jax
import jax.numpy as jnp
from jax import lax
from jax.experimental import pallas as pl
from jax.experimental.pallas import tpu as pltpu
from jax.sharding import Mesh, PartitionSpec as P


SEQ, TP, CHIPS, PLANE = ("z", "x"), ("y", "c"), ("x", "y"), ("x", "y", "c")
BF16, F32 = jnp.bfloat16, jnp.float32


def flips(count, distance):
    return [(i, i ^ distance) for i in range(count)]


def from_behind(block, distance):
    count = lax.axis_size(SEQ)
    route = [(i - distance, i) for i in range(distance, count)]
    return lax.ppermute(block, SEQ, route)


def grant(mib):
    return pltpu.CompilerParams(vmem_limit_bytes=mib << 20)


def cost(flops, arrays):
    size = sum(a.size * a.dtype.itemsize for a in arrays)
    return pl.CostEstimate(flops=flops, bytes_accessed=size, transcendentals=0)


def filter_kernel(parts, taps_count, me_ref, gate_ref, in_ref, val_ref, taps_ref, halo_ref, *rest):
    outs, scratch = rest[:parts], rest[parts]
    length = val_ref.shape[0]
    rows = length // parts
    back = taps_count - 1
    scratch[0:8] = jnp.zeros((8, scratch.shape[1]), F32)
    scratch[8 - back : 8] = halo_ref[...]
    scratch[8:] = in_ref[...].astype(F32) * val_ref[...].astype(F32)
    me = me_ref[0]
    for k in range(parts):
        start = pl.multiple_of((me ^ k) * rows, 16)
        window = scratch[pl.ds(start, rows + 8)]
        total = taps_ref[0:1] * window[8 - back : 8 - back + rows]
        for offset in range(1, taps_count):
            first = 8 - back + offset
            total = total + taps_ref[offset : offset + 1] * window[first : first + rows]
        outs[k][...] = (gate_ref[pl.ds(start, rows)].astype(F32) * total).astype(BF16)


def filter_rows(me, out_gate, in_gate, conv_values, conv_taps, halo, parts):
    length, channels = conv_values.shape
    out = jax.ShapeDtypeStruct((length // parts, channels), BF16)
    whole = pl.BlockSpec(memory_space=pltpu.VMEM)
    return pl.pallas_call(
        functools.partial(filter_kernel, parts, conv_taps.shape[0]),
        out_shape=[out] * parts,
        in_specs=[pl.BlockSpec(memory_space=pltpu.SMEM)] + [whole] * 5,
        out_specs=[whole] * parts,
        scratch_shapes=[pltpu.VMEM((length + 8, channels), F32)],
        cost_estimate=cost(8 * out_gate.size, [out_gate, in_gate, conv_values]),
        compiler_params=grant(8),
        name="filter_rows",
    )(me, out_gate, in_gate, conv_values, conv_taps, halo)


def mix_kernel(parts, me_ref, *refs):
    pieces = refs[:parts]
    mix_gain, out_proj, residual, ffn_gain, stream_ref, normed_ref, acc, squares = refs[parts:]
    step = pl.program_id(0)

    @pl.when(step == 0)
    def _():
        acc[...] = jnp.zeros_like(acc)
        squares[...] = jnp.zeros_like(squares)

    for k in range(parts):

        @pl.when(step == k)
        def _(k=k):
            values = pieces[k][...].astype(F32)
            squares[...] += jnp.sum(values * values, axis=1, keepdims=True)
            scaled = (values * mix_gain[...].reshape(1, -1)).astype(BF16)
            acc[...] += jnp.dot(scaled, out_proj[...], preferred_element_type=F32)

    @pl.when(step == parts - 1)
    def _():
        channels = parts * pieces[0].shape[1]
        inverse = lax.rsqrt(squares[...] / channels + 1e-06)
        stream = residual[...].astype(F32) + acc[...] * inverse
        stream_ref[...] = stream
        mean = jnp.mean(stream * stream, axis=1, keepdims=True)
        normed_ref[...] = (stream * lax.rsqrt(mean + 1e-06) * ffn_gain[...]).astype(BF16)


def mix_project(me, pieces, mix_gain, out_proj, residual, ffn_gain):
    parts = len(pieces)
    rows, channels = pieces[0].shape
    width = out_proj.shape[1]
    fixed = lambda shape: pl.BlockSpec(shape, lambda i, me_ref: (0,) * len(shape))
    if channels % 128:
        gain = mix_gain.reshape(parts, 1, channels)
        gain_spec = pl.BlockSpec((1, 1, channels), lambda i, me_ref: (me_ref[0] ^ i, 0, 0))
    else:
        gain = mix_gain[None]
        gain_spec = pl.BlockSpec((1, channels), lambda i, me_ref: (0, me_ref[0] ^ i))
    out_shape = [
        jax.ShapeDtypeStruct((rows, width), F32),
        jax.ShapeDtypeStruct((rows, width), BF16),
    ]
    grid_spec = pltpu.PrefetchScalarGridSpec(
        num_scalar_prefetch=1,
        grid=(parts,),
        in_specs=[fixed((rows, channels))] * parts
        + [
            gain_spec,
            pl.BlockSpec((channels, width), lambda i, me_ref: (me_ref[0] ^ i, 0)),
            fixed((rows, width)),
            fixed((1, width)),
        ],
        out_specs=[fixed((rows, width))] * 2,
        scratch_shapes=[pltpu.VMEM((rows, width), F32), pltpu.VMEM((rows, 1), F32)],
    )
    return pl.pallas_call(
        functools.partial(mix_kernel, parts),
        out_shape=out_shape,
        grid_spec=grid_spec,
        cost_estimate=cost(2 * rows * out_proj.size, [out_proj, residual] + out_shape),
        compiler_params=grant(14),
        name="mix_project",
    )(me, *pieces, gain, out_proj, residual, ffn_gain[None])


def send_kernel(chips, own_ref, pair_ref, table_ref, *outs):
    size = outs[0].shape[0] // 2
    tokens = own_ref.shape[0]
    slots = lax.broadcasted_iota(jnp.int32, (size, tokens), 0).astype(F32)
    for side, (ref, base) in enumerate(((own_ref, 0), (pair_ref, 4 * chips))):
        pick = jnp.concatenate(
            [
                (table_ref[base + k : base + k + 1] == slots).astype(F32).astype(BF16)
                for k in range(chips)
            ]
        )
        rows = jnp.dot(pick, ref[...], preferred_element_type=F32).astype(BF16)
        for k in range(chips):
            outs[k][side * size : (side + 1) * size] = rows[k * size : (k + 1) * size]


def outgoing_rows(own, pair, table, chips, capacity):
    tokens, width = own.shape
    whole = pl.BlockSpec(memory_space=pltpu.VMEM)
    out_shape = [jax.ShapeDtypeStruct((2 * capacity, width), BF16)] * chips
    return pl.pallas_call(
        functools.partial(send_kernel, chips),
        out_shape=out_shape,
        in_specs=[whole] * 3,
        out_specs=[whole] * chips,
        cost_estimate=cost(4 * chips * capacity * tokens * width, [own, pair] + out_shape),
        compiler_params=grant(6),
        name="outgoing_rows",
    )(own, pair, table)


def swiglu_term(rows, gate_ref, up_ref, down_ref):
    gate_part = jnp.dot(rows, gate_ref, preferred_element_type=F32)
    up_part = jnp.dot(rows, up_ref, preferred_element_type=F32)
    hidden = (gate_part / (1.0 + jnp.exp(-gate_part)) * up_part).astype(BF16)
    return jnp.dot(hidden, down_ref, preferred_element_type=F32)


def expert_kernel(parts, count, *refs):
    pieces, outs = refs[:parts], refs[parts + 3 : parts + 3 + count]
    gate_ref, up_ref, down_ref = refs[parts : parts + 3]
    rows, acc = refs[parts + 3 + count :]
    size, out_size = pieces[0].shape[0], outs[0].shape[0]
    step = pl.program_id(0)

    @pl.when(step == 0)
    def _():
        for k in range(parts):
            rows[k * size : (k + 1) * size] = pieces[k][...]

    term = swiglu_term(rows[...], gate_ref[0], up_ref[0], down_ref[0])

    @pl.when(step == 0)
    def _():
        acc[...] = term

    @pl.when((step > 0) & (step < pl.num_programs(0) - 1))
    def _():
        acc[...] += term

    @pl.when(step == pl.num_programs(0) - 1)
    def _():
        total = acc[...] + term
        for k in range(count):
            outs[k][...] = total[k * out_size : (k + 1) * out_size].astype(BF16)


def expert_rows(pieces, count, expert_gate, expert_up, expert_down):
    parts = len(pieces)
    size, width = pieces[0].shape
    out_size = parts * size // count
    hidden = expert_gate.shape[2]
    tile = hidden // 2
    out = jax.ShapeDtypeStruct((out_size, width), BF16)
    weights = [expert_gate, expert_up, expert_down]
    return pl.pallas_call(
        functools.partial(expert_kernel, parts, count),
        out_shape=[out] * count,
        grid=(2,),
        in_specs=[pl.BlockSpec((size, width), lambda i: (0, 0))] * parts
        + [
            pl.BlockSpec((1, width, tile), lambda i: (0, 0, i)),
            pl.BlockSpec((1, width, tile), lambda i: (0, 0, i)),
            pl.BlockSpec((1, tile, width), lambda i: (0, i, 0)),
        ],
        out_specs=[pl.BlockSpec((out_size, width), lambda i: (0, 0))] * count,
        scratch_shapes=[
            pltpu.VMEM((parts * size, width), BF16),
            pltpu.VMEM((parts * size, width), F32),
        ],
        cost_estimate=cost(2 * parts * size * 3 * width * hidden, weights),
        compiler_params=grant(20),
        name="expert_rows",
    )(*pieces, *weights)


def shared_kernel(rows_ref, stream_ref, gate_ref, up_ref, down_ref, out_ref):
    term = swiglu_term(rows_ref[...], gate_ref[...], up_ref[...], down_ref[...])

    @pl.when(pl.program_id(0) == 0)
    def _():
        out_ref[...] = stream_ref[...] + term

    @pl.when(pl.program_id(0) > 0)
    def _():
        out_ref[...] += term


def shared_rows(normed, stream, gate, up, down):
    rows, width = normed.shape
    hidden = gate.shape[1]
    tile = hidden // 2
    fixed = pl.BlockSpec((rows, width), lambda i: (0, 0))
    return pl.pallas_call(
        shared_kernel,
        out_shape=jax.ShapeDtypeStruct((rows, width), F32),
        grid=(2,),
        in_specs=[
            fixed,
            fixed,
            pl.BlockSpec((width, tile), lambda i: (0, i)),
            pl.BlockSpec((width, tile), lambda i: (0, i)),
            pl.BlockSpec((tile, width), lambda i: (i, 0)),
        ],
        out_specs=fixed,
        cost_estimate=cost(6 * rows * width * hidden, [gate, up, down]),
        compiler_params=grant(12),
        name="shared_rows",
    )(normed, stream, gate, up, down)


def combine_kernel(parts, chips, *refs):
    pieces, table = refs[:parts], refs[parts]
    full_ref, short_ref, high, low, rows = refs[parts + 1 :]
    size = pieces[0].shape[0]
    tokens = table.shape[1]
    slots = lax.broadcasted_iota(jnp.int32, (size, tokens), 0).astype(F32)
    for k in range(parts):
        at = slice(k * size, (k + 1) * size)
        row = (k % 2) * chips + k // 2
        named = table[row : row + 1] == slots
        weight = jnp.where(named, table[2 * chips + row : 2 * chips + row + 1], 0.0)
        top = weight.astype(BF16)
        high[at] = top
        low[at] = (weight - top.astype(F32)).astype(BF16)
        rows[at] = pieces[k][...]
    contract = (((0,), (0,)), ((), ()))
    total = lax.dot_general(high[...], rows[...], contract, preferred_element_type=F32)
    total += lax.dot_general(low[...], rows[...], contract, preferred_element_type=F32)
    full_ref[...] = total
    short_ref[...] = total.astype(BF16)


def combine(pieces, table):
    parts = len(pieces)
    size, width = pieces[0].shape
    tokens = table.shape[1]
    whole = pl.BlockSpec(memory_space=pltpu.VMEM)
    out_shape = [
        jax.ShapeDtypeStruct((tokens, width), F32),
        jax.ShapeDtypeStruct((tokens, width), BF16),
    ]
    return pl.pallas_call(
        functools.partial(combine_kernel, parts, parts // 2),
        out_shape=out_shape,
        in_specs=[whole] * (parts + 1),
        out_specs=[whole] * 2,
        scratch_shapes=[
            pltpu.VMEM((parts * size, tokens), BF16),
            pltpu.VMEM((parts * size, tokens), BF16),
            pltpu.VMEM((parts * size, width), BF16),
        ],
        cost_estimate=cost(4 * parts * size * tokens * width, out_shape),
        compiler_params=grant(8),
        name="combine_rows",
    )(*pieces, table)


def gather_line(own, count):
    if count != 4:
        return [own] + [lax.ppermute(own, "z", flips(count, j)) for j in range(1, count)]
    sides, middle = flips(4, 1), [(1, 2), (2, 1)]
    near = lax.ppermute(own, "z", sides)
    across = lax.ppermute(own, "z", middle)
    across_far = lax.ppermute(near, "z", middle)
    side_far = lax.ppermute(across, "z", sides)
    side_end = lax.ppermute(across_far, "z", sides)
    return [own, near, across_far + side_far, across + side_end]


def exchange(pieces, axes):
    count = len(pieces)
    moved = [lax.ppermute(pieces[k], axes, flips(count, k)) for k in range(1, count)]
    return [pieces[0]] + moved


def layer(
    out_gate,
    in_gate,
    conv_values,
    conv_taps,
    mix_gain,
    out_proj,
    residual,
    ffn_gain,
    routes,
    route_weights,
    shared_gate,
    shared_up,
    shared_down,
    expert_gate,
    expert_up,
    expert_down,
):
    z_count, tp_count = lax.axis_size("z"), lax.axis_size(TP)
    chips = lax.axis_size(CHIPS)
    z_index, tp_index = lax.axis_index("z"), lax.axis_index(TP)
    chip_index, core_index = lax.axis_index(CHIPS), lax.axis_index("c")

    back = conv_taps.shape[0] - 1
    length = conv_values.shape[0]
    tail = in_gate[length - back :].astype(F32) * conv_values[length - back :].astype(F32)
    halo = from_behind(tail, 1)
    me = tp_index.reshape(1).astype(jnp.int32)
    blocks = filter_rows(me, out_gate, in_gate, conv_values, conv_taps, halo, tp_count)
    pieces = exchange(blocks, TP)

    row_count, top_count = routes.shape
    capacity = max(2, 4 * row_count * top_count // (6 * z_count * chips))
    gate_values = route_weights / jnp.sum(route_weights, axis=1, keepdims=True) * 2.5
    layers = jnp.arange(z_count, dtype=jnp.int32) ^ z_index
    cores = jnp.arange(2, dtype=jnp.int32) ^ core_index
    places = jnp.arange(chips, dtype=jnp.int32) ^ chip_index
    experts = (layers[:, None, None] * chips + places) * 2 + cores[:, None]
    hits = routes.T[:, None, :] == experts.reshape(-1)[None, :, None]
    named = jnp.any(hits, axis=0)
    gates_of = jnp.sum(jnp.where(hits, gate_values.T[:, None, :], 0.0), axis=0)
    steps = jnp.arange(row_count, dtype=jnp.int32)
    earlier = (steps[:, None] < steps[None, :]).astype(BF16)
    rank = jnp.dot(named.astype(BF16), earlier, preferred_element_type=F32)
    rank = jnp.where(named, rank, -1.0).reshape(z_count, 2 * chips, row_count)
    gates_of = gates_of.reshape(z_count, 2 * chips, row_count)
    pair_rank = lax.ppermute(rank[:, chips:], "c", flips(2, 1))
    table = jnp.concatenate([rank, gates_of, pair_rank], axis=1)
    tables = [table[0]] + [
        lax.ppermute(table[j], "z", flips(z_count, j))
        for j in range(1, z_count)
    ]

    stream, normed = mix_project(me, pieces, mix_gain, out_proj, residual, ffn_gain)

    sources = gather_line(normed, z_count)
    results = []
    for j in range(z_count):
        pair = lax.ppermute(sources[j], "c", flips(2, 1))
        outgoing = outgoing_rows(sources[j], pair, tables[j], chips, capacity)
        arrived = exchange(outgoing, CHIPS)
        weights = (expert_gate, expert_up, expert_down)
        results.append(expert_rows(arrived, 2 * chips, *weights))

    base = shared_rows(normed, stream, shared_gate, shared_up, shared_down)

    partial, short = [None] * z_count, [None] * z_count
    for j in reversed(range(z_count)):
        returned = exchange(results[j], PLANE)
        partial[j], short[j] = combine(returned, tables[j])

    if z_count == 4:
        outward, middle, sides = [(0, 1), (3, 2)], [(1, 2), (2, 1)], flips(4, 1)

        def hop(block, route):
            return lax.ppermute(block.astype(BF16), "z", route).astype(F32)

        far = hop(short[3], outward)
        mid = hop(short[2], outward)
        far = hop(far + partial[2], middle)
        mid = hop(mid + partial[3], middle)
        last = hop(far + partial[1], sides)
        routed = partial[0] + mid + last
    else:
        routed = partial[0]
        for j in range(1, z_count):
            routed = routed + lax.ppermute(short[j], "z", flips(z_count, j))
    return (base + routed).astype(BF16)


def solution(mesh):
    sp_count, tp_count = mesh.shape["sp"], mesh.shape["tp"]
    z_count = 1 << -(-(sp_count.bit_length() - 1) // 2)
    every = SEQ + TP
    split = Mesh(
        mesh.devices.reshape(z_count, sp_count // z_count, tp_count // 2, 2), every
    )
    in_specs = (
        P(SEQ, TP),
        P(SEQ, TP),
        P(SEQ, TP),
        P(None, TP),
        P(),
        P(),
        P(every, None),
        P(),
        P(every, None),
        P(every, None),
        P(),
        P(),
        P(),
        P(every, None, None),
        P(every, None, None),
        P(every, None, None),
    )
    return jax.shard_map(
        layer, mesh=split, in_specs=in_specs, out_specs=P(every, None), check_vma=False
    )
```

profile of v0, /device:TPU:0, one launch (start us, length us, event | category | flops | bytes accessed | tf_op | source)
XLA Modules:
  0.0 218.7 jit_solution(2506644075927175104)
XLA Ops:
  0.7 4.9 %collective-permute-start = (f32[2,384]{1,0:T(2,128)S(1)}, f32[2,384]{1,0:T(2,128)S(1)}, u32[]{:S(2)}, u32[]{:S(2)}) collective-permute-start(f32[2,384]{1,0:T(2,128)S(1)} %convert_multiply_fusion), channel_id=1, source_target_pairs={{0,4},{4,8},{8,12},{12,16},{16,20},{20,24},{24,28},{1,5},{5,9},{9,... | collective-permute-start | bytes 9224 | tf_op jit(solution)/shard_map/ppermute | solution.py:22
  13.8 3.2 %collective-permute-done.2.refs_2_ = bf16[128,384]{1,0:T(8,128)(2,1)S(1)} collective-permute-done((bf16[128,384]{1,0:T(8,128)(2,1)S(1)}, bf16[128,384]{1,0:T(8,128)(2,1)S(1)}, u32[]{:S(2)}, u32[]{:S(2)}) %collective-permute-start.2) | collective-permute-done | bytes 98336 | tf_op jit(solution)/shard_map/ppermute | solution.py:328
  18.0 2.8 %copy-done.3 = bf16[1536,2048]{1,0:T(8,128)(2,1)S(1)} copy-done((bf16[1536,2048]{1,0:T(8,128)(2,1)S(1)}, bf16[1536,2048]{1,0:T(8,128)(2,1)}, u32[]{:S(2)}) %copy-start.3) | copy-done | bytes 6291480
  22.6 2.1 mix_project.1
  25.7 3.3 %collective-permute-start.16 = (bf16[128,2048]{1,0:T(8,128)(2,1)S(1)}, bf16[128,2048]{1,0:T(8,128)(2,1)S(1)}, u32[]{:S(2)}, u32[]{:S(2)}) collective-permute-start(bf16[128,2048]{1,0:T(8,128)(2,1)S(1)} %get-tuple-element.69.rows_ref.own_ref), channel_id=1, source_target_pairs={{0,8},{8,0},{16,24},{24,16},{1,9},{9,1},{17,25},{25,17},{2,10},{10... | collective-permute-start | bytes 1572872 | tf_op jit(solution)/shard_map/ppermute | solution.py:318
  28.9 12.4 %collective-permute-done.16.own_ref = bf16[128,2048]{1,0:T(8,128)(2,1)S(1)} collective-permute-done((bf16[128,2048]{1,0:T(8,128)(2,1)S(1)}, bf16[128,2048]{1,0:T(8,128)(2,1)S(1)}, u32[]{:S(2)}, u32[]{:S(2)}) %collective-permute-start.16) | collective-permute-done | bytes 524320 | tf_op jit(solution)/shard_map/ppermute | solution.py:318
  44.3 15.5 %collective-permute-start.33 = (bf16[128,2048]{1,0:T(8,128)(2,1)}, bf16[128,2048]{1,0:T(8,128)(2,1)}, u32[]{:S(2)}, u32[]{:S(2)}) collective-permute-start(bf16[128,2048]{1,0:T(8,128)(2,1)} %collective-permute-done.17), channel_id=1, source_target_pairs={{0,8},{8,0},{16,24},{24,16},{1,9},{9,1},{17,25},{25,17},{2,10},{10... | collective-permute-start | bytes 1572872 | tf_op jit(solution)/shard_map/ppermute | solution.py:322
  60.1 9.6 %collective-permute-start.19 = (bf16[128,2048]{1,0:T(8,128)(2,1)}, bf16[128,2048]{1,0:T(8,128)(2,1)}, u32[]{:S(2)}, u32[]{:S(2)}) collective-permute-start(bf16[128,2048]{1,0:T(8,128)(2,1)} %collective-permute-done.18), channel_id=1, source_target_pairs={{0,8},{8,0},{16,24},{24,16},{1,9},{9,1},{17,25},{25,17},{2,10},{10... | collective-permute-start | bytes 1572872 | tf_op jit(solution)/shard_map/ppermute | solution.py:321
  72.1 8.6 %collective-permute-done.19 = bf16[128,2048]{1,0:T(8,128)(2,1)} collective-permute-done((bf16[128,2048]{1,0:T(8,128)(2,1)}, bf16[128,2048]{1,0:T(8,128)(2,1)}, u32[]{:S(2)}, u32[]{:S(2)}) %collective-permute-start.19) | collective-permute-done | bytes 524320 | tf_op jit(solution)/shard_map/ppermute | solution.py:321
  82.1 2.4 %collective-permute-start.35 = (f32[20,128]{1,0:T(8,128)S(1)}, f32[20,128]{1,0:T(8,128)S(1)}, u32[]{:S(2)}, u32[]{:S(2)}) collective-permute-start(f32[20,128]{1,0:T(8,128)S(1)} %get-tuple-element.127), channel_id=1, source_target_pairs={{0,24},{8,16},{16,8},{24,0},{1,25},{9,17},{17,9},{25,1},{2,26},{10... | collective-permute-start | bytes 30728 | tf_op jit(solution)/shard_map/ppermute | solution.py:381
  84.6 3.1 %collective-permute-done.35.table_ref.refs_8_ = f32[20,128]{1,0:T(8,128)S(1)} collective-permute-done((f32[20,128]{1,0:T(8,128)S(1)}, f32[20,128]{1,0:T(8,128)S(1)}, u32[]{:S(2)}, u32[]{:S(2)}) %collective-permute-start.35) | collective-permute-done | bytes 10272 | tf_op jit(solution)/shard_map/ppermute | solution.py:381
  92.5 3.8 %collective-permute-done.21.table_ref.refs_8_ = f32[20,128]{1,0:T(8,128)S(1)} collective-permute-done((f32[20,128]{1,0:T(8,128)S(1)}, f32[20,128]{1,0:T(8,128)S(1)}, u32[]{:S(2)}, u32[]{:S(2)}) %collective-permute-start.21) | collective-permute-done | bytes 10272 | tf_op jit(solution)/shard_map/ppermute | solution.py:381
  98.9 3.7 %collective-permute-done.38.refs_3_ = bf16[64,2048]{1,0:T(8,128)(2,1)S(1)} collective-permute-done((bf16[64,2048]{1,0:T(8,128)(2,1)S(1)}, bf16[64,2048]{1,0:T(8,128)(2,1)S(1)}, u32[]{:S(2)}, u32[]{:S(2)}) %collective-permute-start.38) | collective-permute-done | bytes 262176 | tf_op jit(solution)/shard_map/ppermute | solution.py:328
  102.6 2.9 %expert_rows.6 = (bf16[32,2048]{1,0:T(8,128)(2,1)S(1)}, bf16[32,2048]{1,0:T(8,128)(2,1)S(1)}, bf16[32,2048]{1,0:T(8,128)(2,1)S(1)}, bf16[32,2048]{1,0:T(8,128)(2...) custom-call(bf16[64,2048]{1,0:T(8,128)(2,1)S(1)} %get-tuple-element., ...), custom_call_target="tpu_custom_call" | custom-call | flops 1610612736 | bytes 6291456 | tf_op jit(solution)/shard_map/expert_rows/pallas_call | solution.py:211
  107.3 2.0 collective-permute-done.50.table_ref.refs_8_
  120.7 13.5 %collective-permute-done.44.refs_6_ = bf16[32,2048]{1,0:T(8,128)(2,1)S(1)} collective-permute-done((bf16[32,2048]{1,0:T(8,128)(2,1)S(1)}, bf16[32,2048]{1,0:T(8,128)(2,1)S(1)}, u32[]{:S(2)}, u32[]{:S(2)}) %collective-permute-start.44) | collective-permute-done | bytes 131104 | tf_op jit(solution)/shard_map/ppermute | solution.py:328
  136.9 2.0 collective-permute-start.53
  138.8 2.1 collective-permute-start.47
  140.9 2.9 %expert_rows.5 = (bf16[32,2048]{1,0:T(8,128)(2,1)S(1)}, bf16[32,2048]{1,0:T(8,128)(2,1)S(1)}, bf16[32,2048]{1,0:T(8,128)(2,1)S(1)}, bf16[32,2048]{1,0:T(8,128)(2...) custom-call(bf16[64,2048]{1,0:T(8,128)(2,1)S(1)} %get-tuple-element., ...), custom_call_target="tpu_custom_call" | custom-call | flops 1610612736 | bytes 6291456 | tf_op jit(solution)/shard_map/expert_rows/pallas_call | solution.py:211
  145.8 5.2 %collective-permute-done.53.refs_3_ = bf16[64,2048]{1,0:T(8,128)(2,1)S(1)} collective-permute-done((bf16[64,2048]{1,0:T(8,128)(2,1)S(1)}, bf16[64,2048]{1,0:T(8,128)(2,1)S(1)}, u32[]{:S(2)}, u32[]{:S(2)}) %collective-permute-start.53) | collective-permute-done | bytes 262176 | tf_op jit(solution)/shard_map/ppermute | solution.py:328
  154.3 2.1 collective-permute-done.27.refs_3_
  156.8 2.9 %expert_rows.7 = (bf16[32,2048]{1,0:T(8,128)(2,1)S(1)}, bf16[32,2048]{1,0:T(8,128)(2,1)S(1)}, bf16[32,2048]{1,0:T(8,128)(2,1)S(1)}, bf16[32,2048]{1,0:T(8,128)(2...) custom-call(bf16[64,2048]{1,0:T(8,128)(2,1)S(1)} %get-tuple-element., ...), custom_call_target="tpu_custom_call" | custom-call | flops 1610612736 | bytes 6291456 | tf_op jit(solution)/shard_map/expert_rows/pallas_call | solution.py:211
  164.8 2.2 collective-permute-start.58
  167.1 1.9 collective-permute-start.59
  171.5 1.9 collective-permute-start.32
  177.1 2.2 %collective-permute-done.60.refs_7_ = bf16[32,2048]{1,0:T(8,128)(2,1)S(1)} collective-permute-done((bf16[32,2048]{1,0:T(8,128)(2,1)S(1)}, bf16[32,2048]{1,0:T(8,128)(2,1)S(1)}, u32[]{:S(2)}, u32[]{:S(2)}) %collective-permute-start.60) | collective-permute-done | bytes 131104 | tf_op jit(solution)/shard_map/ppermute | solution.py:328
  181.4 3.7 %collective-permute-done.32 = bf16[128,2048]{1,0:T(8,128)(2,1)S(1)} collective-permute-done((bf16[128,2048]{1,0:T(8,128)(2,1)S(1)}, bf16[128,2048]{1,0:T(8,128)(2,1)S(1)}, u32[]{:S(2)}, u32[]{:S(2)}) %collective-permute-start.32) | collective-permute-done | bytes 524320 | tf_op jit(solution)/shard_map/ppermute | solution.py:407
  186.0 10.2 %collective-permute-start.61 = (bf16[128,2048]{1,0:T(8,128)(2,1)S(1)}, bf16[128,2048]{1,0:T(8,128)(2,1)S(1)}, u32[]{:S(2)}, u32[]{:S(2)}) collective-permute-start(bf16[128,2048]{1,0:T(8,128)(2,1)S(1)} %add_convert_fusion.1), channel_id=1, source_target_pairs={{0,8},{8,0},{16,24},{24,16},{1,9},{9,1},{17,25},{25,17},{2,10},{10... | collective-permute-start | bytes 1572872 | tf_op jit(solution)/shard_map/ppermute | solution.py:407
  196.3 2.9 %expert_rows.4 = (bf16[32,2048]{1,0:T(8,128)(2,1)S(1)}, bf16[32,2048]{1,0:T(8,128)(2,1)S(1)}, bf16[32,2048]{1,0:T(8,128)(2,1)S(1)}, bf16[32,2048]{1,0:T(8,128)(2...) custom-call(bf16[64,2048]{1,0:T(8,128)(2,1)S(1)} %get-tuple-element., ...), custom_call_target="tpu_custom_call" | custom-call | flops 1610612736 | bytes 6291456 | tf_op jit(solution)/shard_map/expert_rows/pallas_call | solution.py:211
  201.6 4.1 %collective-permute-done.10.refs_2_ = bf16[32,2048]{1,0:T(8,128)(2,1)S(1)} collective-permute-done((bf16[32,2048]{1,0:T(8,128)(2,1)S(1)}, bf16[32,2048]{1,0:T(8,128)(2,1)S(1)}, u32[]{:S(2)}, u32[]{:S(2)}) %collective-permute-start.10) | collective-permute-done | bytes 131104 | tf_op jit(solution)/shard_map/ppermute | solution.py:328
  210.1 2.0 shared_rows.1
  212.0 2.7 %collective-permute-done.14.refs_6_ = bf16[32,2048]{1,0:T(8,128)(2,1)S(1)} collective-permute-done((bf16[32,2048]{1,0:T(8,128)(2,1)S(1)}, bf16[32,2048]{1,0:T(8,128)(2,1)S(1)}, u32[]{:S(2)}, u32[]{:S(2)}) %collective-permute-start.14) | collective-permute-done | bytes 131104 | tf_op jit(solution)/shard_map/ppermute | solution.py:328
  (162 shorter events, 73.4 us)
Async XLA Ops:
  25.7 15.7 %collective-permute-start.16 = (bf16[128,2048]{1,0:T(8,128)(2,1)S(1)}, bf16[128,2048]{1,0:T(8,128)(2,1)S(1)}, u32[]{:S(2)}, u32[]{:S(2)}) collective-permute-start(bf16[128,2048]{1,0:T(8,128)(2,1)S(1)} %get-tuple-element.69.rows_ref.own_ref), channel_id=1, source_target_pairs={{0,8},{8,0},{16,24},{24,16},{1,9},{9,1},{17,25},{25,17},{2,10},{10... | collective-permute-start | bytes 1572872 | tf_op jit(solution)/shard_map/ppermute | solution.py:318
  42.8 17.2 %collective-permute-start.18 = (bf16[128,2048]{1,0:T(8,128)(2,1)S(1)}, bf16[128,2048]{1,0:T(8,128)(2,1)}, u32[]{:S(2)}, u32[]{:S(2)}) collective-permute-start(bf16[128,2048]{1,0:T(8,128)(2,1)S(1)} %get-tuple-element.69.rows_ref.own_ref), channel_id=1, source_target_pairs={{8,16},{16,8},{9,17},{17,9},{10,18},{18,10},{11,19},{19,11},{12,20... | collective-permute-start | bytes 1572872 | tf_op jit(solution)/shard_map/ppermute | solution.py:319
  44.3 25.6 %collective-permute-start.33 = (bf16[128,2048]{1,0:T(8,128)(2,1)}, bf16[128,2048]{1,0:T(8,128)(2,1)}, u32[]{:S(2)}, u32[]{:S(2)}) collective-permute-start(bf16[128,2048]{1,0:T(8,128)(2,1)} %collective-permute-done.17), channel_id=1, source_target_pairs={{0,8},{8,0},{16,24},{24,16},{1,9},{9,1},{17,25},{25,17},{2,10},{10... | collective-permute-start | bytes 1572872 | tf_op jit(solution)/shard_map/ppermute | solution.py:322
  60.1 20.6 %collective-permute-start.19 = (bf16[128,2048]{1,0:T(8,128)(2,1)}, bf16[128,2048]{1,0:T(8,128)(2,1)}, u32[]{:S(2)}, u32[]{:S(2)}) collective-permute-start(bf16[128,2048]{1,0:T(8,128)(2,1)} %collective-permute-done.18), channel_id=1, source_target_pairs={{0,8},{8,0},{16,24},{24,16},{1,9},{9,1},{17,25},{25,17},{2,10},{10... | collective-permute-start | bytes 1572872 | tf_op jit(solution)/shard_map/ppermute | solution.py:321
  69.9 12.2 %collective-permute-start.5 = (f32[4,4,128]{2,1,0:T(4,128)S(1)}, f32[4,4,128]{2,1,0:T(4,128)S(1)}, u32[]{:S(2)}, u32[]{:S(2)}) collective-permute-start(f32[4,4,128]{2,1,0:T(4,128)S(1)} %slice.28), channel_id=1, source_target_pairs={{0,1},{1,0},{2,3},{3,2},{4,5},{5,4},{6,7},{7,6},{8,9},{9,8},{10,11... | collective-permute-start | bytes 24584 | tf_op jit(solution)/shard_map/ppermute | solution.py:378
  71.4 16.3 %collective-permute-start.34 = (bf16[128,2048]{1,0:T(8,128)(2,1)S(1)}, bf16[128,2048]{1,0:T(8,128)(2,1)S(1)}, u32[]{:S(2)}, u32[]{:S(2)}) collective-permute-start(bf16[128,2048]{1,0:T(8,128)(2,1)S(1)} %add.78.own_ref), channel_id=1, source_target_pairs={{0,1},{1,0},{2,3},{3,2},{4,5},{5,4},{6,7},{7,6},{8,9},{9,8},{10,11... | collective-permute-start | bytes 1572872 | tf_op jit(solution)/shard_map/ppermute | solution.py:390
  82.0 14.3 %collective-permute-start.20 = (bf16[128,2048]{1,0:T(8,128)(2,1)S(1)}, bf16[128,2048]{1,0:T(8,128)(2,1)S(1)}, u32[]{:S(2)}, u32[]{:S(2)}) collective-permute-start(bf16[128,2048]{1,0:T(8,128)(2,1)S(1)} %add.77.own_ref), channel_id=1, source_target_pairs={{0,1},{1,0},{2,3},{3,2},{4,5},{5,4},{6,7},{7,6},{8,9},{9,8},{10,11... | collective-permute-start | bytes 1572872 | tf_op jit(solution)/shard_map/ppermute | solution.py:390
  88.1 10.2 %collective-permute-start.36 = (bf16[64,2048]{1,0:T(8,128)(2,1)S(1)}, bf16[64,2048]{1,0:T(8,128)(2,1)S(1)}, u32[]{:S(2)}, u32[]{:S(2)}) collective-permute-start(bf16[64,2048]{1,0:T(8,128)(2,1)S(1)} %get-tuple-element.98), channel_id=1, source_target_pairs={{0,2},{2,0},{4,6},{6,4},{1,3},{3,1},{5,7},{7,5},{8,10},{10,8},{12,... | collective-permute-start | bytes 786440 | tf_op jit(solution)/shard_map/ppermute | solution.py:328
  89.8 9.2 %collective-permute-start.37 = (bf16[64,2048]{1,0:T(8,128)(2,1)S(1)}, bf16[64,2048]{1,0:T(8,128)(2,1)S(1)}, u32[]{:S(2)}, u32[]{:S(2)}) collective-permute-start(bf16[64,2048]{1,0:T(8,128)(2,1)S(1)} %get-tuple-element.99), channel_id=1, source_target_pairs={{0,4},{2,6},{4,0},{6,2},{1,5},{3,7},{5,1},{7,3},{8,12},{10,14},{12... | collective-permute-start | bytes 786440 | tf_op jit(solution)/shard_map/ppermute | solution.py:328
  90.4 12.3 %collective-permute-start.38 = (bf16[64,2048]{1,0:T(8,128)(2,1)S(1)}, bf16[64,2048]{1,0:T(8,128)(2,1)S(1)}, u32[]{:S(2)}, u32[]{:S(2)}) collective-permute-start(bf16[64,2048]{1,0:T(8,128)(2,1)S(1)} %get-tuple-element.100), channel_id=1, source_target_pairs={{0,6},{2,4},{4,2},{6,0},{1,7},{3,5},{5,3},{7,1},{8,14},{10,12},{12... | collective-permute-start | bytes 786440 | tf_op jit(solution)/shard_map/ppermute | solution.py:328
  96.3 13.6 %collective-permute-start.49 = (bf16[128,2048]{1,0:T(8,128)(2,1)S(1)}, bf16[128,2048]{1,0:T(8,128)(2,1)S(1)}, u32[]{:S(2)}, u32[]{:S(2)}) collective-permute-start(bf16[128,2048]{1,0:T(8,128)(2,1)S(1)} %collective-permute-done.16.own_ref), channel_id=1, source_target_pairs={{0,1},{1,0},{2,3},{3,2},{4,5},{5,4},{6,7},{7,6},{8,9},{9,8},{10,11... | collective-permute-start | bytes 1572872 | tf_op jit(solution)/shard_map/ppermute | solution.py:390
  96.7 14.4 %collective-permute-start.22 = (bf16[64,2048]{1,0:T(8,128)(2,1)S(1)}, bf16[64,2048]{1,0:T(8,128)(2,1)S(1)}, u32[]{:S(2)}, u32[]{:S(2)}) collective-permute-start(bf16[64,2048]{1,0:T(8,128)(2,1)S(1)} %get-tuple-element.85), channel_id=1, source_target_pairs={{0,2},{2,0},{4,6},{6,4},{1,3},{3,1},{5,7},{7,5},{8,10},{10,8},{12,... | collective-permute-start | bytes 786440 | tf_op jit(solution)/shard_map/ppermute | solution.py:328
  109.8 34.0 %collective-permute-start.4 = (bf16[128,2048]{1,0:T(8,128)(2,1)S(1)}, bf16[128,2048]{1,0:T(8,128)(2,1)S(1)}, u32[]{:S(2)}, u32[]{:S(2)}) collective-permute-start(bf16[128,2048]{1,0:T(8,128)(2,1)S(1)} %get-tuple-element.69.rows_ref.own_ref), channel_id=1, source_target_pairs={{0,1},{1,0},{2,3},{3,2},{4,5},{5,4},{6,7},{7,6},{8,9},{9,8},{10,11... | collective-permute-start | bytes 1572872 | tf_op jit(solution)/shard_map/ppermute | solution.py:390
  112.5 24.4 %collective-permute-start.23 = (bf16[64,2048]{1,0:T(8,128)(2,1)S(1)}, bf16[64,2048]{1,0:T(8,128)(2,1)S(1)}, u32[]{:S(2)}, u32[]{:S(2)}) collective-permute-start(bf16[64,2048]{1,0:T(8,128)(2,1)S(1)} %get-tuple-element.86), channel_id=1, source_target_pairs={{0,4},{2,6},{4,0},{6,2},{1,5},{3,7},{5,1},{7,3},{8,12},{10,14},{12... | collective-permute-start | bytes 786440 | tf_op jit(solution)/shard_map/ppermute | solution.py:328
  115.0 23.8 %collective-permute-start.24 = (bf16[64,2048]{1,0:T(8,128)(2,1)S(1)}, bf16[64,2048]{1,0:T(8,128)(2,1)S(1)}, u32[]{:S(2)}, u32[]{:S(2)}) collective-permute-start(bf16[64,2048]{1,0:T(8,128)(2,1)S(1)} %get-tuple-element.87), channel_id=1, source_target_pairs={{0,6},{2,4},{4,2},{6,0},{1,7},{3,5},{5,3},{7,1},{8,14},{10,12},{12... | collective-permute-start | bytes 786440 | tf_op jit(solution)/shard_map/ppermute | solution.py:328
  117.5 16.7 %collective-permute-start.44 = (bf16[32,2048]{1,0:T(8,128)(2,1)S(1)}, bf16[32,2048]{1,0:T(8,128)(2,1)S(1)}, u32[]{:S(2)}, u32[]{:S(2)}) collective-permute-start(bf16[32,2048]{1,0:T(8,128)(2,1)S(1)} %get-tuple-element.107), channel_id=1, source_target_pairs={{0,6},{1,7},{2,4},{3,5},{4,2},{5,3},{6,0},{7,1},{8,14},{9,15},{10,... | collective-permute-start | bytes 393224 | tf_op jit(solution)/shard_map/ppermute | solution.py:328
  118.5 17.3 %collective-permute-start.45 = (bf16[32,2048]{1,0:T(8,128)(2,1)S(1)}, bf16[32,2048]{1,0:T(8,128)(2,1)S(1)}, u32[]{:S(2)}, u32[]{:S(2)}) collective-permute-start(bf16[32,2048]{1,0:T(8,128)(2,1)S(1)} %get-tuple-element.108), channel_id=1, source_target_pairs={{0,7},{1,6},{2,5},{3,4},{4,3},{5,2},{6,1},{7,0},{8,15},{9,14},{10,... | collective-permute-start | bytes 393224 | tf_op jit(solution)/shard_map/ppermute | solution.py:328
  134.2 9.7 %collective-permute-start.51 = (bf16[64,2048]{1,0:T(8,128)(2,1)S(1)}, bf16[64,2048]{1,0:T(8,128)(2,1)S(1)}, u32[]{:S(2)}, u32[]{:S(2)}) collective-permute-start(bf16[64,2048]{1,0:T(8,128)(2,1)S(1)} %get-tuple-element.113), channel_id=1, source_target_pairs={{0,2},{2,0},{4,6},{6,4},{1,3},{3,1},{5,7},{7,5},{8,10},{10,8},{12,... | collective-permute-start | bytes 786440 | tf_op jit(solution)/shard_map/ppermute | solution.py:328
  135.8 9.3 %collective-permute-start.52 = (bf16[64,2048]{1,0:T(8,128)(2,1)S(1)}, bf16[64,2048]{1,0:T(8,128)(2,1)S(1)}, u32[]{:S(2)}, u32[]{:S(2)}) collective-permute-start(bf16[64,2048]{1,0:T(8,128)(2,1)S(1)} %get-tuple-element.114), channel_id=1, source_target_pairs={{0,4},{2,6},{4,0},{6,2},{1,5},{3,7},{5,1},{7,3},{8,12},{10,14},{12... | collective-permute-start | bytes 786440 | tf_op jit(solution)/shard_map/ppermute | solution.py:328
  136.9 14.1 %collective-permute-start.53 = (bf16[64,2048]{1,0:T(8,128)(2,1)S(1)}, bf16[64,2048]{1,0:T(8,128)(2,1)S(1)}, u32[]{:S(2)}, u32[]{:S(2)}) collective-permute-start(bf16[64,2048]{1,0:T(8,128)(2,1)S(1)} %get-tuple-element.115), channel_id=1, source_target_pairs={{0,6},{2,4},{4,2},{6,0},{1,7},{3,5},{5,3},{7,1},{8,14},{10,12},{12... | collective-permute-start | bytes 786440 | tf_op jit(solution)/shard_map/ppermute | solution.py:328
  138.8 32.7 %collective-permute-start.47 = (bf16[128,2048]{1,0:T(8,128)(2,1)S(1)}, bf16[128,2048]{1,0:T(8,128)(2,1)S(1)}, u32[]{:S(2)}, u32[]{:S(2)}) collective-permute-start(bf16[128,2048]{1,0:T(8,128)(2,1)S(1)} %get-tuple-element.110), channel_id=1, source_target_pairs={{0,8},{24,16},{1,9},{25,17},{2,10},{26,18},{3,11},{27,19},{4,12},{... | collective-permute-start | bytes 1572872 | tf_op jit(solution)/shard_map/ppermute | solution.py:407
  143.9 9.8 %collective-permute-start.26 = (bf16[32,2048]{1,0:T(8,128)(2,1)S(1)}, bf16[32,2048]{1,0:T(8,128)(2,1)S(1)}, u32[]{:S(2)}, u32[]{:S(2)}) collective-permute-start(bf16[32,2048]{1,0:T(8,128)(2,1)S(1)} %get-tuple-element.90), channel_id=1, source_target_pairs={{0,2},{1,3},{2,0},{3,1},{4,6},{5,7},{6,4},{7,5},{8,10},{9,11},{10,... | collective-permute-start | bytes 393224 | tf_op jit(solution)/shard_map/ppermute | solution.py:328
  145.0 11.4 %collective-permute-start.27 = (bf16[32,2048]{1,0:T(8,128)(2,1)S(1)}, bf16[32,2048]{1,0:T(8,128)(2,1)S(1)}, u32[]{:S(2)}, u32[]{:S(2)}) collective-permute-start(bf16[32,2048]{1,0:T(8,128)(2,1)S(1)} %get-tuple-element.91), channel_id=1, source_target_pairs={{0,3},{1,2},{2,1},{3,0},{4,7},{5,6},{6,5},{7,4},{8,11},{9,10},{10,... | collective-permute-start | bytes 393224 | tf_op jit(solution)/shard_map/ppermute | solution.py:328
  163.2 10.4 %collective-permute-start.57 = (bf16[32,2048]{1,0:T(8,128)(2,1)S(1)}, bf16[32,2048]{1,0:T(8,128)(2,1)S(1)}, u32[]{:S(2)}, u32[]{:S(2)}) collective-permute-start(bf16[32,2048]{1,0:T(8,128)(2,1)S(1)} %get-tuple-element.120), channel_id=1, source_target_pairs={{0,4},{1,5},{2,6},{3,7},{4,0},{5,1},{6,2},{7,3},{8,12},{9,13},{10,... | collective-permute-start | bytes 393224 | tf_op jit(solution)/shard_map/ppermute | solution.py:328
  167.1 9.5 %collective-permute-start.59 = (bf16[32,2048]{1,0:T(8,128)(2,1)S(1)}, bf16[32,2048]{1,0:T(8,128)(2,1)S(1)}, u32[]{:S(2)}, u32[]{:S(2)}) collective-permute-start(bf16[32,2048]{1,0:T(8,128)(2,1)S(1)} %get-tuple-element.122), channel_id=1, source_target_pairs={{0,6},{1,7},{2,4},{3,5},{4,2},{5,3},{6,0},{7,1},{8,14},{9,15},{10,... | collective-permute-start | bytes 393224 | tf_op jit(solution)/shard_map/ppermute | solution.py:328
  169.8 9.6 %collective-permute-start.60 = (bf16[32,2048]{1,0:T(8,128)(2,1)S(1)}, bf16[32,2048]{1,0:T(8,128)(2,1)S(1)}, u32[]{:S(2)}, u32[]{:S(2)}) collective-permute-start(bf16[32,2048]{1,0:T(8,128)(2,1)S(1)} %get-tuple-element.123), channel_id=1, source_target_pairs={{0,7},{1,6},{2,5},{3,4},{4,3},{5,2},{6,1},{7,0},{8,15},{9,14},{10,... | collective-permute-start | bytes 393224 | tf_op jit(solution)/shard_map/ppermute | solution.py:328
  171.5 13.6 %collective-permute-start.32 = (bf16[128,2048]{1,0:T(8,128)(2,1)S(1)}, bf16[128,2048]{1,0:T(8,128)(2,1)S(1)}, u32[]{:S(2)}, u32[]{:S(2)}) collective-permute-start(bf16[128,2048]{1,0:T(8,128)(2,1)S(1)} %get-tuple-element.96), channel_id=1, source_target_pairs={{0,8},{24,16},{1,9},{25,17},{2,10},{26,18},{3,11},{27,19},{4,12},{... | collective-permute-start | bytes 1572872 | tf_op jit(solution)/shard_map/ppermute | solution.py:407
  173.6 22.7 %collective-permute-start.6 = (bf16[64,2048]{1,0:T(8,128)(2,1)S(1)}, bf16[64,2048]{1,0:T(8,128)(2,1)S(1)}, u32[]{:S(2)}, u32[]{:S(2)}) collective-permute-start(bf16[64,2048]{1,0:T(8,128)(2,1)S(1)} %get-tuple-element.72), channel_id=1, source_target_pairs={{0,2},{2,0},{4,6},{6,4},{1,3},{3,1},{5,7},{7,5},{8,10},{10,8},{12,... | collective-permute-start | bytes 786440 | tf_op jit(solution)/shard_map/ppermute | solution.py:328
  173.8 22.4 %collective-permute-start.7 = (bf16[64,2048]{1,0:T(8,128)(2,1)S(1)}, bf16[64,2048]{1,0:T(8,128)(2,1)S(1)}, u32[]{:S(2)}, u32[]{:S(2)}) collective-permute-start(bf16[64,2048]{1,0:T(8,128)(2,1)S(1)} %get-tuple-element.73), channel_id=1, source_target_pairs={{0,4},{2,6},{4,0},{6,2},{1,5},{3,7},{5,1},{7,3},{8,12},{10,14},{12... | collective-permute-start | bytes 786440 | tf_op jit(solution)/shard_map/ppermute | solution.py:328
  176.6 19.6 %collective-permute-start.8 = (bf16[64,2048]{1,0:T(8,128)(2,1)S(1)}, bf16[64,2048]{1,0:T(8,128)(2,1)S(1)}, u32[]{:S(2)}, u32[]{:S(2)}) collective-permute-start(bf16[64,2048]{1,0:T(8,128)(2,1)S(1)} %get-tuple-element.74), channel_id=1, source_target_pairs={{0,6},{2,4},{4,2},{6,0},{1,7},{3,5},{5,3},{7,1},{8,14},{10,12},{12... | collective-permute-start | bytes 786440 | tf_op jit(solution)/shard_map/ppermute | solution.py:328
  185.2 32.4 %collective-permute-start.46 = (bf16[128,2048]{1,0:T(8,128)(2,1)S(1)}, bf16[128,2048]{1,0:T(8,128)(2,1)S(1)}, u32[]{:S(2)}, u32[]{:S(2)}) collective-permute-start(bf16[128,2048]{1,0:T(8,128)(2,1)S(1)} %add_convert_fusion.3), channel_id=1, source_target_pairs={{8,16},{16,8},{9,17},{17,9},{10,18},{18,10},{11,19},{19,11},{12,20... | collective-permute-start | bytes 1572872 | tf_op jit(solution)/shard_map/ppermute | solution.py:407
  186.0 31.6 %collective-permute-start.61 = (bf16[128,2048]{1,0:T(8,128)(2,1)S(1)}, bf16[128,2048]{1,0:T(8,128)(2,1)S(1)}, u32[]{:S(2)}, u32[]{:S(2)}) collective-permute-start(bf16[128,2048]{1,0:T(8,128)(2,1)S(1)} %add_convert_fusion.1), channel_id=1, source_target_pairs={{0,8},{8,0},{16,24},{24,16},{1,9},{9,1},{17,25},{25,17},{2,10},{10... | collective-permute-start | bytes 1572872 | tf_op jit(solution)/shard_map/ppermute | solution.py:407
  (47 other events, 491.5 us)
where the time goes:
time: 219 us
  starting transfers between devices  96 us (44%)
  waiting for transfers between devices  85.3 us (39%)
  Pallas kernels  21.5 us (10%)
  local copies, waits for them, and re-layouts  10 us (5%)
  other arithmetic  5.28 us (2%)
    ppermute x43, waiting for transfers between devices, exchange(): lax.ppermute(pieces[k], axes, flips(count, k))  50.2 us
    ppermute x43, starting transfers between devices, exchange(): lax.ppermute(pieces[k], axes, flips(count, k))  39 us
    ppermute x5, starting transfers between devices, hop(): return lax.ppermute(block.astype(BF16), 'z', route).astype(F32)  15.6 us
    ppermute x1, starting transfers between devices, gather_line(): side_end = lax.ppermute(across_far, 'z', sides)  15.5 us
    ppermute x1, waiting for transfers between devices, gather_line(): near = lax.ppermute(own, 'z', sides)  12.4 us
    pallas_call x4, Pallas kernels, expert_rows(): pl.pallas_call(functools.partial(expert_kernel, parts, count), out_shape=...  11.5 us
    ppermute x1, starting transfers between devices, gather_line(): side_far = lax.ppermute(across, 'z', sides)  9.6 us
    unnamed x34, local copies, waits for them, and re-layouts  9.21 us
  transfers between devices with their start and end apart: 62, of which 28 were waited for; matrix products, arithmetic and copies ran while one was open for 2% of the time, Pallas kernels for 9%

commit v1 on v0

--- a/solution.py
+++ b/solution.py
@@ -9,6 +9,7 @@
 
 
 SEQ, TP, CHIPS, PLANE = ("z", "x"), ("y", "c"), ("x", "y"), ("x", "y", "c")
+MIDDLE = [(1, 2), (2, 1)]
 BF16, F32 = jnp.bfloat16, jnp.float32
 
 
@@ -18,7 +19,7 @@
 
 def from_behind(block, distance):
     count = lax.axis_size(SEQ)
-    route = [(i - distance, i) for i in range(distance, count)]
+    route = [((i - distance) % count, i) for i in range(count)]
     return lax.ppermute(block, SEQ, route)
 
 
@@ -31,39 +32,95 @@
     return pl.CostEstimate(flops=flops, bytes_accessed=size, transcendentals=0)
 
 
-def filter_kernel(parts, taps_count, me_ref, gate_ref, in_ref, val_ref, taps_ref, halo_ref, *rest):
-    outs, scratch = rest[:parts], rest[parts]
+def filter_kernel(parts, back, me_ref, gate_ref, in_ref, val_ref, taps_ref, *rest):
+    outs, head_ref, scratch = rest[:parts], rest[parts], rest[parts + 1]
     length = val_ref.shape[0]
     rows = length // parts
-    back = taps_count - 1
     scratch[0:8] = jnp.zeros((8, scratch.shape[1]), F32)
-    scratch[8 - back : 8] = halo_ref[...]
     scratch[8:] = in_ref[...].astype(F32) * val_ref[...].astype(F32)
     me = me_ref[0]
     for k in range(parts):
         start = pl.multiple_of((me ^ k) * rows, 16)
         window = scratch[pl.ds(start, rows + 8)]
         total = taps_ref[0:1] * window[8 - back : 8 - back + rows]
-        for offset in range(1, taps_count):
+        for offset in range(1, back + 1):
             first = 8 - back + offset
             total = total + taps_ref[offset : offset + 1] * window[first : first + rows]
         outs[k][...] = (gate_ref[pl.ds(start, rows)].astype(F32) * total).astype(BF16)
-
-
-def filter_rows(me, out_gate, in_gate, conv_values, conv_taps, halo, parts):
+    window = scratch[0:24]
+    total = taps_ref[0:1] * window[8 - back : 24 - back]
+    for offset in range(1, back + 1):
+        first = 8 - back + offset
+        total = total + taps_ref[offset : offset + 1] * window[first : first + 16]
+    head_ref[0:16] = total
+    head_ref[16:32] = gate_ref[0:16].astype(F32)
+
+
+def filter_rows(me, out_gate, in_gate, conv_values, conv_taps, parts):
     length, channels = conv_values.shape
     out = jax.ShapeDtypeStruct((length // parts, channels), BF16)
     whole = pl.BlockSpec(memory_space=pltpu.VMEM)
-    return pl.pallas_call(
-        functools.partial(filter_kernel, parts, conv_taps.shape[0]),
-        out_shape=[out] * parts,
-        in_specs=[pl.BlockSpec(memory_space=pltpu.SMEM)] + [whole] * 5,
+    *blocks, head = pl.pallas_call(
+        functools.partial(filter_kernel, parts, conv_taps.shape[0] - 1),
+        out_shape=[pltpu.VMEM(out.shape, BF16)] * parts + [pltpu.VMEM((32, channels), F32)],
+        in_specs=[pl.BlockSpec(memory_space=pltpu.SMEM)] + [whole] * 4,
+        out_specs=[whole] * (parts + 1),
+        scratch_shapes=[pltpu.VMEM((length + 8, channels), F32)],
+        cost_estimate=cost(1 << 20, [out_gate, in_gate, conv_values]),
+        name="filter_rows",
+    )(me, out_gate, in_gate, conv_values, conv_taps)
+    return blocks, head
+
+
+def mend_kernel(parts, back, me_ref, head_ref, taps_ref, halo_ref, *refs):
+    outs = refs[parts:]
+    channels = head_ref.shape[1]
+    row = lax.broadcasted_iota(jnp.int32, (16, channels), 0)
+    total = head_ref[0:16]
+    for offset in range(back):
+        for at_row in range(back - offset):
+            term = taps_ref[offset : offset + 1] * halo_ref[at_row + offset : at_row + offset + 1]
+            total = total + jnp.where((row == at_row) & (me_ref[1] > 0), term, 0.0)
+    fresh = (head_ref[16:32] * total).astype(BF16)
+    for k in range(parts):
+
+        @pl.when(me_ref[0] == k)
+        def _(k=k):
+            outs[k][0:16] = fresh
+
+
+def mend_rows(me, blocks, head, conv_taps, halo):
+    parts = len(blocks)
+    whole = pl.BlockSpec(memory_space=pltpu.VMEM)
+    return pl.pallas_call(
+        functools.partial(mend_kernel, parts, conv_taps.shape[0] - 1),
+        out_shape=[pltpu.VMEM(blocks[0].shape, BF16)] * parts,
+        in_specs=[pl.BlockSpec(memory_space=pltpu.SMEM)] + [whole] * (3 + parts),
         out_specs=[whole] * parts,
-        scratch_shapes=[pltpu.VMEM((length + 8, channels), F32)],
-        cost_estimate=cost(8 * out_gate.size, [out_gate, in_gate, conv_values]),
+        input_output_aliases={4 + k: k for k in range(parts)},
+        cost_estimate=cost(1 << 20, blocks),
         compiler_params=grant(8),
-        name="filter_rows",
-    )(me, out_gate, in_gate, conv_values, conv_taps, halo)
+        name="mend_rows",
+    )(me, head, conv_taps, halo, *blocks)
+
+
+def fetch_kernel(from_ref, to_ref, sem):
+    copy = pltpu.make_async_copy(from_ref, to_ref, sem)
+    copy.start()
+    copy.wait()
+
+
+def fetch(array):
+    return pl.pallas_call(
+        fetch_kernel,
+        out_shape=pltpu.VMEM(array.shape, array.dtype),
+        in_specs=[pl.BlockSpec(memory_space=pltpu.HBM)],
+        out_specs=pl.BlockSpec(memory_space=pltpu.VMEM),
+        scratch_shapes=[pltpu.SemaphoreType.DMA],
+        cost_estimate=cost(1 << 20, [array]),
+        compiler_params=grant(1),
+        name="fetch_rows",
+    )(array)
 
 
 def mix_kernel(parts, me_ref, *refs):
@@ -314,7 +371,7 @@
 def gather_line(own, count):
     if count != 4:
         return [own] + [lax.ppermute(own, "z", flips(count, j)) for j in range(1, count)]
-    sides, middle = flips(4, 1), [(1, 2), (2, 1)]
+    sides, middle = flips(4, 1), MIDDLE
     near = lax.ppermute(own, "z", sides)
     across = lax.ppermute(own, "z", middle)
     across_far = lax.ppermute(near, "z", middle)
@@ -356,9 +413,11 @@
     length = conv_values.shape[0]
     tail = in_gate[length - back :].astype(F32) * conv_values[length - back :].astype(F32)
     halo = from_behind(tail, 1)
-    me = tp_index.reshape(1).astype(jnp.int32)
-    blocks = filter_rows(me, out_gate, in_gate, conv_values, conv_taps, halo, tp_count)
+    me = jnp.stack([tp_index, lax.axis_index(SEQ)]).astype(jnp.int32)
+    blocks, head = filter_rows(me, out_gate, in_gate, conv_values, conv_taps, tp_count)
+    blocks = mend_rows(me, blocks, head, conv_taps, halo)
     pieces = exchange(blocks, TP)
+    out_proj = fetch(out_proj)
 
     row_count, top_count = routes.shape
     capacity = max(2, 4 * row_count * top_count // (6 * z_count * chips))
@@ -401,15 +460,15 @@
         partial[j], short[j] = combine(returned, tables[j])
 
     if z_count == 4:
-        outward, middle, sides = [(0, 1), (3, 2)], [(1, 2), (2, 1)], flips(4, 1)
+        sides = flips(4, 1)
 
         def hop(block, route):
             return lax.ppermute(block.astype(BF16), "z", route).astype(F32)
 
-        far = hop(short[3], outward)
-        mid = hop(short[2], outward)
-        far = hop(far + partial[2], middle)
-        mid = hop(mid + partial[3], middle)
+        far = hop(short[3], sides)
+        mid = hop(short[2], sides)
+        far = hop(far + partial[2], MIDDLE)
+        mid = hop(mid + partial[3], MIDDLE)
         last = hop(far + partial[1], sides)
         routed = partial[0] + mid + last
     else:

time: 219 us -> 211 us (0.963)
  starting transfers between devices: 96 us -> 83.5 us
  waiting for transfers between devices: 85.3 us -> 90.9 us
  local copies, waits for them, and re-layouts: 10 us -> 5.92 us
  Pallas kernels: 21.5 us -> 24.2 us
    ppermute x5, starting transfers between devices: 15.6 us -> 11.2 us  [hop(): return lax.ppermute(block.astype(BF16), 'z', route).astype(F32)]
    unnamed x34 -> x32, local copies, waits for them, and re-layouts: 9.21 us -> 5.12 us
    ppermute x1, starting transfers between devices: 3.26 us -> 0.01 us  [gather_line(): near = lax.ppermute(own, 'z', sides)]
  transfers between devices with their start and end apart: 62 -> 62, of which waited for: 28 -> 27; matrix products, arithmetic and copies ran while one was open for 2% -> 2% of each run, Pallas kernels for 9% -> 10%
where the time goes in v1:
time: 211 us
  waiting for transfers between devices  90.9 us (43%)
  starting transfers between devices  83.5 us (40%)
  Pallas kernels  24.2 us (11%)
  local copies, waits for them, and re-layouts  5.92 us (3%)
  other arithmetic  5.88 us (3%)
    ppermute x43, waiting for transfers between devices, exchange(): lax.ppermute(pieces[k], axes, flips(count, k))  51.6 us
    ppermute x43, starting transfers between devices, exchange(): lax.ppermute(pieces[k], axes, flips(count, k))  38.6 us
    ppermute x1, waiting for transfers between devices, gather_line(): near = lax.ppermute(own, 'z', sides)  14.1 us
    ppermute x1, starting transfers between devices, gather_line(): side_end = lax.ppermute(across_far, 'z', sides)  14.1 us
    pallas_call x4, Pallas kernels, expert_rows(): pl.pallas_call(functools.partial(expert_kernel, parts, count), out_shape=...  11.5 us
    ppermute x5, starting transfers between devices, hop(): return lax.ppermute(block.astype(BF16), 'z', route).astype(F32)  11.2 us
    ppermute x3, waiting for transfers between devices, layer(): lax.ppermute(table[j], 'z', flips(z_count, j))  10.1 us
    ppermute x1, starting transfers between devices, gather_line(): side_far = lax.ppermute(across, 'z', sides)  9.8 us
  transfers between devices with their start and end apart: 62, of which 27 were waited for; matrix products, arithmetic and copies ran while one was open for 2% of the time, Pallas kernels for 10%

profile of v1, /device:TPU:0, one launch (start us, length us, event | category | flops | bytes accessed | tf_op | source)
XLA Modules:
  0.0 211.0 jit_solution(2560467511883376888)
XLA Ops:
  0.7 3.0 %collective-permute-start = (f32[2,384]{1,0:T(2,128)S(1)}, f32[2,384]{1,0:T(2,128)S(1)}, u32[]{:S(2)}, u32[]{:S(2)}) collective-permute-start(f32[2,384]{1,0:T(2,128)S(1)} %convert_multiply_fusion), channel_id=1, source_target_pairs={{28,0},{0,4},{4,8},{8,12},{12,16},{16,20},{20,24},{24,28},{29,1},{... | collective-permute-start | bytes 9224 | tf_op jit(solution)/shard_map/ppermute | solution.py:23
  4.3 1.9 filter_rows.1
  6.2 2.1 %collective-permute-done.halo_ref = f32[2,384]{1,0:T(2,128)S(1)} collective-permute-done((f32[2,384]{1,0:T(2,128)S(1)}, f32[2,384]{1,0:T(2,128)S(1)}, u32[]{:S(2)}, u32[]{:S(2)}) %collective-permute-start) | collective-permute-done | bytes 3104 | tf_op jit(solution)/shard_map/ppermute | solution.py:23
  12.8 2.8 %copy-done.3 = bf16[1536,2048]{1,0:T(8,128)(2,1)S(1)} copy-done((bf16[1536,2048]{1,0:T(8,128)(2,1)S(1)}, bf16[1536,2048]{1,0:T(8,128)(2,1)}, u32[]{:S(2)}) %copy-start.3) | copy-done | bytes 6291480
  17.2 2.7 %mix_project.1 = (f32[128,2048]{1,0:T(8,128)S(1)}, bf16[128,2048]{1,0:T(8,128)(2,1)S(1)}) custom-call(s32[2]{0:T(128)S(1)} %copy-done.13, bf16[128,384]{1,0:T(8,128)(2,1)S(1)} %get-tuple-element.75.refs_0_, bf16[128,384]{1,0:T(8,128)(2,1)S(1)} %collective-permute-done.1.refs_1_, bf16[128,384]{1,0:T(8,128)(2,1)S(1)} %collective-permute-done.2.refs_2_, ...), custom_call_target="tpu_custom_call" | custom-call | flops 805306368 | bytes 8388608 | tf_op jit(solution)/shard_map/mix_project/pallas_call | solution.py:183
  20.8 14.1 %collective-permute-done.16.own_ref = bf16[128,2048]{1,0:T(8,128)(2,1)S(1)} collective-permute-done((bf16[128,2048]{1,0:T(8,128)(2,1)S(1)}, bf16[128,2048]{1,0:T(8,128)(2,1)S(1)}, u32[]{:S(2)}, u32[]{:S(2)}) %collective-permute-start.16) | collective-permute-done | bytes 524320 | tf_op jit(solution)/shard_map/ppermute | solution.py:375
  37.9 14.1 %collective-permute-start.33 = (bf16[128,2048]{1,0:T(8,128)(2,1)}, bf16[128,2048]{1,0:T(8,128)(2,1)}, u32[]{:S(2)}, u32[]{:S(2)}) collective-permute-start(bf16[128,2048]{1,0:T(8,128)(2,1)} %collective-permute-done.17), channel_id=1, source_target_pairs={{0,8},{8,0},{16,24},{24,16},{1,9},{9,1},{17,25},{25,17},{2,10},{10... | collective-permute-start | bytes 1572872 | tf_op jit(solution)/shard_map/ppermute | solution.py:379
  52.2 9.8 %collective-permute-start.19 = (bf16[128,2048]{1,0:T(8,128)(2,1)}, bf16[128,2048]{1,0:T(8,128)(2,1)}, u32[]{:S(2)}, u32[]{:S(2)}) collective-permute-start(bf16[128,2048]{1,0:T(8,128)(2,1)} %collective-permute-done.18), channel_id=1, source_target_pairs={{0,8},{8,0},{16,24},{24,16},{1,9},{9,1},{17,25},{25,17},{2,10},{10... | collective-permute-start | bytes 1572872 | tf_op jit(solution)/shard_map/ppermute | solution.py:378
  64.4 8.8 %collective-permute-done.19 = bf16[128,2048]{1,0:T(8,128)(2,1)} collective-permute-done((bf16[128,2048]{1,0:T(8,128)(2,1)}, bf16[128,2048]{1,0:T(8,128)(2,1)}, u32[]{:S(2)}, u32[]{:S(2)}) %collective-permute-start.19) | collective-permute-done | bytes 524320 | tf_op jit(solution)/shard_map/ppermute | solution.py:378
  76.4 3.8 %collective-permute-done.35.table_ref.refs_8_ = f32[20,128]{1,0:T(8,128)S(1)} collective-permute-done((f32[20,128]{1,0:T(8,128)S(1)}, f32[20,128]{1,0:T(8,128)S(1)}, u32[]{:S(2)}, u32[]{:S(2)}) %collective-permute-start.35) | collective-permute-done | bytes 10272 | tf_op jit(solution)/shard_map/ppermute | solution.py:440
  80.7 1.9 collective-permute-start.36
  84.4 4.4 %collective-permute-done.21.table_ref.refs_8_ = f32[20,128]{1,0:T(8,128)S(1)} collective-permute-done((f32[20,128]{1,0:T(8,128)S(1)}, f32[20,128]{1,0:T(8,128)S(1)}, u32[]{:S(2)}, u32[]{:S(2)}) %collective-permute-start.21) | collective-permute-done | bytes 10272 | tf_op jit(solution)/shard_map/ppermute | solution.py:440
  89.2 1.9 collective-permute-start.22
  91.8 3.6 %collective-permute-done.38.refs_3_ = bf16[64,2048]{1,0:T(8,128)(2,1)S(1)} collective-permute-done((bf16[64,2048]{1,0:T(8,128)(2,1)S(1)}, bf16[64,2048]{1,0:T(8,128)(2,1)S(1)}, u32[]{:S(2)}, u32[]{:S(2)}) %collective-permute-start.38) | collective-permute-done | bytes 262176 | tf_op jit(solution)/shard_map/ppermute | solution.py:385
  95.4 2.9 %expert_rows.6 = (bf16[32,2048]{1,0:T(8,128)(2,1)S(1)}, bf16[32,2048]{1,0:T(8,128)(2,1)S(1)}, bf16[32,2048]{1,0:T(8,128)(2,1)S(1)}, bf16[32,2048]{1,0:T(8,128)(2...) custom-call(bf16[64,2048]{1,0:T(8,128)(2,1)S(1)} %get-tuple-element., ...), custom_call_target="tpu_custom_call" | custom-call | flops 1610612736 | bytes 6291456 | tf_op jit(solution)/shard_map/expert_rows/pallas_call | solution.py:268
  100.1 1.9 collective-permute-done.50.table_ref.refs_8_
  112.8 14.0 %collective-permute-done.44.refs_6_ = bf16[32,2048]{1,0:T(8,128)(2,1)S(1)} collective-permute-done((bf16[32,2048]{1,0:T(8,128)(2,1)S(1)}, bf16[32,2048]{1,0:T(8,128)(2,1)S(1)}, u32[]{:S(2)}, u32[]{:S(2)}) %collective-permute-start.44) | collective-permute-done | bytes 131104 | tf_op jit(solution)/shard_map/ppermute | solution.py:385
  129.2 2.4 %collective-permute-start.53 = (bf16[64,2048]{1,0:T(8,128)(2,1)S(1)}, bf16[64,2048]{1,0:T(8,128)(2,1)S(1)}, u32[]{:S(2)}, u32[]{:S(2)}) collective-permute-start(bf16[64,2048]{1,0:T(8,128)(2,1)S(1)} %get-tuple-element.125), channel_id=1, source_target_pairs={{0,6},{2,4},{4,2},{6,0},{1,7},{3,5},{5,3},{7,1},{8,14},{10,12},{12... | collective-permute-start | bytes 786440 | tf_op jit(solution)/shard_map/ppermute | solution.py:385
  131.6 2.9 %expert_rows.5 = (bf16[32,2048]{1,0:T(8,128)(2,1)S(1)}, bf16[32,2048]{1,0:T(8,128)(2,1)S(1)}, bf16[32,2048]{1,0:T(8,128)(2,1)S(1)}, bf16[32,2048]{1,0:T(8,128)(2...) custom-call(bf16[64,2048]{1,0:T(8,128)(2,1)S(1)} %get-tuple-element., ...), custom_call_target="tpu_custom_call" | custom-call | flops 1610612736 | bytes 6291456 | tf_op jit(solution)/shard_map/expert_rows/pallas_call | solution.py:268
  138.2 5.6 %collective-permute-done.53.refs_3_ = bf16[64,2048]{1,0:T(8,128)(2,1)S(1)} collective-permute-done((bf16[64,2048]{1,0:T(8,128)(2,1)S(1)}, bf16[64,2048]{1,0:T(8,128)(2,1)S(1)}, u32[]{:S(2)}, u32[]{:S(2)}) %collective-permute-start.53) | collective-permute-done | bytes 262176 | tf_op jit(solution)/shard_map/ppermute | solution.py:385
  146.6 1.8 collective-permute-done.27.refs_3_
  148.8 2.9 %expert_rows.7 = (bf16[32,2048]{1,0:T(8,128)(2,1)S(1)}, bf16[32,2048]{1,0:T(8,128)(2,1)S(1)}, bf16[32,2048]{1,0:T(8,128)(2,1)S(1)}, bf16[32,2048]{1,0:T(8,128)(2...) custom-call(bf16[64,2048]{1,0:T(8,128)(2,1)S(1)} %get-tuple-element., ...), custom_call_target="tpu_custom_call" | custom-call | flops 1610612736 | bytes 6291456 | tf_op jit(solution)/shard_map/expert_rows/pallas_call | solution.py:268
  157.6 2.2 %collective-permute-start.58 = (bf16[32,2048]{1,0:T(8,128)(2,1)S(1)}, bf16[32,2048]{1,0:T(8,128)(2,1)S(1)}, u32[]{:S(2)}, u32[]{:S(2)}) collective-permute-start(bf16[32,2048]{1,0:T(8,128)(2,1)S(1)} %get-tuple-element.131), channel_id=1, source_target_pairs={{0,5},{1,4},{2,7},{3,6},{4,1},{5,0},{6,3},{7,2},{8,13},{9,12},{10,... | collective-permute-start | bytes 393224 | tf_op jit(solution)/shard_map/ppermute | solution.py:385
  166.3 3.2 %collective-permute-done.59.refs_6_ = bf16[32,2048]{1,0:T(8,128)(2,1)S(1)} collective-permute-done((bf16[32,2048]{1,0:T(8,128)(2,1)S(1)}, bf16[32,2048]{1,0:T(8,128)(2,1)S(1)}, u32[]{:S(2)}, u32[]{:S(2)}) %collective-permute-start.59) | collective-permute-done | bytes 131104 | tf_op jit(solution)/shard_map/ppermute | solution.py:385
  170.0 2.2 %collective-permute-done.60.refs_7_ = bf16[32,2048]{1,0:T(8,128)(2,1)S(1)} collective-permute-done((bf16[32,2048]{1,0:T(8,128)(2,1)S(1)}, bf16[32,2048]{1,0:T(8,128)(2,1)S(1)}, u32[]{:S(2)}, u32[]{:S(2)}) %collective-permute-start.60) | collective-permute-done | bytes 131104 | tf_op jit(solution)/shard_map/ppermute | solution.py:385
  174.2 4.1 %collective-permute-done.32 = bf16[128,2048]{1,0:T(8,128)(2,1)S(1)} collective-permute-done((bf16[128,2048]{1,0:T(8,128)(2,1)S(1)}, bf16[128,2048]{1,0:T(8,128)(2,1)S(1)}, u32[]{:S(2)}, u32[]{:S(2)}) %collective-permute-start.32) | collective-permute-done | bytes 524320 | tf_op jit(solution)/shard_map/ppermute | solution.py:466
  179.4 9.6 %collective-permute-start.61 = (bf16[128,2048]{1,0:T(8,128)(2,1)S(1)}, bf16[128,2048]{1,0:T(8,128)(2,1)S(1)}, u32[]{:S(2)}, u32[]{:S(2)}) collective-permute-start(bf16[128,2048]{1,0:T(8,128)(2,1)S(1)} %add_convert_fusion.1), channel_id=1, source_target_pairs={{0,8},{8,0},{16,24},{24,16},{1,9},{9,1},{17,25},{25,17},{2,10},{10... | collective-permute-start | bytes 1572872 | tf_op jit(solution)/shard_map/ppermute | solution.py:466
  189.1 2.9 %expert_rows.4 = (bf16[32,2048]{1,0:T(8,128)(2,1)S(1)}, bf16[32,2048]{1,0:T(8,128)(2,1)S(1)}, bf16[32,2048]{1,0:T(8,128)(2,1)S(1)}, bf16[32,2048]{1,0:T(8,128)(2...) custom-call(bf16[64,2048]{1,0:T(8,128)(2,1)S(1)} %get-tuple-element., ...), custom_call_target="tpu_custom_call" | custom-call | flops 1610612736 | bytes 6291456 | tf_op jit(solution)/shard_map/expert_rows/pallas_call | solution.py:268
  193.4 4.9 %collective-permute-done.10.refs_2_ = bf16[32,2048]{1,0:T(8,128)(2,1)S(1)} collective-permute-done((bf16[32,2048]{1,0:T(8,128)(2,1)S(1)}, bf16[32,2048]{1,0:T(8,128)(2,1)S(1)}, u32[]{:S(2)}, u32[]{:S(2)}) %collective-permute-start.10) | collective-permute-done | bytes 131104 | tf_op jit(solution)/shard_map/ppermute | solution.py:385
  199.2 2.6 %collective-permute-start.15 = (bf16[32,2048]{1,0:T(8,128)(2,1)S(1)}, bf16[32,2048]{1,0:T(8,128)(2,1)S(1)}, u32[]{:S(2)}, u32[]{:S(2)}) collective-permute-start(bf16[32,2048]{1,0:T(8,128)(2,1)S(1)} %get-tuple-element.92), channel_id=1, source_target_pairs={{0,7},{1,6},{2,5},{3,4},{4,3},{5,2},{6,1},{7,0},{8,15},{9,14},{10,... | collective-permute-start | bytes 393224 | tf_op jit(solution)/shard_map/ppermute | solution.py:385
  202.6 2.0 shared_rows.1
  205.8 2.8 %collective-permute-done.15.refs_7_ = bf16[32,2048]{1,0:T(8,128)(2,1)S(1)} collective-permute-done((bf16[32,2048]{1,0:T(8,128)(2,1)S(1)}, bf16[32,2048]{1,0:T(8,128)(2,1)S(1)}, u32[]{:S(2)}, u32[]{:S(2)}) %collective-permute-start.15) | collective-permute-done | bytes 131104 | tf_op jit(solution)/shard_map/ppermute | solution.py:385
  (163 shorter events, 64.9 us)
Async XLA Ops:
  20.8 14.1 %collective-permute-start.16 = (bf16[128,2048]{1,0:T(8,128)(2,1)S(1)}, bf16[128,2048]{1,0:T(8,128)(2,1)S(1)}, u32[]{:S(2)}, u32[]{:S(2)}) collective-permute-start(bf16[128,2048]{1,0:T(8,128)(2,1)S(1)} %get-tuple-element.79.rows_ref.own_ref), channel_id=1, source_target_pairs={{0,8},{8,0},{16,24},{24,16},{1,9},{9,1},{17,25},{25,17},{2,10},{10... | collective-permute-start | bytes 1572872 | tf_op jit(solution)/shard_map/ppermute | solution.py:375
  36.4 15.8 %collective-permute-start.18 = (bf16[128,2048]{1,0:T(8,128)(2,1)S(1)}, bf16[128,2048]{1,0:T(8,128)(2,1)}, u32[]{:S(2)}, u32[]{:S(2)}) collective-permute-start(bf16[128,2048]{1,0:T(8,128)(2,1)S(1)} %get-tuple-element.79.rows_ref.own_ref), channel_id=1, source_target_pairs={{8,16},{16,8},{9,17},{17,9},{10,18},{18,10},{11,19},{19,11},{12,20... | collective-permute-start | bytes 1572872 | tf_op jit(solution)/shard_map/ppermute | solution.py:376
  37.9 24.3 %collective-permute-start.33 = (bf16[128,2048]{1,0:T(8,128)(2,1)}, bf16[128,2048]{1,0:T(8,128)(2,1)}, u32[]{:S(2)}, u32[]{:S(2)}) collective-permute-start(bf16[128,2048]{1,0:T(8,128)(2,1)} %collective-permute-done.17), channel_id=1, source_target_pairs={{0,8},{8,0},{16,24},{24,16},{1,9},{9,1},{17,25},{25,17},{2,10},{10... | collective-permute-start | bytes 1572872 | tf_op jit(solution)/shard_map/ppermute | solution.py:379
  52.2 21.1 %collective-permute-start.19 = (bf16[128,2048]{1,0:T(8,128)(2,1)}, bf16[128,2048]{1,0:T(8,128)(2,1)}, u32[]{:S(2)}, u32[]{:S(2)}) collective-permute-start(bf16[128,2048]{1,0:T(8,128)(2,1)} %collective-permute-done.18), channel_id=1, source_target_pairs={{0,8},{8,0},{16,24},{24,16},{1,9},{9,1},{17,25},{25,17},{2,10},{10... | collective-permute-start | bytes 1572872 | tf_op jit(solution)/shard_map/ppermute | solution.py:378
  62.2 12.4 %collective-permute-start.5 = (f32[4,4,128]{2,1,0:T(4,128)S(1)}, f32[4,4,128]{2,1,0:T(4,128)S(1)}, u32[]{:S(2)}, u32[]{:S(2)}) collective-permute-start(f32[4,4,128]{2,1,0:T(4,128)S(1)} %slice.28), channel_id=1, source_target_pairs={{0,1},{1,0},{2,3},{3,2},{4,5},{5,4},{6,7},{7,6},{8,9},{9,8},{10,11... | collective-permute-start | bytes 24584 | tf_op jit(solution)/shard_map/ppermute | solution.py:437
  63.8 16.5 %collective-permute-start.34 = (bf16[128,2048]{1,0:T(8,128)(2,1)S(1)}, bf16[128,2048]{1,0:T(8,128)(2,1)S(1)}, u32[]{:S(2)}, u32[]{:S(2)}) collective-permute-start(bf16[128,2048]{1,0:T(8,128)(2,1)S(1)} %add.82.own_ref), channel_id=1, source_target_pairs={{0,1},{1,0},{2,3},{3,2},{4,5},{5,4},{6,7},{7,6},{8,9},{9,8},{10,11... | collective-permute-start | bytes 1572872 | tf_op jit(solution)/shard_map/ppermute | solution.py:449
  74.6 14.3 %collective-permute-start.20 = (bf16[128,2048]{1,0:T(8,128)(2,1)S(1)}, bf16[128,2048]{1,0:T(8,128)(2,1)S(1)}, u32[]{:S(2)}, u32[]{:S(2)}) collective-permute-start(bf16[128,2048]{1,0:T(8,128)(2,1)S(1)} %add.81.own_ref), channel_id=1, source_target_pairs={{0,1},{1,0},{2,3},{3,2},{4,5},{5,4},{6,7},{7,6},{8,9},{9,8},{10,11... | collective-permute-start | bytes 1572872 | tf_op jit(solution)/shard_map/ppermute | solution.py:449
  80.7 10.5 %collective-permute-start.36 = (bf16[64,2048]{1,0:T(8,128)(2,1)S(1)}, bf16[64,2048]{1,0:T(8,128)(2,1)S(1)}, u32[]{:S(2)}, u32[]{:S(2)}) collective-permute-start(bf16[64,2048]{1,0:T(8,128)(2,1)S(1)} %get-tuple-element.108), channel_id=1, source_target_pairs={{0,2},{2,0},{4,6},{6,4},{1,3},{3,1},{5,7},{7,5},{8,10},{10,8},{12,... | collective-permute-start | bytes 786440 | tf_op jit(solution)/shard_map/ppermute | solution.py:385
  82.6 9.2 %collective-permute-start.37 = (bf16[64,2048]{1,0:T(8,128)(2,1)S(1)}, bf16[64,2048]{1,0:T(8,128)(2,1)S(1)}, u32[]{:S(2)}, u32[]{:S(2)}) collective-permute-start(bf16[64,2048]{1,0:T(8,128)(2,1)S(1)} %get-tuple-element.109), channel_id=1, source_target_pairs={{0,4},{2,6},{4,0},{6,2},{1,5},{3,7},{5,1},{7,3},{8,12},{10,14},{12... | collective-permute-start | bytes 786440 | tf_op jit(solution)/shard_map/ppermute | solution.py:385
  82.7 12.7 %collective-permute-start.38 = (bf16[64,2048]{1,0:T(8,128)(2,1)S(1)}, bf16[64,2048]{1,0:T(8,128)(2,1)S(1)}, u32[]{:S(2)}, u32[]{:S(2)}) collective-permute-start(bf16[64,2048]{1,0:T(8,128)(2,1)S(1)} %get-tuple-element.110), channel_id=1, source_target_pairs={{0,6},{2,4},{4,2},{6,0},{1,7},{3,5},{5,3},{7,1},{8,14},{10,12},{12... | collective-permute-start | bytes 786440 | tf_op jit(solution)/shard_map/ppermute | solution.py:385
  88.8 13.8 %collective-permute-start.49 = (bf16[128,2048]{1,0:T(8,128)(2,1)S(1)}, bf16[128,2048]{1,0:T(8,128)(2,1)S(1)}, u32[]{:S(2)}, u32[]{:S(2)}) collective-permute-start(bf16[128,2048]{1,0:T(8,128)(2,1)S(1)} %collective-permute-done.16.own_ref), channel_id=1, source_target_pairs={{0,1},{1,0},{2,3},{3,2},{4,5},{5,4},{6,7},{7,6},{8,9},{9,8},{10,11... | collective-permute-start | bytes 1572872 | tf_op jit(solution)/shard_map/ppermute | solution.py:449
  89.2 14.6 %collective-permute-start.22 = (bf16[64,2048]{1,0:T(8,128)(2,1)S(1)}, bf16[64,2048]{1,0:T(8,128)(2,1)S(1)}, u32[]{:S(2)}, u32[]{:S(2)}) collective-permute-start(bf16[64,2048]{1,0:T(8,128)(2,1)S(1)} %get-tuple-element.95), channel_id=1, source_target_pairs={{0,2},{2,0},{4,6},{6,4},{1,3},{3,1},{5,7},{7,5},{8,10},{10,8},{12,... | collective-permute-start | bytes 786440 | tf_op jit(solution)/shard_map/ppermute | solution.py:385
  102.7 31.9 %collective-permute-start.4 = (bf16[128,2048]{1,0:T(8,128)(2,1)S(1)}, bf16[128,2048]{1,0:T(8,128)(2,1)S(1)}, u32[]{:S(2)}, u32[]{:S(2)}) collective-permute-start(bf16[128,2048]{1,0:T(8,128)(2,1)S(1)} %get-tuple-element.79.rows_ref.own_ref), channel_id=1, source_target_pairs={{0,1},{1,0},{2,3},{3,2},{4,5},{5,4},{6,7},{7,6},{8,9},{9,8},{10,11... | collective-permute-start | bytes 1572872 | tf_op jit(solution)/shard_map/ppermute | solution.py:449
  105.3 23.9 %collective-permute-start.23 = (bf16[64,2048]{1,0:T(8,128)(2,1)S(1)}, bf16[64,2048]{1,0:T(8,128)(2,1)S(1)}, u32[]{:S(2)}, u32[]{:S(2)}) collective-permute-start(bf16[64,2048]{1,0:T(8,128)(2,1)S(1)} %get-tuple-element.96), channel_id=1, source_target_pairs={{0,4},{2,6},{4,0},{6,2},{1,5},{3,7},{5,1},{7,3},{8,12},{10,14},{12... | collective-permute-start | bytes 786440 | tf_op jit(solution)/shard_map/ppermute | solution.py:385
  107.6 24.0 %collective-permute-start.24 = (bf16[64,2048]{1,0:T(8,128)(2,1)S(1)}, bf16[64,2048]{1,0:T(8,128)(2,1)S(1)}, u32[]{:S(2)}, u32[]{:S(2)}) collective-permute-start(bf16[64,2048]{1,0:T(8,128)(2,1)S(1)} %get-tuple-element.97), channel_id=1, source_target_pairs={{0,6},{2,4},{4,2},{6,0},{1,7},{3,5},{5,3},{7,1},{8,14},{10,12},{12... | collective-permute-start | bytes 786440 | tf_op jit(solution)/shard_map/ppermute | solution.py:385
  110.3 16.6 %collective-permute-start.44 = (bf16[32,2048]{1,0:T(8,128)(2,1)S(1)}, bf16[32,2048]{1,0:T(8,128)(2,1)S(1)}, u32[]{:S(2)}, u32[]{:S(2)}) collective-permute-start(bf16[32,2048]{1,0:T(8,128)(2,1)S(1)} %get-tuple-element.117), channel_id=1, source_target_pairs={{0,6},{1,7},{2,4},{3,5},{4,2},{5,3},{6,0},{7,1},{8,14},{9,15},{10,... | collective-permute-start | bytes 393224 | tf_op jit(solution)/shard_map/ppermute | solution.py:385
  111.3 17.3 %collective-permute-start.45 = (bf16[32,2048]{1,0:T(8,128)(2,1)S(1)}, bf16[32,2048]{1,0:T(8,128)(2,1)S(1)}, u32[]{:S(2)}, u32[]{:S(2)}) collective-permute-start(bf16[32,2048]{1,0:T(8,128)(2,1)S(1)} %get-tuple-element.118), channel_id=1, source_target_pairs={{0,7},{1,6},{2,5},{3,4},{4,3},{5,2},{6,1},{7,0},{8,15},{9,14},{10,... | collective-permute-start | bytes 393224 | tf_op jit(solution)/shard_map/ppermute | solution.py:385
  128.6 9.2 %collective-permute-start.52 = (bf16[64,2048]{1,0:T(8,128)(2,1)S(1)}, bf16[64,2048]{1,0:T(8,128)(2,1)S(1)}, u32[]{:S(2)}, u32[]{:S(2)}) collective-permute-start(bf16[64,2048]{1,0:T(8,128)(2,1)S(1)} %get-tuple-element.124), channel_id=1, source_target_pairs={{0,4},{2,6},{4,0},{6,2},{1,5},{3,7},{5,1},{7,3},{8,12},{10,14},{12... | collective-permute-start | bytes 786440 | tf_op jit(solution)/shard_map/ppermute | solution.py:385
  129.2 14.6 %collective-permute-start.53 = (bf16[64,2048]{1,0:T(8,128)(2,1)S(1)}, bf16[64,2048]{1,0:T(8,128)(2,1)S(1)}, u32[]{:S(2)}, u32[]{:S(2)}) collective-permute-start(bf16[64,2048]{1,0:T(8,128)(2,1)S(1)} %get-tuple-element.125), channel_id=1, source_target_pairs={{0,6},{2,4},{4,2},{6,0},{1,7},{3,5},{5,3},{7,1},{8,14},{10,12},{12... | collective-permute-start | bytes 786440 | tf_op jit(solution)/shard_map/ppermute | solution.py:385
  131.6 32.4 %collective-permute-start.47 = (bf16[128,2048]{1,0:T(8,128)(2,1)S(1)}, bf16[128,2048]{1,0:T(8,128)(2,1)S(1)}, u32[]{:S(2)}, u32[]{:S(2)}) collective-permute-start(bf16[128,2048]{1,0:T(8,128)(2,1)S(1)} %get-tuple-element.120), channel_id=1, source_target_pairs={{0,8},{8,0},{16,24},{24,16},{1,9},{9,1},{17,25},{25,17},{2,10},{10... | collective-permute-start | bytes 1572872 | tf_op jit(solution)/shard_map/ppermute | solution.py:466
  134.5 9.5 %collective-permute-start.25 = (bf16[32,2048]{1,0:T(8,128)(2,1)S(1)}, bf16[32,2048]{1,0:T(8,128)(2,1)S(1)}, u32[]{:S(2)}, u32[]{:S(2)}) collective-permute-start(bf16[32,2048]{1,0:T(8,128)(2,1)S(1)} %get-tuple-element.99), channel_id=1, source_target_pairs={{0,1},{1,0},{2,3},{3,2},{4,5},{5,4},{6,7},{7,6},{8,9},{9,8},{10,11... | collective-permute-start | bytes 393224 | tf_op jit(solution)/shard_map/ppermute | solution.py:385
  134.9 11.7 %collective-permute-start.26 = (bf16[32,2048]{1,0:T(8,128)(2,1)S(1)}, bf16[32,2048]{1,0:T(8,128)(2,1)S(1)}, u32[]{:S(2)}, u32[]{:S(2)}) collective-permute-start(bf16[32,2048]{1,0:T(8,128)(2,1)S(1)} %get-tuple-element.100), channel_id=1, source_target_pairs={{0,2},{1,3},{2,0},{3,1},{4,6},{5,7},{6,4},{7,5},{8,10},{9,11},{10,... | collective-permute-start | bytes 393224 | tf_op jit(solution)/shard_map/ppermute | solution.py:385
  137.8 10.7 %collective-permute-start.27 = (bf16[32,2048]{1,0:T(8,128)(2,1)S(1)}, bf16[32,2048]{1,0:T(8,128)(2,1)S(1)}, u32[]{:S(2)}, u32[]{:S(2)}) collective-permute-start(bf16[32,2048]{1,0:T(8,128)(2,1)S(1)} %get-tuple-element.101), channel_id=1, source_target_pairs={{0,3},{1,2},{2,1},{3,0},{4,7},{5,6},{6,5},{7,4},{8,11},{9,10},{10,... | collective-permute-start | bytes 393224 | tf_op jit(solution)/shard_map/ppermute | solution.py:385
  159.8 9.7 %collective-permute-start.59 = (bf16[32,2048]{1,0:T(8,128)(2,1)S(1)}, bf16[32,2048]{1,0:T(8,128)(2,1)S(1)}, u32[]{:S(2)}, u32[]{:S(2)}) collective-permute-start(bf16[32,2048]{1,0:T(8,128)(2,1)S(1)} %get-tuple-element.132), channel_id=1, source_target_pairs={{0,6},{1,7},{2,4},{3,5},{4,2},{5,3},{6,0},{7,1},{8,14},{9,15},{10,... | collective-permute-start | bytes 393224 | tf_op jit(solution)/shard_map/ppermute | solution.py:385
  162.2 9.9 %collective-permute-start.60 = (bf16[32,2048]{1,0:T(8,128)(2,1)S(1)}, bf16[32,2048]{1,0:T(8,128)(2,1)S(1)}, u32[]{:S(2)}, u32[]{:S(2)}) collective-permute-start(bf16[32,2048]{1,0:T(8,128)(2,1)S(1)} %get-tuple-element.133), channel_id=1, source_target_pairs={{0,7},{1,6},{2,5},{3,4},{4,3},{5,2},{6,1},{7,0},{8,15},{9,14},{10,... | collective-permute-start | bytes 393224 | tf_op jit(solution)/shard_map/ppermute | solution.py:385
  164.0 14.2 %collective-permute-start.32 = (bf16[128,2048]{1,0:T(8,128)(2,1)S(1)}, bf16[128,2048]{1,0:T(8,128)(2,1)S(1)}, u32[]{:S(2)}, u32[]{:S(2)}) collective-permute-start(bf16[128,2048]{1,0:T(8,128)(2,1)S(1)} %get-tuple-element.106), channel_id=1, source_target_pairs={{0,8},{8,0},{16,24},{24,16},{1,9},{9,1},{17,25},{25,17},{2,10},{10... | collective-permute-start | bytes 1572872 | tf_op jit(solution)/shard_map/ppermute | solution.py:466
  164.2 24.9 %collective-permute-start.6 = (bf16[64,2048]{1,0:T(8,128)(2,1)S(1)}, bf16[64,2048]{1,0:T(8,128)(2,1)S(1)}, u32[]{:S(2)}, u32[]{:S(2)}) collective-permute-start(bf16[64,2048]{1,0:T(8,128)(2,1)S(1)} %get-tuple-element.82), channel_id=1, source_target_pairs={{0,2},{2,0},{4,6},{6,4},{1,3},{3,1},{5,7},{7,5},{8,10},{10,8},{12,... | collective-permute-start | bytes 786440 | tf_op jit(solution)/shard_map/ppermute | solution.py:385
  165.1 24.0 %collective-permute-start.7 = (bf16[64,2048]{1,0:T(8,128)(2,1)S(1)}, bf16[64,2048]{1,0:T(8,128)(2,1)S(1)}, u32[]{:S(2)}, u32[]{:S(2)}) collective-permute-start(bf16[64,2048]{1,0:T(8,128)(2,1)S(1)} %get-tuple-element.83), channel_id=1, source_target_pairs={{0,4},{2,6},{4,0},{6,2},{1,5},{3,7},{5,1},{7,3},{8,12},{10,14},{12... | collective-permute-start | bytes 786440 | tf_op jit(solution)/shard_map/ppermute | solution.py:385
  169.5 19.5 %collective-permute-start.8 = (bf16[64,2048]{1,0:T(8,128)(2,1)S(1)}, bf16[64,2048]{1,0:T(8,128)(2,1)S(1)}, u32[]{:S(2)}, u32[]{:S(2)}) collective-permute-start(bf16[64,2048]{1,0:T(8,128)(2,1)S(1)} %get-tuple-element.84), channel_id=1, source_target_pairs={{0,6},{2,4},{4,2},{6,0},{1,7},{3,5},{5,3},{7,1},{8,14},{10,12},{12... | collective-permute-start | bytes 786440 | tf_op jit(solution)/shard_map/ppermute | solution.py:385
  178.3 31.6 %collective-permute-start.46 = (bf16[128,2048]{1,0:T(8,128)(2,1)S(1)}, bf16[128,2048]{1,0:T(8,128)(2,1)S(1)}, u32[]{:S(2)}, u32[]{:S(2)}) collective-permute-start(bf16[128,2048]{1,0:T(8,128)(2,1)S(1)} %add_convert_fusion.3), channel_id=1, source_target_pairs={{8,16},{16,8},{9,17},{17,9},{10,18},{18,10},{11,19},{19,11},{12,20... | collective-permute-start | bytes 1572872 | tf_op jit(solution)/shard_map/ppermute | solution.py:466
  179.4 30.5 %collective-permute-start.61 = (bf16[128,2048]{1,0:T(8,128)(2,1)S(1)}, bf16[128,2048]{1,0:T(8,128)(2,1)S(1)}, u32[]{:S(2)}, u32[]{:S(2)}) collective-permute-start(bf16[128,2048]{1,0:T(8,128)(2,1)S(1)} %add_convert_fusion.1), channel_id=1, source_target_pairs={{0,8},{8,0},{16,24},{24,16},{1,9},{9,1},{17,25},{25,17},{2,10},{10... | collective-permute-start | bytes 1572872 | tf_op jit(solution)/shard_map/ppermute | solution.py:466
  199.2 9.4 %collective-permute-start.15 = (bf16[32,2048]{1,0:T(8,128)(2,1)S(1)}, bf16[32,2048]{1,0:T(8,128)(2,1)S(1)}, u32[]{:S(2)}, u32[]{:S(2)}) collective-permute-start(bf16[32,2048]{1,0:T(8,128)(2,1)S(1)} %get-tuple-element.92), channel_id=1, source_target_pairs={{0,7},{1,6},{2,5},{3,4},{4,3},{5,2},{6,1},{7,0},{8,15},{9,14},{10,... | collective-permute-start | bytes 393224 | tf_op jit(solution)/shard_map/ppermute | solution.py:385
  (46 other events, 490.1 us)

commit v2 on v1

--- a/solution.py
+++ b/solution.py
@@ -9,7 +9,6 @@
 
 
 SEQ, TP, CHIPS, PLANE = ("z", "x"), ("y", "c"), ("x", "y"), ("x", "y", "c")
-MIDDLE = [(1, 2), (2, 1)]
 BF16, F32 = jnp.bfloat16, jnp.float32
 
 
@@ -54,6 +53,7 @@
         total = total + taps_ref[offset : offset + 1] * window[first : first + 16]
     head_ref[0:16] = total
     head_ref[16:32] = gate_ref[0:16].astype(F32)
+    head_ref[32 : 33 + back] = taps_ref[...]
 
 
 def filter_rows(me, out_gate, in_gate, conv_values, conv_taps, parts):
@@ -62,7 +62,7 @@
     whole = pl.BlockSpec(memory_space=pltpu.VMEM)
     *blocks, head = pl.pallas_call(
         functools.partial(filter_kernel, parts, conv_taps.shape[0] - 1),
-        out_shape=[pltpu.VMEM(out.shape, BF16)] * parts + [pltpu.VMEM((32, channels), F32)],
+        out_shape=[pltpu.VMEM(out.shape, BF16)] * parts + [pltpu.VMEM((40, channels), F32)],
         in_specs=[pl.BlockSpec(memory_space=pltpu.SMEM)] + [whole] * 4,
         out_specs=[whole] * (parts + 1),
         scratch_shapes=[pltpu.VMEM((length + 8, channels), F32)],
@@ -72,15 +72,16 @@
     return blocks, head
 
 
-def mend_kernel(parts, back, me_ref, head_ref, taps_ref, halo_ref, *refs):
+def mend_kernel(parts, back, me_ref, seq_ref, head_ref, halo_ref, *refs):
     outs = refs[parts:]
     channels = head_ref.shape[1]
     row = lax.broadcasted_iota(jnp.int32, (16, channels), 0)
     total = head_ref[0:16]
     for offset in range(back):
         for at_row in range(back - offset):
-            term = taps_ref[offset : offset + 1] * halo_ref[at_row + offset : at_row + offset + 1]
-            total = total + jnp.where((row == at_row) & (me_ref[1] > 0), term, 0.0)
+            tap = head_ref[32 + offset : 33 + offset]
+            term = tap * halo_ref[at_row + offset : at_row + offset + 1]
+            total = total + jnp.where((row == at_row) & (seq_ref[0] > 0), term, 0.0)
     fresh = (head_ref[16:32] * total).astype(BF16)
     for k in range(parts):
 
@@ -89,19 +90,19 @@
             outs[k][0:16] = fresh
 
 
-def mend_rows(me, blocks, head, conv_taps, halo):
+def mend_rows(me, seq, blocks, head, back, halo):
     parts = len(blocks)
     whole = pl.BlockSpec(memory_space=pltpu.VMEM)
     return pl.pallas_call(
-        functools.partial(mend_kernel, parts, conv_taps.shape[0] - 1),
+        functools.partial(mend_kernel, parts, back),
         out_shape=[pltpu.VMEM(blocks[0].shape, BF16)] * parts,
-        in_specs=[pl.BlockSpec(memory_space=pltpu.SMEM)] + [whole] * (3 + parts),
+        in_specs=[pl.BlockSpec(memory_space=pltpu.SMEM)] * 2 + [whole] * (2 + parts),
         out_specs=[whole] * parts,
         input_output_aliases={4 + k: k for k in range(parts)},
         cost_estimate=cost(1 << 20, blocks),
         compiler_params=grant(8),
         name="mend_rows",
-    )(me, head, conv_taps, halo, *blocks)
+    )(me, seq, head, halo, *blocks)
 
 
 def fetch_kernel(from_ref, to_ref, sem):
@@ -118,7 +119,7 @@
         out_specs=pl.BlockSpec(memory_space=pltpu.VMEM),
         scratch_shapes=[pltpu.SemaphoreType.DMA],
         cost_estimate=cost(1 << 20, [array]),
-        compiler_params=grant(1),
+        compiler_params=grant(54),
         name="fetch_rows",
     )(array)
 
@@ -164,7 +165,7 @@
         gain = mix_gain[None]
         gain_spec = pl.BlockSpec((1, channels), lambda i, me_ref: (0, me_ref[0] ^ i))
     out_shape = [
-        jax.ShapeDtypeStruct((rows, width), F32),
+        pltpu.HBM((rows, width), F32),
         jax.ShapeDtypeStruct((rows, width), BF16),
     ]
     grid_spec = pltpu.PrefetchScalarGridSpec(
@@ -184,20 +185,20 @@
         functools.partial(mix_kernel, parts),
         out_shape=out_shape,
         grid_spec=grid_spec,
-        cost_estimate=cost(2 * rows * out_proj.size, [out_proj, residual] + out_shape),
+        cost_estimate=cost(2 * rows * out_proj.size, [out_proj, residual]),
         compiler_params=grant(14),
         name="mix_project",
     )(me, *pieces, gain, out_proj, residual, ffn_gain[None])
 
 
-def send_kernel(chips, own_ref, pair_ref, table_ref, *outs):
+def send_kernel(chips, base, own_ref, pair_ref, table_ref, *outs):
     size = outs[0].shape[0] // 2
     tokens = own_ref.shape[0]
     slots = lax.broadcasted_iota(jnp.int32, (size, tokens), 0).astype(F32)
-    for side, (ref, base) in enumerate(((own_ref, 0), (pair_ref, 4 * chips))):
+    for side, (ref, first) in enumerate(((own_ref, 0), (pair_ref, base))):
         pick = jnp.concatenate(
             [
-                (table_ref[base + k : base + k + 1] == slots).astype(F32).astype(BF16)
+                (table_ref[first + k : first + k + 1] == slots).astype(F32).astype(BF16)
                 for k in range(chips)
             ]
         )
@@ -211,7 +212,7 @@
     whole = pl.BlockSpec(memory_space=pltpu.VMEM)
     out_shape = [jax.ShapeDtypeStruct((2 * capacity, width), BF16)] * chips
     return pl.pallas_call(
-        functools.partial(send_kernel, chips),
+        functools.partial(send_kernel, chips, table.shape[0] - chips),
         out_shape=out_shape,
         in_specs=[whole] * 3,
         out_specs=[whole] * chips,
@@ -368,22 +369,33 @@
     )(*pieces, table)
 
 
-def gather_line(own, count):
+def ring(count, distance):
+    order = [p ^ (p >> 1) for p in range(count)]
+    return [(order[p], order[(p + distance) % count]) for p in range(count)]
+
+
+def gather_ring(own, count):
     if count != 4:
-        return [own] + [lax.ppermute(own, "z", flips(count, j)) for j in range(1, count)]
-    sides, middle = flips(4, 1), MIDDLE
-    near = lax.ppermute(own, "z", sides)
-    across = lax.ppermute(own, "z", middle)
-    across_far = lax.ppermute(near, "z", middle)
-    side_far = lax.ppermute(across, "z", sides)
-    side_end = lax.ppermute(across_far, "z", sides)
-    return [own, near, across_far + side_far, across + side_end]
+        return [own] + [lax.ppermute(own, "z", ring(count, j)) for j in range(1, count)]
+    one = lax.ppermute(own, "z", ring(4, 1))
+    two = lax.ppermute(one, "z", ring(4, 1))
+    three = lax.ppermute(own, "z", ring(4, -1))
+    return [own, one, two, three]
 
 
 def exchange(pieces, axes):
     count = len(pieces)
     moved = [lax.ppermute(pieces[k], axes, flips(count, k)) for k in range(1, count)]
     return [pieces[0]] + moved
+
+
+def gate_tables(routes, route_weights, experts, rank, pair_rank):
+    gate_values = route_weights / jnp.sum(route_weights, axis=1, keepdims=True) * 2.5
+    hits = routes.T[:, None, :] == experts
+    gates_of = jnp.sum(jnp.where(hits, gate_values.T[:, None, :], 0.0), axis=0)
+    table = jnp.concatenate([rank, gates_of.reshape(rank.shape), pair_rank], axis=1)
+    count = rank.shape[0]
+    return [table[0]] + [lax.ppermute(table[j], "z", ring(count, j)) for j in range(1, count)]
 
 
 def layer(
@@ -413,43 +425,45 @@
     length = conv_values.shape[0]
     tail = in_gate[length - back :].astype(F32) * conv_values[length - back :].astype(F32)
     halo = from_behind(tail, 1)
-    me = jnp.stack([tp_index, lax.axis_index(SEQ)]).astype(jnp.int32)
+    me = tp_index.reshape(1).astype(jnp.int32)
+    seq = lax.axis_index(SEQ).reshape(1).astype(jnp.int32)
     blocks, head = filter_rows(me, out_gate, in_gate, conv_values, conv_taps, tp_count)
-    blocks = mend_rows(me, blocks, head, conv_taps, halo)
+    blocks = mend_rows(me, seq, blocks, head, back, halo)
     pieces = exchange(blocks, TP)
-    out_proj = fetch(out_proj)
+    late = (routes, mix_gain, pieces[1])
+    routes, mix_gain, _ = lax.optimization_barrier(late)
 
     row_count, top_count = routes.shape
     capacity = max(2, 4 * row_count * top_count // (6 * z_count * chips))
-    gate_values = route_weights / jnp.sum(route_weights, axis=1, keepdims=True) * 2.5
-    layers = jnp.arange(z_count, dtype=jnp.int32) ^ z_index
+    place = z_index ^ (z_index >> 1) ^ (z_index >> 2)
+    later = (jnp.arange(z_count, dtype=jnp.int32) + place) & (z_count - 1)
+    layers = later ^ (later >> 1)
     cores = jnp.arange(2, dtype=jnp.int32) ^ core_index
     places = jnp.arange(chips, dtype=jnp.int32) ^ chip_index
     experts = (layers[:, None, None] * chips + places) * 2 + cores[:, None]
-    hits = routes.T[:, None, :] == experts.reshape(-1)[None, :, None]
-    named = jnp.any(hits, axis=0)
-    gates_of = jnp.sum(jnp.where(hits, gate_values.T[:, None, :], 0.0), axis=0)
+    experts = experts.reshape(-1)[None, :, None]
+    named = jnp.any(routes.T[:, None, :] == experts, axis=0)
     steps = jnp.arange(row_count, dtype=jnp.int32)
     earlier = (steps[:, None] < steps[None, :]).astype(BF16)
     rank = jnp.dot(named.astype(BF16), earlier, preferred_element_type=F32)
-    rank = jnp.where(named, rank, -1.0).reshape(z_count, 2 * chips, row_count)
-    gates_of = gates_of.reshape(z_count, 2 * chips, row_count)
+    rank = jnp.where(named, rank, -1.0)
+    out_proj, rank = lax.optimization_barrier((out_proj, rank))
+    rank = rank.reshape(z_count, 2 * chips, row_count)
     pair_rank = lax.ppermute(rank[:, chips:], "c", flips(2, 1))
-    table = jnp.concatenate([rank, gates_of, pair_rank], axis=1)
-    tables = [table[0]] + [
-        lax.ppermute(table[j], "z", flips(z_count, j))
-        for j in range(1, z_count)
-    ]
+    out_proj = fetch(out_proj)
 
     stream, normed = mix_project(me, pieces, mix_gain, out_proj, residual, ffn_gain)
 
-    sources = gather_line(normed, z_count)
-    results = []
+    sources = gather_ring(normed, z_count)
+    weights = (expert_gate, expert_up, expert_down)
+    tables, results = [], []
     for j in range(z_count):
         pair = lax.ppermute(sources[j], "c", flips(2, 1))
-        outgoing = outgoing_rows(sources[j], pair, tables[j], chips, capacity)
+        table = tables[j] if j else jnp.concatenate([rank[0], pair_rank[0]])
+        outgoing = outgoing_rows(sources[j], pair, table, chips, capacity)
+        if j == 0:
+            tables = gate_tables(routes, route_weights, experts, rank, pair_rank)
         arrived = exchange(outgoing, CHIPS)
-        weights = (expert_gate, expert_up, expert_down)
         results.append(expert_rows(arrived, 2 * chips, *weights))
 
     base = shared_rows(normed, stream, shared_gate, shared_up, shared_down)
@@ -460,21 +474,18 @@
         partial[j], short[j] = combine(returned, tables[j])
 
     if z_count == 4:
-        sides = flips(4, 1)
-
-        def hop(block, route):
+
+        def hop(block, distance):
+            route = ring(4, distance)
             return lax.ppermute(block.astype(BF16), "z", route).astype(F32)
 
-        far = hop(short[3], sides)
-        mid = hop(short[2], sides)
-        far = hop(far + partial[2], MIDDLE)
-        mid = hop(mid + partial[3], MIDDLE)
-        last = hop(far + partial[1], sides)
-        routed = partial[0] + mid + last
+        far = hop(short[2], -1)
+        last = hop(far + partial[1], -1)
+        routed = partial[0] + hop(short[3], 1) + last
     else:
         routed = partial[0]
         for j in range(1, z_count):
-            routed = routed + lax.ppermute(short[j], "z", flips(z_count, j))
+            routed = routed + lax.ppermute(short[j], "z", ring(z_count, -j))
     return (base + routed).astype(BF16)
 
 

time: 211 us -> 186 us (0.88)
  starting transfers between devices: 83.5 us -> 55.1 us
  Pallas kernels: 24.2 us -> 30.6 us
  other arithmetic: 5.88 us -> 2.94 us
    ppermute x8 -> x6, starting transfers between devices: 28.8 us -> 7.97 us  [the longest x3 5.05 us: gate_tables(): lax.ppermute(table[j], 'z', ring(count, j))]
    ppermute x5 -> x3, starting transfers between devices: 11.2 us -> 4.73 us  [hop(): return lax.ppermute(block.astype(BF16), 'z', route).astype(F32)]
    ppermute x8 -> x6, waiting for transfers between devices: 33.1 us -> 38.6 us  [the longest x1 23.8 us: gather_ring(): one = lax.ppermute(own, 'z', ring(4, 1))]
    ppermute x5 -> x3, waiting for transfers between devices: 4.06 us -> 0.01 us  [hop(): return lax.ppermute(block.astype(BF16), 'z', route).astype(F32)]
    add x2 -> x0, other arithmetic: 2.8 us -> none  [gather_line(): return [own, near, across_far + side_far, across + side_end]]
    pallas_call x1, Pallas kernels: 0.43 us -> 2.85 us  [fetch(): pl.pallas_call(fetch_kernel, out_shape=pltpu.VMEM(array.shape, array.dtyp...]
    ppermute x43, waiting for transfers between devices: 51.6 us -> 49.2 us  [exchange(): lax.ppermute(pieces[k], axes, flips(count, k))]
    unnamed x32 -> x24, local copies, waits for them, and re-layouts: 5.12 us -> 3.22 us
  transfers between devices with their start and end apart: 62 -> 58, of which waited for: 27 -> 28; matrix products, arithmetic and copies ran while one was open for 2% -> 1% of each run, Pallas kernels for 10% -> 15%
where the time goes in v2:
time: 186 us; the launch traced here: 185 us
  waiting for transfers between devices  91.8 us (49%)
  starting transfers between devices  55.1 us (30%)
  Pallas kernels  30.6 us (16%)
  local copies, waits for them, and re-layouts  4.02 us (2%)
  other arithmetic  2.94 us (2%)
    ppermute x43, waiting for transfers between devices, exchange(): lax.ppermute(pieces[k], axes, flips(count, k))  49.2 us
    ppermute x43, starting transfers between devices, exchange(): lax.ppermute(pieces[k], axes, flips(count, k))  38.8 us
    ppermute x1, waiting for transfers between devices, gather_ring(): one = lax.ppermute(own, 'z', ring(4, 1))  23.8 us
    pallas_call x4, Pallas kernels, expert_rows(): pl.pallas_call(functools.partial(expert_kernel, parts, count), out_shape=...  11.5 us
    ppermute x1, waiting for transfers between devices, gather_ring(): two = lax.ppermute(one, 'z', ring(4, 1))  10.8 us
    pallas_call x4, Pallas kernels, combine(): pl.pallas_call(functools.partial(combine_kernel, parts, parts // 2), out_...  5.52 us
    ppermute x3, starting transfers between devices, gate_tables(): lax.ppermute(table[j], 'z', ring(count, j))  5.05 us
    ppermute x3, starting transfers between devices, hop(): return lax.ppermute(block.astype(BF16), 'z', route).astype(F32)  4.73 us
  transfers between devices with their start and end apart: 58, of which 28 were waited for; matrix products, arithmetic and copies ran while one was open for 1% of the time, Pallas kernels for 15%

profile of v2, /device:TPU:0, one launch (start us, length us, event | category | flops | bytes accessed | tf_op | source)
XLA Modules:
  0.0 184.9 jit_solution(4028540213719828121)
XLA Ops:
  0.7 3.0 %collective-permute-start = (f32[2,384]{1,0:T(2,128)S(1)}, f32[2,384]{1,0:T(2,128)S(1)}, u32[]{:S(2)}, u32[]{:S(2)}) collective-permute-start(f32[2,384]{1,0:T(2,128)S(1)} %convert_multiply_fusion), channel_id=1, source_target_pairs={{28,0},{0,4},{4,8},{8,12},{12,16},{16,20},{20,24},{24,28},{29,1},{... | collective-permute-start | bytes 9224 | tf_op jit(solution)/shard_map/ppermute | solution.py:22
  3.8 1.9 %filter_rows.1 = (bf16[128,384]{1,0:T(8,128)(2,1)S(1)}, bf16[128,384]{1,0:T(8,128)(2,1)S(1)}, bf16[128,384]{1,0:T(8,128)(2,1)S(1)}, bf16[128,384]{1,0:T(8,128)(2,1)S(1)}, f32[40,384]{1,0:T(8,128)S(1)}) custom-call(s32[1]{0:T(128)} %bitcast.me_ref, bf16[512,384]{1,0:T(8,128)(2,1)} %gate_ref.2, bf16[512,384]{1,0:T(8,128)(2,1)} %in_ref.1, ...), custom_call_target="tpu_custom_call" | custom-call | flops 1048576 | bytes 1179648 | tf_op jit(solution)/shard_map/filter_rows/pallas_call | solution.py:63
  5.6 2.7 %collective-permute-done.halo_ref = f32[2,384]{1,0:T(2,128)S(1)} collective-permute-done((f32[2,384]{1,0:T(2,128)S(1)}, f32[2,384]{1,0:T(2,128)S(1)}, u32[]{:S(2)}, u32[]{:S(2)}) %collective-permute-start) | collective-permute-done | bytes 3104 | tf_op jit(solution)/shard_map/ppermute | solution.py:22
  8.6 1.7 collective-permute-start.2
  12.1 2.9 %fetch_rows.1.refs_5_ = bf16[1536,2048]{1,0:T(8,128)(2,1)S(1)} custom-call(bf16[1536,2048]{1,0:T(8,128)(2,1)} %from_ref), custom_call_target="tpu_custom_call" | custom-call | flops 1048576 | bytes 6291456 | tf_op jit(solution)/shard_map/fetch_rows/pallas_call | solution.py:115
  15.4 3.1 %mix_project.1 = (f32[128,2048]{1,0:T(8,128)}, bf16[128,2048]{1,0:T(8,128)(2,1)S(1)}) custom-call(s32[1]{0:T(128)} %bitcast.me_ref, bf16[128,384]{1,0:T(8,128)(2,1)S(1)} %get-tuple-element.77.refs_0_, bf16[128,384]{1,0:T(8,128)(2,1)S(1)} %collective-permute-done.1.refs_1_, bf16[128,384]{1,0:T(8,128)(2,1)S(1)} %collective-permute-done.2.refs_2_, ...), custom_call_target="tpu_custom_call" | custom-call | flops 805306368 | bytes 6815744 | tf_op jit(solution)/shard_map/mix_project/pallas_call | solution.py:184
  18.5 2.9 %collective-permute-start.16 = (bf16[128,2048]{1,0:T(8,128)(2,1)S(1)}, bf16[128,2048]{1,0:T(8,128)(2,1)}, u32[]{:S(2)}, u32[]{:S(2)}) collective-permute-start(bf16[128,2048]{1,0:T(8,128)(2,1)S(1)} %get-tuple-element.84.rows_ref.own_ref), channel_id=1, source_target_pairs={{0,16},{8,0},{24,8},{16,24},{1,17},{9,1},{25,9},{17,25},{2,18},{10... | collective-permute-start | bytes 1572872 | tf_op jit(solution)/shard_map/ppermute | solution.py:382
  21.5 23.8 %collective-permute-done.30.own_ref = bf16[128,2048]{1,0:T(8,128)(2,1)S(1)} collective-permute-done((bf16[128,2048]{1,0:T(8,128)(2,1)S(1)}, bf16[128,2048]{1,0:T(8,128)(2,1)S(1)}, u32[]{:S(2)}, u32[]{:S(2)}) %collective-permute-start.30) | collective-permute-done | bytes 524320 | tf_op jit(solution)/shard_map/ppermute | solution.py:380
  45.3 10.8 %collective-permute-done.31.own_ref = bf16[128,2048]{1,0:T(8,128)(2,1)} collective-permute-done((bf16[128,2048]{1,0:T(8,128)(2,1)S(1)}, bf16[128,2048]{1,0:T(8,128)(2,1)}, u32[]{:S(2)}, u32[]{:S(2)}) %collective-permute-start.31) | collective-permute-done | bytes 524320 | tf_op jit(solution)/shard_map/ppermute | solution.py:381
  58.3 4.7 %collective-permute-start.33 = (f32[20,128]{1,0:T(8,128)S(1)}, f32[20,128]{1,0:T(8,128)S(1)}, u32[]{:S(2)}, u32[]{:S(2)}) collective-permute-start(f32[20,128]{1,0:T(8,128)S(1)} %get-tuple-element.141), channel_id=1, source_target_pairs={{0,24},{8,16},{24,0},{16,8},{1,25},{9,17},{25,1},{17,9},{2,26},{10... | collective-permute-start | bytes 30728 | tf_op jit(solution)/shard_map/ppermute | solution.py:398
  63.0 1.7 collective-permute-done.33.table_ref.refs_8_
  67.1 2.1 %collective-permute-done.46.table_ref.refs_8_ = f32[20,128]{1,0:T(8,128)S(1)} collective-permute-done((f32[20,128]{1,0:T(8,128)S(1)}, f32[20,128]{1,0:T(8,128)S(1)}, u32[]{:S(2)}, u32[]{:S(2)}) %collective-permute-start.46) | collective-permute-done | bytes 10272 | tf_op jit(solution)/shard_map/ppermute | solution.py:398
  73.1 3.3 %collective-permute-done.34.refs_1_ = bf16[64,2048]{1,0:T(8,128)(2,1)S(1)} collective-permute-done((bf16[64,2048]{1,0:T(8,128)(2,1)S(1)}, bf16[64,2048]{1,0:T(8,128)(2,1)S(1)}, u32[]{:S(2)}, u32[]{:S(2)}) %collective-permute-start.34) | collective-permute-done | bytes 262176 | tf_op jit(solution)/shard_map/ppermute | solution.py:388
  79.3 5.1 %collective-permute-done.36.refs_3_ = bf16[64,2048]{1,0:T(8,128)(2,1)S(1)} collective-permute-done((bf16[64,2048]{1,0:T(8,128)(2,1)S(1)}, bf16[64,2048]{1,0:T(8,128)(2,1)S(1)}, u32[]{:S(2)}, u32[]{:S(2)}) %collective-permute-start.36) | collective-permute-done | bytes 262176 | tf_op jit(solution)/shard_map/ppermute | solution.py:388
  89.1 2.9 %expert_rows.6 = (bf16[32,2048]{1,0:T(8,128)(2,1)S(1)}, bf16[32,2048]{1,0:T(8,128)(2,1)S(1)}, bf16[32,2048]{1,0:T(8,128)(2,1)S(1)}, bf16[32,2048]{1,0:T(8,128)(2...) custom-call(bf16[64,2048]{1,0:T(8,128)(2,1)S(1)} %get-tuple-element., ...), custom_call_target="tpu_custom_call" | custom-call | flops 1610612736 | bytes 6291456 | tf_op jit(solution)/shard_map/expert_rows/pallas_call | solution.py:269
  103.2 1.7 collective-permute-start.43
  104.9 2.9 %expert_rows.5 = (bf16[32,2048]{1,0:T(8,128)(2,1)S(1)}, bf16[32,2048]{1,0:T(8,128)(2,1)S(1)}, bf16[32,2048]{1,0:T(8,128)(2,1)S(1)}, bf16[32,2048]{1,0:T(8,128)(2...) custom-call(bf16[64,2048]{1,0:T(8,128)(2,1)S(1)} %get-tuple-element., ...), custom_call_target="tpu_custom_call" | custom-call | flops 1610612736 | bytes 6291456 | tf_op jit(solution)/shard_map/expert_rows/pallas_call | solution.py:269
  107.7 10.1 %collective-permute-done.42.refs_6_ = bf16[32,2048]{1,0:T(8,128)(2,1)S(1)} collective-permute-done((bf16[32,2048]{1,0:T(8,128)(2,1)S(1)}, bf16[32,2048]{1,0:T(8,128)(2,1)S(1)}, u32[]{:S(2)}, u32[]{:S(2)}) %collective-permute-start.42) | collective-permute-done | bytes 131104 | tf_op jit(solution)/shard_map/ppermute | solution.py:388
  125.8 1.8 collective-permute-start.44
  127.5 2.9 %expert_rows.7 = (bf16[32,2048]{1,0:T(8,128)(2,1)S(1)}, bf16[32,2048]{1,0:T(8,128)(2,1)S(1)}, bf16[32,2048]{1,0:T(8,128)(2,1)S(1)}, bf16[32,2048]{1,0:T(8,128)(2...) custom-call(bf16[64,2048]{1,0:T(8,128)(2,1)S(1)} %get-tuple-element., ...), custom_call_target="tpu_custom_call" | custom-call | flops 1610612736 | bytes 6291456 | tf_op jit(solution)/shard_map/expert_rows/pallas_call | solution.py:269
  132.6 1.6 collective-permute-done.27.refs_6_
  134.6 2.6 %collective-permute-done.28.refs_7_ = bf16[32,2048]{1,0:T(8,128)(2,1)S(1)} collective-permute-done((bf16[32,2048]{1,0:T(8,128)(2,1)S(1)}, bf16[32,2048]{1,0:T(8,128)(2,1)S(1)}, u32[]{:S(2)}, u32[]{:S(2)}) %collective-permute-start.28) | collective-permute-done | bytes 131104 | tf_op jit(solution)/shard_map/ppermute | solution.py:388
  140.0 1.6 collective-permute-start.55
  151.0 2.7 %collective-permute-start.29 = (bf16[128,2048]{1,0:T(8,128)(2,1)S(1)}, bf16[128,2048]{1,0:T(8,128)(2,1)S(1)}, u32[]{:S(2)}, u32[]{:S(2)}) collective-permute-start(bf16[128,2048]{1,0:T(8,128)(2,1)S(1)} %get-tuple-element.112), channel_id=1, source_target_pairs={{0,8},{8,24},{24,16},{16,0},{1,9},{9,25},{25,17},{17,1},{2,10},{10... | collective-permute-start | bytes 1572872 | tf_op jit(solution)/shard_map/ppermute | solution.py:480
  155.4 2.3 %collective-permute-done.6.refs_1_ = bf16[64,2048]{1,0:T(8,128)(2,1)S(1)} collective-permute-done((bf16[64,2048]{1,0:T(8,128)(2,1)S(1)}, bf16[64,2048]{1,0:T(8,128)(2,1)S(1)}, u32[]{:S(2)}, u32[]{:S(2)}) %collective-permute-start.6) | collective-permute-done | bytes 262176 | tf_op jit(solution)/shard_map/ppermute | solution.py:388
  157.7 5.1 %collective-permute-done.8.refs_3_ = bf16[64,2048]{1,0:T(8,128)(2,1)S(1)} collective-permute-done((bf16[64,2048]{1,0:T(8,128)(2,1)S(1)}, bf16[64,2048]{1,0:T(8,128)(2,1)S(1)}, u32[]{:S(2)}, u32[]{:S(2)}) %collective-permute-start.8) | collective-permute-done | bytes 262176 | tf_op jit(solution)/shard_map/ppermute | solution.py:388
  162.8 2.9 %expert_rows.4 = (bf16[32,2048]{1,0:T(8,128)(2,1)S(1)}, bf16[32,2048]{1,0:T(8,128)(2,1)S(1)}, bf16[32,2048]{1,0:T(8,128)(2,1)S(1)}, bf16[32,2048]{1,0:T(8,128)(2...) custom-call(bf16[64,2048]{1,0:T(8,128)(2,1)S(1)} %get-tuple-element., ...), custom_call_target="tpu_custom_call" | custom-call | flops 1610612736 | bytes 6291456 | tf_op jit(solution)/shard_map/expert_rows/pallas_call | solution.py:269
  167.5 4.3 %collective-permute-done.10.refs_2_ = bf16[32,2048]{1,0:T(8,128)(2,1)S(1)} collective-permute-done((bf16[32,2048]{1,0:T(8,128)(2,1)S(1)}, bf16[32,2048]{1,0:T(8,128)(2,1)S(1)}, u32[]{:S(2)}, u32[]{:S(2)}) %collective-permute-start.10) | collective-permute-done | bytes 131104 | tf_op jit(solution)/shard_map/ppermute | solution.py:388
  172.5 1.7 collective-permute-start.14
  174.2 1.7 collective-permute-start.15
  177.7 2.0 %shared_rows.1 = f32[128,2048]{1,0:T(8,128)S(1)} custom-call(bf16[128,2048]{1,0:T(8,128)(2,1)S(1)} %get-tuple-element.84.rows_ref.own_ref, f32[128,2048]{1,0:T(8,128)S(1)} %copy-done.7, bf16[2048,512]{1,0:T(8,128)(2,1)S(1)} %copy-done.4, bf16[2048,512]{1,0:T(8,128)(2,1)S(1)} %copy-done.5, bf16[512,2048]{1,0:T(8,128)(2,1)S(1)} %copy-done.6), custom_call_target="tpu_custom_call" | custom-call | flops 805306368 | bytes 6291456 | tf_op jit(solution)/shard_map/shared_rows/pallas_call | solution.py:307
  179.7 2.8 %collective-permute-done.15.refs_7_ = bf16[32,2048]{1,0:T(8,128)(2,1)S(1)} collective-permute-done((bf16[32,2048]{1,0:T(8,128)(2,1)S(1)}, bf16[32,2048]{1,0:T(8,128)(2,1)S(1)}, u32[]{:S(2)}, u32[]{:S(2)}) %collective-permute-start.15) | collective-permute-done | bytes 131104 | tf_op jit(solution)/shard_map/ppermute | solution.py:388
  (145 shorter events, 61.7 us)
Async XLA Ops:
  18.5 26.7 %collective-permute-start.30 = (bf16[128,2048]{1,0:T(8,128)(2,1)S(1)}, bf16[128,2048]{1,0:T(8,128)(2,1)S(1)}, u32[]{:S(2)}, u32[]{:S(2)}) collective-permute-start(bf16[128,2048]{1,0:T(8,128)(2,1)S(1)} %get-tuple-element.84.rows_ref.own_ref), channel_id=1, source_target_pairs={{0,8},{8,24},{24,16},{16,0},{1,9},{9,25},{25,17},{17,1},{2,10},{10... | collective-permute-start | bytes 1572872 | tf_op jit(solution)/shard_map/ppermute | solution.py:380
  18.5 26.7 %collective-permute-start.16 = (bf16[128,2048]{1,0:T(8,128)(2,1)S(1)}, bf16[128,2048]{1,0:T(8,128)(2,1)}, u32[]{:S(2)}, u32[]{:S(2)}) collective-permute-start(bf16[128,2048]{1,0:T(8,128)(2,1)S(1)} %get-tuple-element.84.rows_ref.own_ref), channel_id=1, source_target_pairs={{0,16},{8,0},{24,8},{16,24},{1,17},{9,1},{25,9},{17,25},{2,18},{10... | collective-permute-start | bytes 1572872 | tf_op jit(solution)/shard_map/ppermute | solution.py:382
  45.2 10.9 %collective-permute-start.31 = (bf16[128,2048]{1,0:T(8,128)(2,1)S(1)}, bf16[128,2048]{1,0:T(8,128)(2,1)}, u32[]{:S(2)}, u32[]{:S(2)}) collective-permute-start(bf16[128,2048]{1,0:T(8,128)(2,1)S(1)} %collective-permute-done.30.own_ref), channel_id=1, source_target_pairs={{0,8},{8,24},{24,16},{16,0},{1,9},{9,25},{25,17},{17,1},{2,10},{10... | collective-permute-start | bytes 1572872 | tf_op jit(solution)/shard_map/ppermute | solution.py:381
  45.3 24.9 %collective-permute-start.17 = (bf16[128,2048]{1,0:T(8,128)(2,1)}, bf16[128,2048]{1,0:T(8,128)(2,1)S(1)}, u32[]{:S(2)}, u32[]{:S(2)}) collective-permute-start(bf16[128,2048]{1,0:T(8,128)(2,1)} %collective-permute-done.16.own_ref), channel_id=1, source_target_pairs={{0,1},{1,0},{2,3},{3,2},{4,5},{5,4},{6,7},{7,6},{8,9},{9,8},{10,11... | collective-permute-start | bytes 1572872 | tf_op jit(solution)/shard_map/ppermute | solution.py:461
  56.1 8.9 %collective-permute-start.32 = (bf16[128,2048]{1,0:T(8,128)(2,1)}, bf16[128,2048]{1,0:T(8,128)(2,1)S(1)}, u32[]{:S(2)}, u32[]{:S(2)}) collective-permute-start(bf16[128,2048]{1,0:T(8,128)(2,1)} %collective-permute-done.31.own_ref), channel_id=1, source_target_pairs={{0,1},{1,0},{2,3},{3,2},{4,5},{5,4},{6,7},{7,6},{8,9},{9,8},{10,11... | collective-permute-start | bytes 1572872 | tf_op jit(solution)/shard_map/ppermute | solution.py:461
  63.0 29.0 %collective-permute-start.4 = (bf16[128,2048]{1,0:T(8,128)(2,1)S(1)}, bf16[128,2048]{1,0:T(8,128)(2,1)S(1)}, u32[]{:S(2)}, u32[]{:S(2)}) collective-permute-start(bf16[128,2048]{1,0:T(8,128)(2,1)S(1)} %get-tuple-element.84.rows_ref.own_ref), channel_id=1, source_target_pairs={{0,1},{1,0},{2,3},{3,2},{4,5},{5,4},{6,7},{7,6},{8,9},{9,8},{10,11... | collective-permute-start | bytes 1572872 | tf_op jit(solution)/shard_map/ppermute | solution.py:461
  65.0 27.0 %collective-permute-start.45 = (bf16[128,2048]{1,0:T(8,128)(2,1)S(1)}, bf16[128,2048]{1,0:T(8,128)(2,1)S(1)}, u32[]{:S(2)}, u32[]{:S(2)}) collective-permute-start(bf16[128,2048]{1,0:T(8,128)(2,1)S(1)} %collective-permute-done.30.own_ref), channel_id=1, source_target_pairs={{0,1},{1,0},{2,3},{3,2},{4,5},{5,4},{6,7},{7,6},{8,9},{9,8},{10,11... | collective-permute-start | bytes 1572872 | tf_op jit(solution)/shard_map/ppermute | solution.py:461
  66.7 9.7 %collective-permute-start.34 = (bf16[64,2048]{1,0:T(8,128)(2,1)S(1)}, bf16[64,2048]{1,0:T(8,128)(2,1)S(1)}, u32[]{:S(2)}, u32[]{:S(2)}) collective-permute-start(bf16[64,2048]{1,0:T(8,128)(2,1)S(1)} %get-tuple-element.114), channel_id=1, source_target_pairs={{0,2},{2,0},{4,6},{6,4},{1,3},{3,1},{5,7},{7,5},{8,10},{10,8},{12,... | collective-permute-start | bytes 786440 | tf_op jit(solution)/shard_map/ppermute | solution.py:388
  69.3 9.2 %collective-permute-start.35 = (bf16[64,2048]{1,0:T(8,128)(2,1)S(1)}, bf16[64,2048]{1,0:T(8,128)(2,1)S(1)}, u32[]{:S(2)}, u32[]{:S(2)}) collective-permute-start(bf16[64,2048]{1,0:T(8,128)(2,1)S(1)} %get-tuple-element.115), channel_id=1, source_target_pairs={{0,4},{2,6},{4,0},{6,2},{1,5},{3,7},{5,1},{7,3},{8,12},{10,14},{12... | collective-permute-start | bytes 786440 | tf_op jit(solution)/shard_map/ppermute | solution.py:388
  70.2 14.3 %collective-permute-start.36 = (bf16[64,2048]{1,0:T(8,128)(2,1)S(1)}, bf16[64,2048]{1,0:T(8,128)(2,1)S(1)}, u32[]{:S(2)}, u32[]{:S(2)}) collective-permute-start(bf16[64,2048]{1,0:T(8,128)(2,1)S(1)} %get-tuple-element.116), channel_id=1, source_target_pairs={{0,6},{2,4},{4,2},{6,0},{1,7},{3,5},{5,3},{7,1},{8,14},{10,12},{12... | collective-permute-start | bytes 786440 | tf_op jit(solution)/shard_map/ppermute | solution.py:388
  76.4 16.9 %collective-permute-start.19 = (bf16[64,2048]{1,0:T(8,128)(2,1)S(1)}, bf16[64,2048]{1,0:T(8,128)(2,1)S(1)}, u32[]{:S(2)}, u32[]{:S(2)}) collective-permute-start(bf16[64,2048]{1,0:T(8,128)(2,1)S(1)} %get-tuple-element.101), channel_id=1, source_target_pairs={{0,2},{2,0},{4,6},{6,4},{1,3},{3,1},{5,7},{7,5},{8,10},{10,8},{12,... | collective-permute-start | bytes 786440 | tf_op jit(solution)/shard_map/ppermute | solution.py:388
  78.4 15.5 %collective-permute-start.20 = (bf16[64,2048]{1,0:T(8,128)(2,1)S(1)}, bf16[64,2048]{1,0:T(8,128)(2,1)S(1)}, u32[]{:S(2)}, u32[]{:S(2)}) collective-permute-start(bf16[64,2048]{1,0:T(8,128)(2,1)S(1)} %get-tuple-element.102), channel_id=1, source_target_pairs={{0,4},{2,6},{4,0},{6,2},{1,5},{3,7},{5,1},{7,3},{8,12},{10,14},{12... | collective-permute-start | bytes 786440 | tf_op jit(solution)/shard_map/ppermute | solution.py:388
  84.4 10.4 %collective-permute-start.21 = (bf16[64,2048]{1,0:T(8,128)(2,1)S(1)}, bf16[64,2048]{1,0:T(8,128)(2,1)S(1)}, u32[]{:S(2)}, u32[]{:S(2)}) collective-permute-start(bf16[64,2048]{1,0:T(8,128)(2,1)S(1)} %get-tuple-element.103), channel_id=1, source_target_pairs={{0,6},{2,4},{4,2},{6,0},{1,7},{3,5},{5,3},{7,1},{8,14},{10,12},{12... | collective-permute-start | bytes 786440 | tf_op jit(solution)/shard_map/ppermute | solution.py:388
  96.1 25.6 %collective-permute-start.47 = (bf16[64,2048]{1,0:T(8,128)(2,1)S(1)}, bf16[64,2048]{1,0:T(8,128)(2,1)S(1)}, u32[]{:S(2)}, u32[]{:S(2)}) collective-permute-start(bf16[64,2048]{1,0:T(8,128)(2,1)S(1)} %get-tuple-element.127), channel_id=1, source_target_pairs={{0,2},{2,0},{4,6},{6,4},{1,3},{3,1},{5,7},{7,5},{8,10},{10,8},{12,... | collective-permute-start | bytes 786440 | tf_op jit(solution)/shard_map/ppermute | solution.py:388
  98.5 24.2 %collective-permute-start.48 = (bf16[64,2048]{1,0:T(8,128)(2,1)S(1)}, bf16[64,2048]{1,0:T(8,128)(2,1)S(1)}, u32[]{:S(2)}, u32[]{:S(2)}) collective-permute-start(bf16[64,2048]{1,0:T(8,128)(2,1)S(1)} %get-tuple-element.128), channel_id=1, source_target_pairs={{0,4},{2,6},{4,0},{6,2},{1,5},{3,7},{5,1},{7,3},{8,12},{10,14},{12... | collective-permute-start | bytes 786440 | tf_op jit(solution)/shard_map/ppermute | solution.py:388
  100.2 23.3 %collective-permute-start.49 = (bf16[64,2048]{1,0:T(8,128)(2,1)S(1)}, bf16[64,2048]{1,0:T(8,128)(2,1)S(1)}, u32[]{:S(2)}, u32[]{:S(2)}) collective-permute-start(bf16[64,2048]{1,0:T(8,128)(2,1)S(1)} %get-tuple-element.129), channel_id=1, source_target_pairs={{0,6},{2,4},{4,2},{6,0},{1,7},{3,5},{5,3},{7,1},{8,14},{10,12},{12... | collective-permute-start | bytes 786440 | tf_op jit(solution)/shard_map/ppermute | solution.py:388
  101.7 16.1 %collective-permute-start.42 = (bf16[32,2048]{1,0:T(8,128)(2,1)S(1)}, bf16[32,2048]{1,0:T(8,128)(2,1)S(1)}, u32[]{:S(2)}, u32[]{:S(2)}) collective-permute-start(bf16[32,2048]{1,0:T(8,128)(2,1)S(1)} %get-tuple-element.123), channel_id=1, source_target_pairs={{0,6},{1,7},{2,4},{3,5},{4,2},{5,3},{6,0},{7,1},{8,14},{9,15},{10,... | collective-permute-start | bytes 393224 | tf_op jit(solution)/shard_map/ppermute | solution.py:388
  103.2 16.3 %collective-permute-start.43 = (bf16[32,2048]{1,0:T(8,128)(2,1)S(1)}, bf16[32,2048]{1,0:T(8,128)(2,1)S(1)}, u32[]{:S(2)}, u32[]{:S(2)}) collective-permute-start(bf16[32,2048]{1,0:T(8,128)(2,1)S(1)} %get-tuple-element.124), channel_id=1, source_target_pairs={{0,7},{1,6},{2,5},{3,4},{4,3},{5,2},{6,1},{7,0},{8,15},{9,14},{10,... | collective-permute-start | bytes 393224 | tf_op jit(solution)/shard_map/ppermute | solution.py:388
  121.7 8.7 %collective-permute-start.24 = (bf16[32,2048]{1,0:T(8,128)(2,1)S(1)}, bf16[32,2048]{1,0:T(8,128)(2,1)S(1)}, u32[]{:S(2)}, u32[]{:S(2)}) collective-permute-start(bf16[32,2048]{1,0:T(8,128)(2,1)S(1)} %get-tuple-element.107), channel_id=1, source_target_pairs={{0,3},{1,2},{2,1},{3,0},{4,7},{5,6},{6,5},{7,4},{8,11},{9,10},{10,... | collective-permute-start | bytes 393224 | tf_op jit(solution)/shard_map/ppermute | solution.py:388
  122.7 8.8 %collective-permute-start.25 = (bf16[32,2048]{1,0:T(8,128)(2,1)S(1)}, bf16[32,2048]{1,0:T(8,128)(2,1)S(1)}, u32[]{:S(2)}, u32[]{:S(2)}) collective-permute-start(bf16[32,2048]{1,0:T(8,128)(2,1)S(1)} %get-tuple-element.108), channel_id=1, source_target_pairs={{0,4},{1,5},{2,6},{3,7},{4,0},{5,1},{6,2},{7,3},{8,12},{9,13},{10,... | collective-permute-start | bytes 393224 | tf_op jit(solution)/shard_map/ppermute | solution.py:388
  123.5 8.7 %collective-permute-start.26 = (bf16[32,2048]{1,0:T(8,128)(2,1)S(1)}, bf16[32,2048]{1,0:T(8,128)(2,1)S(1)}, u32[]{:S(2)}, u32[]{:S(2)}) collective-permute-start(bf16[32,2048]{1,0:T(8,128)(2,1)S(1)} %get-tuple-element.109), channel_id=1, source_target_pairs={{0,5},{1,4},{2,7},{3,6},{4,1},{5,0},{6,3},{7,2},{8,13},{9,12},{10,... | collective-permute-start | bytes 393224 | tf_op jit(solution)/shard_map/ppermute | solution.py:388
  124.4 9.9 %collective-permute-start.27 = (bf16[32,2048]{1,0:T(8,128)(2,1)S(1)}, bf16[32,2048]{1,0:T(8,128)(2,1)S(1)}, u32[]{:S(2)}, u32[]{:S(2)}) collective-permute-start(bf16[32,2048]{1,0:T(8,128)(2,1)S(1)} %get-tuple-element.110), channel_id=1, source_target_pairs={{0,6},{1,7},{2,4},{3,5},{4,2},{5,3},{6,0},{7,1},{8,14},{9,15},{10,... | collective-permute-start | bytes 393224 | tf_op jit(solution)/shard_map/ppermute | solution.py:388
  125.8 29.2 %collective-permute-start.44 = (bf16[128,2048]{1,0:T(8,128)(2,1)S(1)}, bf16[128,2048]{1,0:T(8,128)(2,1)S(1)}, u32[]{:S(2)}, u32[]{:S(2)}) collective-permute-start(bf16[128,2048]{1,0:T(8,128)(2,1)S(1)} %get-tuple-element.125), channel_id=1, source_target_pairs={{0,16},{8,0},{24,8},{16,24},{1,17},{9,1},{25,9},{17,25},{2,18},{10... | collective-permute-start | bytes 1572872 | tf_op jit(solution)/shard_map/ppermute | solution.py:480
  137.2 8.8 %collective-permute-start.53 = (bf16[32,2048]{1,0:T(8,128)(2,1)S(1)}, bf16[32,2048]{1,0:T(8,128)(2,1)S(1)}, u32[]{:S(2)}, u32[]{:S(2)}) collective-permute-start(bf16[32,2048]{1,0:T(8,128)(2,1)S(1)} %get-tuple-element.134), channel_id=1, source_target_pairs={{0,4},{1,5},{2,6},{3,7},{4,0},{5,1},{6,2},{7,3},{8,12},{9,13},{10,... | collective-permute-start | bytes 393224 | tf_op jit(solution)/shard_map/ppermute | solution.py:388
  137.8 8.9 %collective-permute-start.54 = (bf16[32,2048]{1,0:T(8,128)(2,1)S(1)}, bf16[32,2048]{1,0:T(8,128)(2,1)S(1)}, u32[]{:S(2)}, u32[]{:S(2)}) collective-permute-start(bf16[32,2048]{1,0:T(8,128)(2,1)S(1)} %get-tuple-element.135), channel_id=1, source_target_pairs={{0,5},{1,4},{2,7},{3,6},{4,1},{5,0},{6,3},{7,2},{8,13},{9,12},{10,... | collective-permute-start | bytes 393224 | tf_op jit(solution)/shard_map/ppermute | solution.py:388
  140.0 9.4 %collective-permute-start.55 = (bf16[32,2048]{1,0:T(8,128)(2,1)S(1)}, bf16[32,2048]{1,0:T(8,128)(2,1)S(1)}, u32[]{:S(2)}, u32[]{:S(2)}) collective-permute-start(bf16[32,2048]{1,0:T(8,128)(2,1)S(1)} %get-tuple-element.136), channel_id=1, source_target_pairs={{0,6},{1,7},{2,4},{3,5},{4,2},{5,3},{6,0},{7,1},{8,14},{9,15},{10,... | collective-permute-start | bytes 393224 | tf_op jit(solution)/shard_map/ppermute | solution.py:388
  146.0 11.7 %collective-permute-start.6 = (bf16[64,2048]{1,0:T(8,128)(2,1)S(1)}, bf16[64,2048]{1,0:T(8,128)(2,1)S(1)}, u32[]{:S(2)}, u32[]{:S(2)}) collective-permute-start(bf16[64,2048]{1,0:T(8,128)(2,1)S(1)} %get-tuple-element.88), channel_id=1, source_target_pairs={{0,2},{2,0},{4,6},{6,4},{1,3},{3,1},{5,7},{7,5},{8,10},{10,8},{12,... | collective-permute-start | bytes 786440 | tf_op jit(solution)/shard_map/ppermute | solution.py:388
  146.7 11.0 %collective-permute-start.7 = (bf16[64,2048]{1,0:T(8,128)(2,1)S(1)}, bf16[64,2048]{1,0:T(8,128)(2,1)S(1)}, u32[]{:S(2)}, u32[]{:S(2)}) collective-permute-start(bf16[64,2048]{1,0:T(8,128)(2,1)S(1)} %get-tuple-element.89), channel_id=1, source_target_pairs={{0,4},{2,6},{4,0},{6,2},{1,5},{3,7},{5,1},{7,3},{8,12},{10,14},{12... | collective-permute-start | bytes 786440 | tf_op jit(solution)/shard_map/ppermute | solution.py:388
  149.3 13.4 %collective-permute-start.8 = (bf16[64,2048]{1,0:T(8,128)(2,1)S(1)}, bf16[64,2048]{1,0:T(8,128)(2,1)S(1)}, u32[]{:S(2)}, u32[]{:S(2)}) collective-permute-start(bf16[64,2048]{1,0:T(8,128)(2,1)S(1)} %get-tuple-element.90), channel_id=1, source_target_pairs={{0,6},{2,4},{4,2},{6,0},{1,7},{3,5},{5,3},{7,1},{8,14},{10,12},{12... | collective-permute-start | bytes 786440 | tf_op jit(solution)/shard_map/ppermute | solution.py:388
  151.0 32.9 %collective-permute-start.29 = (bf16[128,2048]{1,0:T(8,128)(2,1)S(1)}, bf16[128,2048]{1,0:T(8,128)(2,1)S(1)}, u32[]{:S(2)}, u32[]{:S(2)}) collective-permute-start(bf16[128,2048]{1,0:T(8,128)(2,1)S(1)} %get-tuple-element.112), channel_id=1, source_target_pairs={{0,8},{8,24},{24,16},{16,0},{1,9},{9,25},{25,17},{17,1},{2,10},{10... | collective-permute-start | bytes 1572872 | tf_op jit(solution)/shard_map/ppermute | solution.py:480
  155.1 28.8 %collective-permute-start.57 = (bf16[128,2048]{1,0:T(8,128)(2,1)S(1)}, bf16[128,2048]{1,0:T(8,128)(2,1)S(1)}, u32[]{:S(2)}, u32[]{:S(2)}) collective-permute-start(bf16[128,2048]{1,0:T(8,128)(2,1)S(1)} %add_convert_fusion.1), channel_id=1, source_target_pairs={{0,16},{8,0},{24,8},{16,24},{1,17},{9,1},{25,9},{17,25},{2,18},{10... | collective-permute-start | bytes 1572872 | tf_op jit(solution)/shard_map/ppermute | solution.py:480
  174.2 8.4 %collective-permute-start.15 = (bf16[32,2048]{1,0:T(8,128)(2,1)S(1)}, bf16[32,2048]{1,0:T(8,128)(2,1)S(1)}, u32[]{:S(2)}, u32[]{:S(2)}) collective-permute-start(bf16[32,2048]{1,0:T(8,128)(2,1)S(1)} %get-tuple-element.98), channel_id=1, source_target_pairs={{0,7},{1,6},{2,5},{3,4},{4,3},{5,2},{6,1},{7,0},{8,15},{9,14},{10,... | collective-permute-start | bytes 393224 | tf_op jit(solution)/shard_map/ppermute | solution.py:388
  (38 other events, 390.2 us)

commit v3 on v2

--- a/solution.py
+++ b/solution.py
@@ -479,9 +479,10 @@
             route = ring(4, distance)
             return lax.ppermute(block.astype(BF16), "z", route).astype(F32)
 
-        far = hop(short[2], -1)
-        last = hop(far + partial[1], -1)
-        routed = partial[0] + hop(short[3], 1) + last
+        back = hop(short[1], -1)
+        ahead = hop(short[2], 1)
+        ahead = hop(ahead + partial[3], 1)
+        routed = partial[0] + back + ahead
     else:
         routed = partial[0]
         for j in range(1, z_count):

time: 186 us -> 190 us (1.022)
  waiting for transfers between devices: 91.8 us -> 95.1 us
  starting transfers between devices: 55.1 us -> 57.7 us
    ppermute x1, waiting for transfers between devices: 10.8 us -> 22.5 us  [gather_ring(): two = lax.ppermute(one, 'z', ring(4, 1))]
    ppermute x1, waiting for transfers between devices: 23.8 us -> 15 us  [gather_ring(): one = lax.ppermute(own, 'z', ring(4, 1))]
    ppermute x43, starting transfers between devices: 38.8 us -> 43.3 us  [exchange(): lax.ppermute(pieces[k], axes, flips(count, k))]
  transfers between devices with their start and end apart: 58 -> 58, of which waited for: 28 -> 26; matrix products, arithmetic and copies ran while one was open for 1% -> 1% of each run, Pallas kernels for 15% -> 14%
where the time goes in v3:
time: 190 us
  waiting for transfers between devices  95.1 us (50%)
  starting transfers between devices  57.7 us (30%)
  Pallas kernels  29.6 us (16%)
  local copies, waits for them, and re-layouts  4.02 us (2%)
  other arithmetic  2.94 us (2%)
    ppermute x43, waiting for transfers between devices, exchange(): lax.ppermute(pieces[k], axes, flips(count, k))  49.8 us
    ppermute x43, starting transfers between devices, exchange(): lax.ppermute(pieces[k], axes, flips(count, k))  43.3 us
    ppermute x1, waiting for transfers between devices, gather_ring(): two = lax.ppermute(one, 'z', ring(4, 1))  22.5 us
    ppermute x1, waiting for transfers between devices, gather_ring(): one = lax.ppermute(own, 'z', ring(4, 1))  15 us
    pallas_call x4, Pallas kernels, expert_rows(): pl.pallas_call(functools.partial(expert_kernel, parts, count), out_shape=...  11.5 us
    pallas_call x4, Pallas kernels, combine(): pl.pallas_call(functools.partial(combine_kernel, parts, parts // 2), out_...  5.52 us
    ppermute x3, starting transfers between devices, gate_tables(): lax.ppermute(table[j], 'z', ring(count, j))  5 us
  transfers between devices with their start and end apart: 58, of which 26 were waited for; matrix products, arithmetic and copies ran while one was open for 1% of the time, Pallas kernels for 14%

profile of v3, /device:TPU:0, one launch (start us, length us, event | category | flops | bytes accessed | tf_op | source)
XLA Modules:
  0.0 189.8 jit_solution(9917155415568749174)
XLA Ops:
  0.7 3.0 %collective-permute-start = (f32[2,384]{1,0:T(2,128)S(1)}, f32[2,384]{1,0:T(2,128)S(1)}, u32[]{:S(2)}, u32[]{:S(2)}) collective-permute-start(f32[2,384]{1,0:T(2,128)S(1)} %convert_multiply_fusion), channel_id=1, source_target_pairs={{28,0},{0,4},{4,8},{8,12},{12,16},{16,20},{20,24},{24,28},{29,1},{... | collective-permute-start | bytes 9224 | tf_op jit(solution)/shard_map/ppermute | solution.py:22
  5.6 2.7 %collective-permute-done.halo_ref = f32[2,384]{1,0:T(2,128)S(1)} collective-permute-done((f32[2,384]{1,0:T(2,128)S(1)}, f32[2,384]{1,0:T(2,128)S(1)}, u32[]{:S(2)}, u32[]{:S(2)}) %collective-permute-start) | collective-permute-done | bytes 3104 | tf_op jit(solution)/shard_map/ppermute | solution.py:22
  12.1 2.9 %fetch_rows.1.refs_5_ = bf16[1536,2048]{1,0:T(8,128)(2,1)S(1)} custom-call(bf16[1536,2048]{1,0:T(8,128)(2,1)} %from_ref), custom_call_target="tpu_custom_call" | custom-call | flops 1048576 | bytes 6291456 | tf_op jit(solution)/shard_map/fetch_rows/pallas_call | solution.py:115
  15.4 3.1 %mix_project.1 = (f32[128,2048]{1,0:T(8,128)}, bf16[128,2048]{1,0:T(8,128)(2,1)S(1)}) custom-call(s32[1]{0:T(128)} %bitcast.me_ref, bf16[128,384]{1,0:T(8,128)(2,1)S(1)} %get-tuple-element.77.refs_0_, bf16[128,384]{1,0:T(8,128)(2,1)S(1)} %collective-permute-done.1.refs_1_, bf16[128,384]{1,0:T(8,128)(2,1)S(1)} %collective-permute-done.2.refs_2_, ...), custom_call_target="tpu_custom_call" | custom-call | flops 805306368 | bytes 6815744 | tf_op jit(solution)/shard_map/mix_project/pallas_call | solution.py:184
  18.5 15.0 %collective-permute-done.16.own_ref = bf16[128,2048]{1,0:T(8,128)(2,1)S(1)} collective-permute-done((bf16[128,2048]{1,0:T(8,128)(2,1)S(1)}, bf16[128,2048]{1,0:T(8,128)(2,1)S(1)}, u32[]{:S(2)}, u32[]{:S(2)}) %collective-permute-start.16) | collective-permute-done | bytes 524320 | tf_op jit(solution)/shard_map/ppermute | solution.py:380
  33.5 3.0 %collective-permute-start.44 = (bf16[128,2048]{1,0:T(8,128)(2,1)S(1)}, bf16[128,2048]{1,0:T(8,128)(2,1)S(1)}, u32[]{:S(2)}, u32[]{:S(2)}) collective-permute-start(bf16[128,2048]{1,0:T(8,128)(2,1)S(1)} %get-tuple-element.84.rows_ref.own_ref), channel_id=1, source_target_pairs={{0,16},{8,0},{24,8},{16,24},{1,17},{9,1},{25,9},{17,25},{2,18},{10... | collective-permute-start | bytes 1572872 | tf_op jit(solution)/shard_map/ppermute | solution.py:382
  36.5 22.5 %collective-permute-done.30.own_ref = bf16[128,2048]{1,0:T(8,128)(2,1)} collective-permute-done((bf16[128,2048]{1,0:T(8,128)(2,1)S(1)}, bf16[128,2048]{1,0:T(8,128)(2,1)}, u32[]{:S(2)}, u32[]{:S(2)}) %collective-permute-start.30) | collective-permute-done | bytes 524320 | tf_op jit(solution)/shard_map/ppermute | solution.py:381
  61.2 2.1 %collective-permute-start.32 = (f32[20,128]{1,0:T(8,128)S(1)}, f32[20,128]{1,0:T(8,128)S(1)}, u32[]{:S(2)}, u32[]{:S(2)}) collective-permute-start(f32[20,128]{1,0:T(8,128)S(1)} %get-tuple-element.141), channel_id=1, source_target_pairs={{0,24},{8,16},{24,0},{16,8},{1,25},{9,17},{25,1},{17,9},{2,26},{10... | collective-permute-start | bytes 30728 | tf_op jit(solution)/shard_map/ppermute | solution.py:398
  63.3 3.5 %collective-permute-done.32.table_ref.refs_8_ = f32[20,128]{1,0:T(8,128)S(1)} collective-permute-done((f32[20,128]{1,0:T(8,128)S(1)}, f32[20,128]{1,0:T(8,128)S(1)}, u32[]{:S(2)}, u32[]{:S(2)}) %collective-permute-start.32) | collective-permute-done | bytes 10272 | tf_op jit(solution)/shard_map/ppermute | solution.py:398
  66.8 2.9 %collective-permute-start.46 = (f32[20,128]{1,0:T(8,128)S(1)}, f32[20,128]{1,0:T(8,128)S(1)}, u32[]{:S(2)}, u32[]{:S(2)}) collective-permute-start(f32[20,128]{1,0:T(8,128)S(1)} %get-tuple-element.140), channel_id=1, source_target_pairs={{0,16},{8,0},{24,8},{16,24},{1,17},{9,1},{25,9},{17,25},{2,18},{10... | collective-permute-start | bytes 30728 | tf_op jit(solution)/shard_map/ppermute | solution.py:398
  75.3 4.7 %collective-permute-done.33.refs_1_ = bf16[64,2048]{1,0:T(8,128)(2,1)S(1)} collective-permute-done((bf16[64,2048]{1,0:T(8,128)(2,1)S(1)}, bf16[64,2048]{1,0:T(8,128)(2,1)S(1)}, u32[]{:S(2)}, u32[]{:S(2)}) %collective-permute-start.33) | collective-permute-done | bytes 262176 | tf_op jit(solution)/shard_map/ppermute | solution.py:388
  82.3 5.4 %collective-permute-done.35.refs_3_ = bf16[64,2048]{1,0:T(8,128)(2,1)S(1)} collective-permute-done((bf16[64,2048]{1,0:T(8,128)(2,1)S(1)}, bf16[64,2048]{1,0:T(8,128)(2,1)S(1)}, u32[]{:S(2)}, u32[]{:S(2)}) %collective-permute-start.35) | collective-permute-done | bytes 262176 | tf_op jit(solution)/shard_map/ppermute | solution.py:388
  92.0 2.9 %expert_rows.6 = (bf16[32,2048]{1,0:T(8,128)(2,1)S(1)}, bf16[32,2048]{1,0:T(8,128)(2,1)S(1)}, bf16[32,2048]{1,0:T(8,128)(2,1)S(1)}, bf16[32,2048]{1,0:T(8,128)(2...) custom-call(bf16[64,2048]{1,0:T(8,128)(2,1)S(1)} %get-tuple-element., ...), custom_call_target="tpu_custom_call" | custom-call | flops 1610612736 | bytes 6291456 | tf_op jit(solution)/shard_map/expert_rows/pallas_call | solution.py:269
  96.9 2.0 %collective-permute-start.39 = (bf16[32,2048]{1,0:T(8,128)(2,1)S(1)}, bf16[32,2048]{1,0:T(8,128)(2,1)S(1)}, u32[]{:S(2)}, u32[]{:S(2)}) collective-permute-start(bf16[32,2048]{1,0:T(8,128)(2,1)S(1)} %get-tuple-element.121), channel_id=1, source_target_pairs={{0,4},{1,5},{2,6},{3,7},{4,0},{5,1},{6,2},{7,3},{8,12},{9,13},{10,... | collective-permute-start | bytes 393224 | tf_op jit(solution)/shard_map/ppermute | solution.py:388
  101.4 2.0 %collective-permute-start.48 = (bf16[64,2048]{1,0:T(8,128)(2,1)S(1)}, bf16[64,2048]{1,0:T(8,128)(2,1)S(1)}, u32[]{:S(2)}, u32[]{:S(2)}) collective-permute-start(bf16[64,2048]{1,0:T(8,128)(2,1)S(1)} %get-tuple-element.128), channel_id=1, source_target_pairs={{0,4},{2,6},{4,0},{6,2},{1,5},{3,7},{5,1},{7,3},{8,12},{10,14},{12... | collective-permute-start | bytes 786440 | tf_op jit(solution)/shard_map/ppermute | solution.py:388
  108.1 2.9 %expert_rows.5 = (bf16[32,2048]{1,0:T(8,128)(2,1)S(1)}, bf16[32,2048]{1,0:T(8,128)(2,1)S(1)}, bf16[32,2048]{1,0:T(8,128)(2,1)S(1)}, bf16[32,2048]{1,0:T(8,128)(2...) custom-call(bf16[64,2048]{1,0:T(8,128)(2,1)S(1)} %get-tuple-element., ...), custom_call_target="tpu_custom_call" | custom-call | flops 1610612736 | bytes 6291456 | tf_op jit(solution)/shard_map/expert_rows/pallas_call | solution.py:269
  111.0 8.8 %collective-permute-done.41.refs_6_ = bf16[32,2048]{1,0:T(8,128)(2,1)S(1)} collective-permute-done((bf16[32,2048]{1,0:T(8,128)(2,1)S(1)}, bf16[32,2048]{1,0:T(8,128)(2,1)S(1)}, u32[]{:S(2)}, u32[]{:S(2)}) %collective-permute-start.41) | collective-permute-done | bytes 131104 | tf_op jit(solution)/shard_map/ppermute | solution.py:388
  119.8 2.2 %collective-permute-done.42.refs_7_ = bf16[32,2048]{1,0:T(8,128)(2,1)S(1)} collective-permute-done((bf16[32,2048]{1,0:T(8,128)(2,1)S(1)}, bf16[32,2048]{1,0:T(8,128)(2,1)S(1)}, u32[]{:S(2)}, u32[]{:S(2)}) %collective-permute-start.42) | collective-permute-done | bytes 131104 | tf_op jit(solution)/shard_map/ppermute | solution.py:388
  127.0 2.6 %collective-permute-start.27 = (bf16[32,2048]{1,0:T(8,128)(2,1)S(1)}, bf16[32,2048]{1,0:T(8,128)(2,1)S(1)}, u32[]{:S(2)}, u32[]{:S(2)}) collective-permute-start(bf16[32,2048]{1,0:T(8,128)(2,1)S(1)} %get-tuple-element.110), channel_id=1, source_target_pairs={{0,6},{1,7},{2,4},{3,5},{4,2},{5,3},{6,0},{7,1},{8,14},{9,15},{10,... | collective-permute-start | bytes 393224 | tf_op jit(solution)/shard_map/ppermute | solution.py:388
  130.4 2.9 %expert_rows.7 = (bf16[32,2048]{1,0:T(8,128)(2,1)S(1)}, bf16[32,2048]{1,0:T(8,128)(2,1)S(1)}, bf16[32,2048]{1,0:T(8,128)(2,1)S(1)}, bf16[32,2048]{1,0:T(8,128)(2...) custom-call(bf16[64,2048]{1,0:T(8,128)(2,1)S(1)} %get-tuple-element., ...), custom_call_target="tpu_custom_call" | custom-call | flops 1610612736 | bytes 6291456 | tf_op jit(solution)/shard_map/expert_rows/pallas_call | solution.py:269
  135.6 2.6 %collective-permute-done.27.refs_6_ = bf16[32,2048]{1,0:T(8,128)(2,1)S(1)} collective-permute-done((bf16[32,2048]{1,0:T(8,128)(2,1)S(1)}, bf16[32,2048]{1,0:T(8,128)(2,1)S(1)}, u32[]{:S(2)}, u32[]{:S(2)}) %collective-permute-start.27) | collective-permute-done | bytes 131104 | tf_op jit(solution)/shard_map/ppermute | solution.py:388
  138.2 2.2 %collective-permute-done.28.refs_7_ = bf16[32,2048]{1,0:T(8,128)(2,1)S(1)} collective-permute-done((bf16[32,2048]{1,0:T(8,128)(2,1)S(1)}, bf16[32,2048]{1,0:T(8,128)(2,1)S(1)}, u32[]{:S(2)}, u32[]{:S(2)}) %collective-permute-start.28) | collective-permute-done | bytes 131104 | tf_op jit(solution)/shard_map/ppermute | solution.py:388
  152.1 2.4 %collective-permute-start.8 = (bf16[64,2048]{1,0:T(8,128)(2,1)S(1)}, bf16[64,2048]{1,0:T(8,128)(2,1)S(1)}, u32[]{:S(2)}, u32[]{:S(2)}) collective-permute-start(bf16[64,2048]{1,0:T(8,128)(2,1)S(1)} %get-tuple-element.90), channel_id=1, source_target_pairs={{0,6},{2,4},{4,2},{6,0},{1,7},{3,5},{5,3},{7,1},{8,14},{10,12},{12... | collective-permute-start | bytes 786440 | tf_op jit(solution)/shard_map/ppermute | solution.py:388
  158.0 2.5 %collective-permute-done.6.refs_1_ = bf16[64,2048]{1,0:T(8,128)(2,1)S(1)} collective-permute-done((bf16[64,2048]{1,0:T(8,128)(2,1)S(1)}, bf16[64,2048]{1,0:T(8,128)(2,1)S(1)}, u32[]{:S(2)}, u32[]{:S(2)}) %collective-permute-start.6) | collective-permute-done | bytes 262176 | tf_op jit(solution)/shard_map/ppermute | solution.py:388
  160.8 4.8 %collective-permute-done.8.refs_3_ = bf16[64,2048]{1,0:T(8,128)(2,1)S(1)} collective-permute-done((bf16[64,2048]{1,0:T(8,128)(2,1)S(1)}, bf16[64,2048]{1,0:T(8,128)(2,1)S(1)}, u32[]{:S(2)}, u32[]{:S(2)}) %collective-permute-start.8) | collective-permute-done | bytes 262176 | tf_op jit(solution)/shard_map/ppermute | solution.py:388
  165.6 2.9 %expert_rows.4 = (bf16[32,2048]{1,0:T(8,128)(2,1)S(1)}, bf16[32,2048]{1,0:T(8,128)(2,1)S(1)}, bf16[32,2048]{1,0:T(8,128)(2,1)S(1)}, bf16[32,2048]{1,0:T(8,128)(2...) custom-call(bf16[64,2048]{1,0:T(8,128)(2,1)S(1)} %get-tuple-element., ...), custom_call_target="tpu_custom_call" | custom-call | flops 1610612736 | bytes 6291456 | tf_op jit(solution)/shard_map/expert_rows/pallas_call | solution.py:269
  171.8 2.4 %collective-permute-done.10.refs_2_ = bf16[32,2048]{1,0:T(8,128)(2,1)S(1)} collective-permute-done((bf16[32,2048]{1,0:T(8,128)(2,1)S(1)}, bf16[32,2048]{1,0:T(8,128)(2,1)S(1)}, u32[]{:S(2)}, u32[]{:S(2)}) %collective-permute-start.10) | collective-permute-done | bytes 131104 | tf_op jit(solution)/shard_map/ppermute | solution.py:388
  174.1 1.9 %collective-permute-done.11.refs_3_ = bf16[32,2048]{1,0:T(8,128)(2,1)S(1)} collective-permute-done((bf16[32,2048]{1,0:T(8,128)(2,1)S(1)}, bf16[32,2048]{1,0:T(8,128)(2,1)S(1)}, u32[]{:S(2)}, u32[]{:S(2)}) %collective-permute-start.11) | collective-permute-done | bytes 131104 | tf_op jit(solution)/shard_map/ppermute | solution.py:388
  176.1 2.0 %collective-permute-start.14 = (bf16[32,2048]{1,0:T(8,128)(2,1)S(1)}, bf16[32,2048]{1,0:T(8,128)(2,1)S(1)}, u32[]{:S(2)}, u32[]{:S(2)}) collective-permute-start(bf16[32,2048]{1,0:T(8,128)(2,1)S(1)} %get-tuple-element.97), channel_id=1, source_target_pairs={{0,6},{1,7},{2,4},{3,5},{4,2},{5,3},{6,0},{7,1},{8,14},{9,15},{10,... | collective-permute-start | bytes 393224 | tf_op jit(solution)/shard_map/ppermute | solution.py:388
  180.1 2.0 %shared_rows.1 = f32[128,2048]{1,0:T(8,128)S(1)} custom-call(bf16[128,2048]{1,0:T(8,128)(2,1)S(1)} %get-tuple-element.84.rows_ref.own_ref, f32[128,2048]{1,0:T(8,128)S(1)} %copy-done.7, bf16[2048,512]{1,0:T(8,128)(2,1)S(1)} %copy-done.4, bf16[2048,512]{1,0:T(8,128)(2,1)S(1)} %copy-done.5, bf16[512,2048]{1,0:T(8,128)(2,1)S(1)} %copy-done.6), custom_call_target="tpu_custom_call" | custom-call | flops 805306368 | bytes 6291456 | tf_op jit(solution)/shard_map/shared_rows/pallas_call | solution.py:307
  182.0 2.7 %collective-permute-done.14.refs_6_ = bf16[32,2048]{1,0:T(8,128)(2,1)S(1)} collective-permute-done((bf16[32,2048]{1,0:T(8,128)(2,1)S(1)}, bf16[32,2048]{1,0:T(8,128)(2,1)S(1)}, u32[]{:S(2)}, u32[]{:S(2)}) %collective-permute-start.14) | collective-permute-done | bytes 131104 | tf_op jit(solution)/shard_map/ppermute | solution.py:388
  184.7 2.7 %collective-permute-done.15.refs_7_ = bf16[32,2048]{1,0:T(8,128)(2,1)S(1)} collective-permute-done((bf16[32,2048]{1,0:T(8,128)(2,1)S(1)}, bf16[32,2048]{1,0:T(8,128)(2,1)S(1)}, u32[]{:S(2)}, u32[]{:S(2)}) %collective-permute-start.15) | collective-permute-done | bytes 131104 | tf_op jit(solution)/shard_map/ppermute | solution.py:388
  (145 shorter events, 61.6 us)
Async XLA Ops:
  18.5 15.0 %collective-permute-start.16 = (bf16[128,2048]{1,0:T(8,128)(2,1)S(1)}, bf16[128,2048]{1,0:T(8,128)(2,1)S(1)}, u32[]{:S(2)}, u32[]{:S(2)}) collective-permute-start(bf16[128,2048]{1,0:T(8,128)(2,1)S(1)} %get-tuple-element.84.rows_ref.own_ref), channel_id=1, source_target_pairs={{0,8},{8,24},{24,16},{16,0},{1,9},{9,25},{25,17},{17,1},{2,10},{10... | collective-permute-start | bytes 1572872 | tf_op jit(solution)/shard_map/ppermute | solution.py:380
  33.5 25.5 %collective-permute-start.30 = (bf16[128,2048]{1,0:T(8,128)(2,1)S(1)}, bf16[128,2048]{1,0:T(8,128)(2,1)}, u32[]{:S(2)}, u32[]{:S(2)}) collective-permute-start(bf16[128,2048]{1,0:T(8,128)(2,1)S(1)} %collective-permute-done.16.own_ref), channel_id=1, source_target_pairs={{0,8},{8,24},{24,16},{16,0},{1,9},{9,25},{25,17},{17,1},{2,10},{10... | collective-permute-start | bytes 1572872 | tf_op jit(solution)/shard_map/ppermute | solution.py:381
  33.5 33.2 %collective-permute-start.44 = (bf16[128,2048]{1,0:T(8,128)(2,1)S(1)}, bf16[128,2048]{1,0:T(8,128)(2,1)S(1)}, u32[]{:S(2)}, u32[]{:S(2)}) collective-permute-start(bf16[128,2048]{1,0:T(8,128)(2,1)S(1)} %get-tuple-element.84.rows_ref.own_ref), channel_id=1, source_target_pairs={{0,16},{8,0},{24,8},{16,24},{1,17},{9,1},{25,9},{17,25},{2,18},{10... | collective-permute-start | bytes 1572872 | tf_op jit(solution)/shard_map/ppermute | solution.py:382
  36.5 36.6 %collective-permute-start.17 = (bf16[128,2048]{1,0:T(8,128)(2,1)S(1)}, bf16[128,2048]{1,0:T(8,128)(2,1)S(1)}, u32[]{:S(2)}, u32[]{:S(2)}) collective-permute-start(bf16[128,2048]{1,0:T(8,128)(2,1)S(1)} %collective-permute-done.16.own_ref), channel_id=1, source_target_pairs={{0,1},{1,0},{2,3},{3,2},{4,5},{5,4},{6,7},{7,6},{8,9},{9,8},{10,11... | collective-permute-start | bytes 1572872 | tf_op jit(solution)/shard_map/ppermute | solution.py:461
  59.1 10.6 %collective-permute-start.31 = (bf16[128,2048]{1,0:T(8,128)(2,1)}, bf16[128,2048]{1,0:T(8,128)(2,1)S(1)}, u32[]{:S(2)}, u32[]{:S(2)}) collective-permute-start(bf16[128,2048]{1,0:T(8,128)(2,1)} %collective-permute-done.30.own_ref), channel_id=1, source_target_pairs={{0,1},{1,0},{2,3},{3,2},{4,5},{5,4},{6,7},{7,6},{8,9},{9,8},{10,11... | collective-permute-start | bytes 1572872 | tf_op jit(solution)/shard_map/ppermute | solution.py:461
  63.3 31.6 %collective-permute-start.4 = (bf16[128,2048]{1,0:T(8,128)(2,1)S(1)}, bf16[128,2048]{1,0:T(8,128)(2,1)S(1)}, u32[]{:S(2)}, u32[]{:S(2)}) collective-permute-start(bf16[128,2048]{1,0:T(8,128)(2,1)S(1)} %get-tuple-element.84.rows_ref.own_ref), channel_id=1, source_target_pairs={{0,1},{1,0},{2,3},{3,2},{4,5},{5,4},{6,7},{7,6},{8,9},{9,8},{10,11... | collective-permute-start | bytes 1572872 | tf_op jit(solution)/shard_map/ppermute | solution.py:461
  69.7 25.3 %collective-permute-start.45 = (bf16[128,2048]{1,0:T(8,128)(2,1)S(1)}, bf16[128,2048]{1,0:T(8,128)(2,1)S(1)}, u32[]{:S(2)}, u32[]{:S(2)}) collective-permute-start(bf16[128,2048]{1,0:T(8,128)(2,1)S(1)} %collective-permute-done.44.own_ref), channel_id=1, source_target_pairs={{0,1},{1,0},{2,3},{3,2},{4,5},{5,4},{6,7},{7,6},{8,9},{9,8},{10,11... | collective-permute-start | bytes 1572872 | tf_op jit(solution)/shard_map/ppermute | solution.py:461
  71.4 8.6 %collective-permute-start.33 = (bf16[64,2048]{1,0:T(8,128)(2,1)S(1)}, bf16[64,2048]{1,0:T(8,128)(2,1)S(1)}, u32[]{:S(2)}, u32[]{:S(2)}) collective-permute-start(bf16[64,2048]{1,0:T(8,128)(2,1)S(1)} %get-tuple-element.114), channel_id=1, source_target_pairs={{0,2},{2,0},{4,6},{6,4},{1,3},{3,1},{5,7},{7,5},{8,10},{10,8},{12,... | collective-permute-start | bytes 786440 | tf_op jit(solution)/shard_map/ppermute | solution.py:388
  73.1 9.2 %collective-permute-start.34 = (bf16[64,2048]{1,0:T(8,128)(2,1)S(1)}, bf16[64,2048]{1,0:T(8,128)(2,1)S(1)}, u32[]{:S(2)}, u32[]{:S(2)}) collective-permute-start(bf16[64,2048]{1,0:T(8,128)(2,1)S(1)} %get-tuple-element.115), channel_id=1, source_target_pairs={{0,4},{2,6},{4,0},{6,2},{1,5},{3,7},{5,1},{7,3},{8,12},{10,14},{12... | collective-permute-start | bytes 786440 | tf_op jit(solution)/shard_map/ppermute | solution.py:388
  73.1 14.5 %collective-permute-start.35 = (bf16[64,2048]{1,0:T(8,128)(2,1)S(1)}, bf16[64,2048]{1,0:T(8,128)(2,1)S(1)}, u32[]{:S(2)}, u32[]{:S(2)}) collective-permute-start(bf16[64,2048]{1,0:T(8,128)(2,1)S(1)} %get-tuple-element.116), channel_id=1, source_target_pairs={{0,6},{2,4},{4,2},{6,0},{1,7},{3,5},{5,3},{7,1},{8,14},{10,12},{12... | collective-permute-start | bytes 786440 | tf_op jit(solution)/shard_map/ppermute | solution.py:388
  80.0 15.7 %collective-permute-start.19 = (bf16[64,2048]{1,0:T(8,128)(2,1)S(1)}, bf16[64,2048]{1,0:T(8,128)(2,1)S(1)}, u32[]{:S(2)}, u32[]{:S(2)}) collective-permute-start(bf16[64,2048]{1,0:T(8,128)(2,1)S(1)} %get-tuple-element.101), channel_id=1, source_target_pairs={{0,2},{2,0},{4,6},{6,4},{1,3},{3,1},{5,7},{7,5},{8,10},{10,8},{12,... | collective-permute-start | bytes 786440 | tf_op jit(solution)/shard_map/ppermute | solution.py:388
  82.3 14.6 %collective-permute-start.20 = (bf16[64,2048]{1,0:T(8,128)(2,1)S(1)}, bf16[64,2048]{1,0:T(8,128)(2,1)S(1)}, u32[]{:S(2)}, u32[]{:S(2)}) collective-permute-start(bf16[64,2048]{1,0:T(8,128)(2,1)S(1)} %get-tuple-element.102), channel_id=1, source_target_pairs={{0,4},{2,6},{4,0},{6,2},{1,5},{3,7},{5,1},{7,3},{8,12},{10,14},{12... | collective-permute-start | bytes 786440 | tf_op jit(solution)/shard_map/ppermute | solution.py:388
  87.7 11.2 %collective-permute-start.21 = (bf16[64,2048]{1,0:T(8,128)(2,1)S(1)}, bf16[64,2048]{1,0:T(8,128)(2,1)S(1)}, u32[]{:S(2)}, u32[]{:S(2)}) collective-permute-start(bf16[64,2048]{1,0:T(8,128)(2,1)S(1)} %get-tuple-element.103), channel_id=1, source_target_pairs={{0,6},{2,4},{4,2},{6,0},{1,7},{3,5},{5,3},{7,1},{8,14},{10,12},{12... | collective-permute-start | bytes 786440 | tf_op jit(solution)/shard_map/ppermute | solution.py:388
  96.9 8.4 %collective-permute-start.39 = (bf16[32,2048]{1,0:T(8,128)(2,1)S(1)}, bf16[32,2048]{1,0:T(8,128)(2,1)S(1)}, u32[]{:S(2)}, u32[]{:S(2)}) collective-permute-start(bf16[32,2048]{1,0:T(8,128)(2,1)S(1)} %get-tuple-element.121), channel_id=1, source_target_pairs={{0,4},{1,5},{2,6},{3,7},{4,0},{5,1},{6,2},{7,3},{8,12},{9,13},{10,... | collective-permute-start | bytes 393224 | tf_op jit(solution)/shard_map/ppermute | solution.py:388
  99.4 25.8 %collective-permute-start.47 = (bf16[64,2048]{1,0:T(8,128)(2,1)S(1)}, bf16[64,2048]{1,0:T(8,128)(2,1)S(1)}, u32[]{:S(2)}, u32[]{:S(2)}) collective-permute-start(bf16[64,2048]{1,0:T(8,128)(2,1)S(1)} %get-tuple-element.127), channel_id=1, source_target_pairs={{0,2},{2,0},{4,6},{6,4},{1,3},{3,1},{5,7},{7,5},{8,10},{10,8},{12,... | collective-permute-start | bytes 786440 | tf_op jit(solution)/shard_map/ppermute | solution.py:388
  101.4 23.7 %collective-permute-start.48 = (bf16[64,2048]{1,0:T(8,128)(2,1)S(1)}, bf16[64,2048]{1,0:T(8,128)(2,1)S(1)}, u32[]{:S(2)}, u32[]{:S(2)}) collective-permute-start(bf16[64,2048]{1,0:T(8,128)(2,1)S(1)} %get-tuple-element.128), channel_id=1, source_target_pairs={{0,4},{2,6},{4,0},{6,2},{1,5},{3,7},{5,1},{7,3},{8,12},{10,14},{12... | collective-permute-start | bytes 786440 | tf_op jit(solution)/shard_map/ppermute | solution.py:388
  103.5 23.2 %collective-permute-start.49 = (bf16[64,2048]{1,0:T(8,128)(2,1)S(1)}, bf16[64,2048]{1,0:T(8,128)(2,1)S(1)}, u32[]{:S(2)}, u32[]{:S(2)}) collective-permute-start(bf16[64,2048]{1,0:T(8,128)(2,1)S(1)} %get-tuple-element.129), channel_id=1, source_target_pairs={{0,6},{2,4},{4,2},{6,0},{1,7},{3,5},{5,3},{7,1},{8,14},{10,12},{12... | collective-permute-start | bytes 786440 | tf_op jit(solution)/shard_map/ppermute | solution.py:388
  105.3 14.5 %collective-permute-start.41 = (bf16[32,2048]{1,0:T(8,128)(2,1)S(1)}, bf16[32,2048]{1,0:T(8,128)(2,1)S(1)}, u32[]{:S(2)}, u32[]{:S(2)}) collective-permute-start(bf16[32,2048]{1,0:T(8,128)(2,1)S(1)} %get-tuple-element.123), channel_id=1, source_target_pairs={{0,6},{1,7},{2,4},{3,5},{4,2},{5,3},{6,0},{7,1},{8,14},{9,15},{10,... | collective-permute-start | bytes 393224 | tf_op jit(solution)/shard_map/ppermute | solution.py:388
  106.4 15.6 %collective-permute-start.42 = (bf16[32,2048]{1,0:T(8,128)(2,1)S(1)}, bf16[32,2048]{1,0:T(8,128)(2,1)S(1)}, u32[]{:S(2)}, u32[]{:S(2)}) collective-permute-start(bf16[32,2048]{1,0:T(8,128)(2,1)S(1)} %get-tuple-element.124), channel_id=1, source_target_pairs={{0,7},{1,6},{2,5},{3,4},{4,3},{5,2},{6,1},{7,0},{8,15},{9,14},{10,... | collective-permute-start | bytes 393224 | tf_op jit(solution)/shard_map/ppermute | solution.py:388
  127.0 11.2 %collective-permute-start.27 = (bf16[32,2048]{1,0:T(8,128)(2,1)S(1)}, bf16[32,2048]{1,0:T(8,128)(2,1)S(1)}, u32[]{:S(2)}, u32[]{:S(2)}) collective-permute-start(bf16[32,2048]{1,0:T(8,128)(2,1)S(1)} %get-tuple-element.110), channel_id=1, source_target_pairs={{0,6},{1,7},{2,4},{3,5},{4,2},{5,3},{6,0},{7,1},{8,14},{9,15},{10,... | collective-permute-start | bytes 393224 | tf_op jit(solution)/shard_map/ppermute | solution.py:388
  129.6 27.5 %collective-permute-start.43 = (bf16[128,2048]{1,0:T(8,128)(2,1)S(1)}, bf16[128,2048]{1,0:T(8,128)(2,1)S(1)}, u32[]{:S(2)}, u32[]{:S(2)}) collective-permute-start(bf16[128,2048]{1,0:T(8,128)(2,1)S(1)} %get-tuple-element.125), channel_id=1, source_target_pairs={{0,8},{8,24},{24,16},{16,0},{1,9},{9,25},{25,17},{17,1},{2,10},{10... | collective-permute-start | bytes 1572872 | tf_op jit(solution)/shard_map/ppermute | solution.py:480
  134.9 8.6 %collective-permute-start.51 = (bf16[32,2048]{1,0:T(8,128)(2,1)S(1)}, bf16[32,2048]{1,0:T(8,128)(2,1)S(1)}, u32[]{:S(2)}, u32[]{:S(2)}) collective-permute-start(bf16[32,2048]{1,0:T(8,128)(2,1)S(1)} %get-tuple-element.132), channel_id=1, source_target_pairs={{0,2},{1,3},{2,0},{3,1},{4,6},{5,7},{6,4},{7,5},{8,10},{9,11},{10,... | collective-permute-start | bytes 393224 | tf_op jit(solution)/shard_map/ppermute | solution.py:388
  140.4 8.6 %collective-permute-start.53 = (bf16[32,2048]{1,0:T(8,128)(2,1)S(1)}, bf16[32,2048]{1,0:T(8,128)(2,1)S(1)}, u32[]{:S(2)}, u32[]{:S(2)}) collective-permute-start(bf16[32,2048]{1,0:T(8,128)(2,1)S(1)} %get-tuple-element.134), channel_id=1, source_target_pairs={{0,4},{1,5},{2,6},{3,7},{4,0},{5,1},{6,2},{7,3},{8,12},{9,13},{10,... | collective-permute-start | bytes 393224 | tf_op jit(solution)/shard_map/ppermute | solution.py:388
  141.5 9.2 %collective-permute-start.54 = (bf16[32,2048]{1,0:T(8,128)(2,1)S(1)}, bf16[32,2048]{1,0:T(8,128)(2,1)S(1)}, u32[]{:S(2)}, u32[]{:S(2)}) collective-permute-start(bf16[32,2048]{1,0:T(8,128)(2,1)S(1)} %get-tuple-element.135), channel_id=1, source_target_pairs={{0,5},{1,4},{2,7},{3,6},{4,1},{5,0},{6,3},{7,2},{8,13},{9,12},{10,... | collective-permute-start | bytes 393224 | tf_op jit(solution)/shard_map/ppermute | solution.py:388
  143.5 8.6 %collective-permute-start.55 = (bf16[32,2048]{1,0:T(8,128)(2,1)S(1)}, bf16[32,2048]{1,0:T(8,128)(2,1)S(1)}, u32[]{:S(2)}, u32[]{:S(2)}) collective-permute-start(bf16[32,2048]{1,0:T(8,128)(2,1)S(1)} %get-tuple-element.136), channel_id=1, source_target_pairs={{0,6},{1,7},{2,4},{3,5},{4,2},{5,3},{6,0},{7,1},{8,14},{9,15},{10,... | collective-permute-start | bytes 393224 | tf_op jit(solution)/shard_map/ppermute | solution.py:388
  148.9 11.6 %collective-permute-start.6 = (bf16[64,2048]{1,0:T(8,128)(2,1)S(1)}, bf16[64,2048]{1,0:T(8,128)(2,1)S(1)}, u32[]{:S(2)}, u32[]{:S(2)}) collective-permute-start(bf16[64,2048]{1,0:T(8,128)(2,1)S(1)} %get-tuple-element.88), channel_id=1, source_target_pairs={{0,2},{2,0},{4,6},{6,4},{1,3},{3,1},{5,7},{7,5},{8,10},{10,8},{12,... | collective-permute-start | bytes 786440 | tf_op jit(solution)/shard_map/ppermute | solution.py:388
  150.8 10.0 %collective-permute-start.7 = (bf16[64,2048]{1,0:T(8,128)(2,1)S(1)}, bf16[64,2048]{1,0:T(8,128)(2,1)S(1)}, u32[]{:S(2)}, u32[]{:S(2)}) collective-permute-start(bf16[64,2048]{1,0:T(8,128)(2,1)S(1)} %get-tuple-element.89), channel_id=1, source_target_pairs={{0,4},{2,6},{4,0},{6,2},{1,5},{3,7},{5,1},{7,3},{8,12},{10,14},{12... | collective-permute-start | bytes 786440 | tf_op jit(solution)/shard_map/ppermute | solution.py:388
  152.1 13.4 %collective-permute-start.8 = (bf16[64,2048]{1,0:T(8,128)(2,1)S(1)}, bf16[64,2048]{1,0:T(8,128)(2,1)S(1)}, u32[]{:S(2)}, u32[]{:S(2)}) collective-permute-start(bf16[64,2048]{1,0:T(8,128)(2,1)S(1)} %get-tuple-element.90), channel_id=1, source_target_pairs={{0,6},{2,4},{4,2},{6,0},{1,7},{3,5},{5,3},{7,1},{8,14},{10,12},{12... | collective-permute-start | bytes 786440 | tf_op jit(solution)/shard_map/ppermute | solution.py:388
  154.5 34.2 %collective-permute-start.29 = (bf16[128,2048]{1,0:T(8,128)(2,1)S(1)}, bf16[128,2048]{1,0:T(8,128)(2,1)S(1)}, u32[]{:S(2)}, u32[]{:S(2)}) collective-permute-start(bf16[128,2048]{1,0:T(8,128)(2,1)S(1)} %get-tuple-element.112), channel_id=1, source_target_pairs={{0,16},{8,0},{24,8},{16,24},{1,17},{9,1},{25,9},{17,25},{2,18},{10... | collective-permute-start | bytes 1572872 | tf_op jit(solution)/shard_map/ppermute | solution.py:480
  157.2 31.5 %collective-permute-start.57 = (bf16[128,2048]{1,0:T(8,128)(2,1)S(1)}, bf16[128,2048]{1,0:T(8,128)(2,1)S(1)}, u32[]{:S(2)}, u32[]{:S(2)}) collective-permute-start(bf16[128,2048]{1,0:T(8,128)(2,1)S(1)} %add_convert_fusion.1), channel_id=1, source_target_pairs={{0,8},{8,24},{24,16},{16,0},{1,9},{9,25},{25,17},{17,1},{2,10},{10... | collective-permute-start | bytes 1572872 | tf_op jit(solution)/shard_map/ppermute | solution.py:480
  176.1 8.6 %collective-permute-start.14 = (bf16[32,2048]{1,0:T(8,128)(2,1)S(1)}, bf16[32,2048]{1,0:T(8,128)(2,1)S(1)}, u32[]{:S(2)}, u32[]{:S(2)}) collective-permute-start(bf16[32,2048]{1,0:T(8,128)(2,1)S(1)} %get-tuple-element.97), channel_id=1, source_target_pairs={{0,6},{1,7},{2,4},{3,5},{4,2},{5,3},{6,0},{7,1},{8,14},{9,15},{10,... | collective-permute-start | bytes 393224 | tf_op jit(solution)/shard_map/ppermute | solution.py:388
  178.1 9.3 %collective-permute-start.15 = (bf16[32,2048]{1,0:T(8,128)(2,1)S(1)}, bf16[32,2048]{1,0:T(8,128)(2,1)S(1)}, u32[]{:S(2)}, u32[]{:S(2)}) collective-permute-start(bf16[32,2048]{1,0:T(8,128)(2,1)S(1)} %get-tuple-element.98), channel_id=1, source_target_pairs={{0,7},{1,6},{2,5},{3,4},{4,3},{5,2},{6,1},{7,0},{8,15},{9,14},{10,... | collective-permute-start | bytes 393224 | tf_op jit(solution)/shard_map/ppermute | solution.py:388
  (38 other events, 392.2 us)

commit v4 on v3

--- a/solution.py
+++ b/solution.py
@@ -105,10 +105,16 @@
     )(me, seq, head, halo, *blocks)
 
 
-def fetch_kernel(from_ref, to_ref, sem):
-    copy = pltpu.make_async_copy(from_ref, to_ref, sem)
-    copy.start()
-    copy.wait()
+def fetch_kernel(from_ref, to_ref, sems):
+    rows = from_ref.shape[0] // 4
+    copies = []
+    for k in range(4):
+        part = pl.ds(k * rows, rows)
+        copies.append(pltpu.make_async_copy(from_ref.at[part], to_ref.at[part], sems.at[k]))
+    for copy in copies:
+        copy.start()
+    for copy in copies:
+        copy.wait()
 
 
 def fetch(array):
@@ -117,7 +123,7 @@
         out_shape=pltpu.VMEM(array.shape, array.dtype),
         in_specs=[pl.BlockSpec(memory_space=pltpu.HBM)],
         out_specs=pl.BlockSpec(memory_space=pltpu.VMEM),
-        scratch_shapes=[pltpu.SemaphoreType.DMA],
+        scratch_shapes=[pltpu.SemaphoreType.DMA((4,))],
         cost_estimate=cost(1 << 20, [array]),
         compiler_params=grant(54),
         name="fetch_rows",
@@ -430,8 +436,8 @@
     blocks, head = filter_rows(me, out_gate, in_gate, conv_values, conv_taps, tp_count)
     blocks = mend_rows(me, seq, blocks, head, back, halo)
     pieces = exchange(blocks, TP)
-    late = (routes, mix_gain, pieces[1])
-    routes, mix_gain, _ = lax.optimization_barrier(late)
+    routes, _ = lax.optimization_barrier((routes, blocks[0]))
+    mix_gain, _ = lax.optimization_barrier((mix_gain, pieces[1]))
 
     row_count, top_count = routes.shape
     capacity = max(2, 4 * row_count * top_count // (6 * z_count * chips))

time: 190 us -> 187 us (0.984)
  waiting for transfers between devices: 95.1 us -> 92.7 us
    ppermute x3, starting transfers between devices: 5 us -> 2.21 us  [gate_tables(): lax.ppermute(table[j], 'z', ring(count, j))]
    ppermute x43, waiting for transfers between devices: 49.8 us -> 47.9 us  [exchange(): lax.ppermute(pieces[k], axes, flips(count, k))]
  transfers between devices with their start and end apart: 58 -> 58, of which waited for: 26 -> 25; matrix products, arithmetic and copies ran while one was open for 1% -> 1% of each run, Pallas kernels for 14% -> 14%
where the time goes in v4:
time: 187 us
  waiting for transfers between devices  92.7 us (50%)
  starting transfers between devices  57.6 us (31%)
  Pallas kernels  29.6 us (16%)
  local copies, waits for them, and re-layouts  3.33 us (2%)
  other arithmetic  2.94 us (2%)
    ppermute x43, waiting for transfers between devices, exchange(): lax.ppermute(pieces[k], axes, flips(count, k))  47.9 us
    ppermute x43, starting transfers between devices, exchange(): lax.ppermute(pieces[k], axes, flips(count, k))  44.2 us
    ppermute x1, waiting for transfers between devices, gather_ring(): two = lax.ppermute(one, 'z', ring(4, 1))  22.5 us
    ppermute x1, waiting for transfers between devices, gather_ring(): one = lax.ppermute(own, 'z', ring(4, 1))  15 us
    pallas_call x4, Pallas kernels, expert_rows(): pl.pallas_call(functools.partial(expert_kernel, parts, count), out_shape=...  11.5 us
    pallas_call x4, Pallas kernels, combine(): pl.pallas_call(functools.partial(combine_kernel, parts, parts // 2), out_...  5.53 us
    ppermute x3, starting transfers between devices, hop(): return lax.ppermute(block.astype(BF16), 'z', route).astype(F32)  4.1 us
  transfers between devices with their start and end apart: 58, of which 25 were waited for; matrix products, arithmetic and copies ran while one was open for 1% of the time, Pallas kernels for 14%

profile of v4, /device:TPU:0, one launch (start us, length us, event | category | flops | bytes accessed | tf_op | source)
XLA Modules:
  0.0 186.6 jit_solution(2446329947071353322)
XLA Ops:
  0.7 3.0 %collective-permute-start = (f32[2,384]{1,0:T(2,128)S(1)}, f32[2,384]{1,0:T(2,128)S(1)}, u32[]{:S(2)}, u32[]{:S(2)}) collective-permute-start(f32[2,384]{1,0:T(2,128)S(1)} %convert_multiply_fusion), channel_id=1, source_target_pairs={{28,0},{0,4},{4,8},{8,12},{12,16},{16,20},{20,24},{24,28},{29,1},{... | collective-permute-start | bytes 9224 | tf_op jit(solution)/shard_map/ppermute | solution.py:22
  3.9 1.9 %filter_rows.1 = (bf16[128,384]{1,0:T(8,128)(2,1)S(1)}, bf16[128,384]{1,0:T(8,128)(2,1)S(1)}, bf16[128,384]{1,0:T(8,128)(2,1)S(1)}, bf16[128,384]{1,0:T(8,128)(2,1)S(1)}, f32[40,384]{1,0:T(8,128)S(1)}) custom-call(s32[1]{0:T(128)} %bitcast.me_ref, bf16[512,384]{1,0:T(8,128)(2,1)} %gate_ref.2, bf16[512,384]{1,0:T(8,128)(2,1)} %in_ref.1, ...), custom_call_target="tpu_custom_call" | custom-call | flops 1048576 | bytes 1179648 | tf_op jit(solution)/shard_map/filter_rows/pallas_call | solution.py:63
  5.8 2.5 %collective-permute-done.halo_ref = f32[2,384]{1,0:T(2,128)S(1)} collective-permute-done((f32[2,384]{1,0:T(2,128)S(1)}, f32[2,384]{1,0:T(2,128)S(1)}, u32[]{:S(2)}, u32[]{:S(2)}) %collective-permute-start) | collective-permute-done | bytes 3104 | tf_op jit(solution)/shard_map/ppermute | solution.py:22
  11.2 2.9 %fetch_rows.1.refs_5_ = bf16[1536,2048]{1,0:T(8,128)(2,1)S(1)} custom-call(bf16[1536,2048]{1,0:T(8,128)(2,1)} %from_ref), custom_call_target="tpu_custom_call" | custom-call | flops 1048576 | bytes 6291456 | tf_op jit(solution)/shard_map/fetch_rows/pallas_call | solution.py:121
  15.3 3.1 %mix_project.1 = (f32[128,2048]{1,0:T(8,128)}, bf16[128,2048]{1,0:T(8,128)(2,1)S(1)}) custom-call(s32[1]{0:T(128)} %bitcast.me_ref, bf16[128,384]{1,0:T(8,128)(2,1)S(1)} %get-tuple-element.77.refs_0_, bf16[128,384]{1,0:T(8,128)(2,1)S(1)} %collective-permute-done.1.refs_1_, bf16[128,384]{1,0:T(8,128)(2,1)S(1)} %collective-permute-done.2.refs_2_, ...), custom_call_target="tpu_custom_call" | custom-call | flops 805306368 | bytes 6815744 | tf_op jit(solution)/shard_map/mix_project/pallas_call | solution.py:190
  18.4 15.0 %collective-permute-done.16.own_ref = bf16[128,2048]{1,0:T(8,128)(2,1)S(1)} collective-permute-done((bf16[128,2048]{1,0:T(8,128)(2,1)S(1)}, bf16[128,2048]{1,0:T(8,128)(2,1)S(1)}, u32[]{:S(2)}, u32[]{:S(2)}) %collective-permute-start.16) | collective-permute-done | bytes 524320 | tf_op jit(solution)/shard_map/ppermute | solution.py:386
  33.4 3.0 %collective-permute-start.44 = (bf16[128,2048]{1,0:T(8,128)(2,1)S(1)}, bf16[128,2048]{1,0:T(8,128)(2,1)S(1)}, u32[]{:S(2)}, u32[]{:S(2)}) collective-permute-start(bf16[128,2048]{1,0:T(8,128)(2,1)S(1)} %get-tuple-element.84.rows_ref.own_ref), channel_id=1, source_target_pairs={{0,16},{8,0},{24,8},{16,24},{1,17},{9,1},{25,9},{17,25},{2,18},{10... | collective-permute-start | bytes 1572872 | tf_op jit(solution)/shard_map/ppermute | solution.py:388
  36.3 22.5 %collective-permute-done.30.own_ref = bf16[128,2048]{1,0:T(8,128)(2,1)} collective-permute-done((bf16[128,2048]{1,0:T(8,128)(2,1)S(1)}, bf16[128,2048]{1,0:T(8,128)(2,1)}, u32[]{:S(2)}, u32[]{:S(2)}) %collective-permute-start.30) | collective-permute-done | bytes 524320 | tf_op jit(solution)/shard_map/ppermute | solution.py:387
  61.0 2.2 %collective-permute-start.32 = (f32[20,128]{1,0:T(8,128)S(1)}, f32[20,128]{1,0:T(8,128)S(1)}, u32[]{:S(2)}, u32[]{:S(2)}) collective-permute-start(f32[20,128]{1,0:T(8,128)S(1)} %get-tuple-element.141), channel_id=1, source_target_pairs={{0,24},{8,16},{24,0},{16,8},{1,25},{9,17},{25,1},{17,9},{2,26},{10... | collective-permute-start | bytes 30728 | tf_op jit(solution)/shard_map/ppermute | solution.py:404
  63.2 3.3 %collective-permute-done.32.table_ref.refs_8_ = f32[20,128]{1,0:T(8,128)S(1)} collective-permute-done((f32[20,128]{1,0:T(8,128)S(1)}, f32[20,128]{1,0:T(8,128)S(1)}, u32[]{:S(2)}, u32[]{:S(2)}) %collective-permute-start.32) | collective-permute-done | bytes 10272 | tf_op jit(solution)/shard_map/ppermute | solution.py:404
  68.6 1.9 %collective-permute-start.33 = (bf16[64,2048]{1,0:T(8,128)(2,1)S(1)}, bf16[64,2048]{1,0:T(8,128)(2,1)S(1)}, u32[]{:S(2)}, u32[]{:S(2)}) collective-permute-start(bf16[64,2048]{1,0:T(8,128)(2,1)S(1)} %get-tuple-element.114), channel_id=1, source_target_pairs={{0,2},{2,0},{4,6},{6,4},{1,3},{3,1},{5,7},{7,5},{8,10},{10,8},{12,... | collective-permute-start | bytes 786440 | tf_op jit(solution)/shard_map/ppermute | solution.py:394
  70.5 3.1 %collective-permute-start.35 = (bf16[64,2048]{1,0:T(8,128)(2,1)S(1)}, bf16[64,2048]{1,0:T(8,128)(2,1)S(1)}, u32[]{:S(2)}, u32[]{:S(2)}) collective-permute-start(bf16[64,2048]{1,0:T(8,128)(2,1)S(1)} %get-tuple-element.116), channel_id=1, source_target_pairs={{0,6},{2,4},{4,2},{6,0},{1,7},{3,5},{5,3},{7,1},{8,14},{10,12},{12... | collective-permute-start | bytes 786440 | tf_op jit(solution)/shard_map/ppermute | solution.py:394
  74.0 4.2 %collective-permute-done.33.refs_1_ = bf16[64,2048]{1,0:T(8,128)(2,1)S(1)} collective-permute-done((bf16[64,2048]{1,0:T(8,128)(2,1)S(1)}, bf16[64,2048]{1,0:T(8,128)(2,1)S(1)}, u32[]{:S(2)}, u32[]{:S(2)}) %collective-permute-start.33) | collective-permute-done | bytes 262176 | tf_op jit(solution)/shard_map/ppermute | solution.py:394
  79.6 6.7 %collective-permute-done.35.refs_3_ = bf16[64,2048]{1,0:T(8,128)(2,1)S(1)} collective-permute-done((bf16[64,2048]{1,0:T(8,128)(2,1)S(1)}, bf16[64,2048]{1,0:T(8,128)(2,1)S(1)}, u32[]{:S(2)}, u32[]{:S(2)}) %collective-permute-start.35) | collective-permute-done | bytes 262176 | tf_op jit(solution)/shard_map/ppermute | solution.py:394
  89.5 2.9 %expert_rows.6 = (bf16[32,2048]{1,0:T(8,128)(2,1)S(1)}, bf16[32,2048]{1,0:T(8,128)(2,1)S(1)}, bf16[32,2048]{1,0:T(8,128)(2,1)S(1)}, bf16[32,2048]{1,0:T(8,128)(2...) custom-call(bf16[64,2048]{1,0:T(8,128)(2,1)S(1)} %get-tuple-element., ...), custom_call_target="tpu_custom_call" | custom-call | flops 1610612736 | bytes 6291456 | tf_op jit(solution)/shard_map/expert_rows/pallas_call | solution.py:275
  94.3 1.9 %collective-permute-start.39 = (bf16[32,2048]{1,0:T(8,128)(2,1)S(1)}, bf16[32,2048]{1,0:T(8,128)(2,1)S(1)}, u32[]{:S(2)}, u32[]{:S(2)}) collective-permute-start(bf16[32,2048]{1,0:T(8,128)(2,1)S(1)} %get-tuple-element.121), channel_id=1, source_target_pairs={{0,4},{1,5},{2,6},{3,7},{4,0},{5,1},{6,2},{7,3},{8,12},{9,13},{10,... | collective-permute-start | bytes 393224 | tf_op jit(solution)/shard_map/ppermute | solution.py:394
  98.9 1.9 %collective-permute-start.48 = (bf16[64,2048]{1,0:T(8,128)(2,1)S(1)}, bf16[64,2048]{1,0:T(8,128)(2,1)S(1)}, u32[]{:S(2)}, u32[]{:S(2)}) collective-permute-start(bf16[64,2048]{1,0:T(8,128)(2,1)S(1)} %get-tuple-element.128), channel_id=1, source_target_pairs={{0,4},{2,6},{4,0},{6,2},{1,5},{3,7},{5,1},{7,3},{8,12},{10,14},{12... | collective-permute-start | bytes 786440 | tf_op jit(solution)/shard_map/ppermute | solution.py:394
  100.8 2.7 %collective-permute-start.49 = (bf16[64,2048]{1,0:T(8,128)(2,1)S(1)}, bf16[64,2048]{1,0:T(8,128)(2,1)S(1)}, u32[]{:S(2)}, u32[]{:S(2)}) collective-permute-start(bf16[64,2048]{1,0:T(8,128)(2,1)S(1)} %get-tuple-element.129), channel_id=1, source_target_pairs={{0,6},{2,4},{4,2},{6,0},{1,7},{3,5},{5,3},{7,1},{8,14},{10,12},{12... | collective-permute-start | bytes 786440 | tf_op jit(solution)/shard_map/ppermute | solution.py:394
  103.8 3.0 %collective-permute-start.42 = (bf16[32,2048]{1,0:T(8,128)(2,1)S(1)}, bf16[32,2048]{1,0:T(8,128)(2,1)S(1)}, u32[]{:S(2)}, u32[]{:S(2)}) collective-permute-start(bf16[32,2048]{1,0:T(8,128)(2,1)S(1)} %get-tuple-element.124), channel_id=1, source_target_pairs={{0,7},{1,6},{2,5},{3,4},{4,3},{5,2},{6,1},{7,0},{8,15},{9,14},{10,... | collective-permute-start | bytes 393224 | tf_op jit(solution)/shard_map/ppermute | solution.py:394
  106.8 2.9 %expert_rows.5 = (bf16[32,2048]{1,0:T(8,128)(2,1)S(1)}, bf16[32,2048]{1,0:T(8,128)(2,1)S(1)}, bf16[32,2048]{1,0:T(8,128)(2,1)S(1)}, bf16[32,2048]{1,0:T(8,128)(2...) custom-call(bf16[64,2048]{1,0:T(8,128)(2,1)S(1)} %get-tuple-element., ...), custom_call_target="tpu_custom_call" | custom-call | flops 1610612736 | bytes 6291456 | tf_op jit(solution)/shard_map/expert_rows/pallas_call | solution.py:275
  109.6 8.9 %collective-permute-done.41.refs_6_ = bf16[32,2048]{1,0:T(8,128)(2,1)S(1)} collective-permute-done((bf16[32,2048]{1,0:T(8,128)(2,1)S(1)}, bf16[32,2048]{1,0:T(8,128)(2,1)S(1)}, u32[]{:S(2)}, u32[]{:S(2)}) %collective-permute-start.41) | collective-permute-done | bytes 131104 | tf_op jit(solution)/shard_map/ppermute | solution.py:394
  118.5 2.1 %collective-permute-done.42.refs_7_ = bf16[32,2048]{1,0:T(8,128)(2,1)S(1)} collective-permute-done((bf16[32,2048]{1,0:T(8,128)(2,1)S(1)}, bf16[32,2048]{1,0:T(8,128)(2,1)S(1)}, u32[]{:S(2)}, u32[]{:S(2)}) %collective-permute-start.42) | collective-permute-done | bytes 131104 | tf_op jit(solution)/shard_map/ppermute | solution.py:394
  127.0 2.0 %collective-permute-start.43 = (bf16[128,2048]{1,0:T(8,128)(2,1)S(1)}, bf16[128,2048]{1,0:T(8,128)(2,1)S(1)}, u32[]{:S(2)}, u32[]{:S(2)}) collective-permute-start(bf16[128,2048]{1,0:T(8,128)(2,1)S(1)} %get-tuple-element.125), channel_id=1, source_target_pairs={{0,8},{8,24},{24,16},{16,0},{1,9},{9,25},{25,17},{17,1},{2,10},{10... | collective-permute-start | bytes 1572872 | tf_op jit(solution)/shard_map/ppermute | solution.py:486
  129.0 2.9 %expert_rows.7 = (bf16[32,2048]{1,0:T(8,128)(2,1)S(1)}, bf16[32,2048]{1,0:T(8,128)(2,1)S(1)}, bf16[32,2048]{1,0:T(8,128)(2,1)S(1)}, bf16[32,2048]{1,0:T(8,128)(2...) custom-call(bf16[64,2048]{1,0:T(8,128)(2,1)S(1)} %get-tuple-element., ...), custom_call_target="tpu_custom_call" | custom-call | flops 1610612736 | bytes 6291456 | tf_op jit(solution)/shard_map/expert_rows/pallas_call | solution.py:275
  136.0 2.6 %collective-permute-done.28.refs_7_ = bf16[32,2048]{1,0:T(8,128)(2,1)S(1)} collective-permute-done((bf16[32,2048]{1,0:T(8,128)(2,1)S(1)}, bf16[32,2048]{1,0:T(8,128)(2,1)S(1)}, u32[]{:S(2)}, u32[]{:S(2)}) %collective-permute-start.28) | collective-permute-done | bytes 131104 | tf_op jit(solution)/shard_map/ppermute | solution.py:394
  152.5 1.9 %collective-permute-start.29 = (bf16[128,2048]{1,0:T(8,128)(2,1)S(1)}, bf16[128,2048]{1,0:T(8,128)(2,1)S(1)}, u32[]{:S(2)}, u32[]{:S(2)}) collective-permute-start(bf16[128,2048]{1,0:T(8,128)(2,1)S(1)} %get-tuple-element.112), channel_id=1, source_target_pairs={{0,16},{8,0},{24,8},{16,24},{1,17},{9,1},{25,9},{17,25},{2,18},{10... | collective-permute-start | bytes 1572872 | tf_op jit(solution)/shard_map/ppermute | solution.py:486
  156.0 3.1 %collective-permute-done.6.refs_1_ = bf16[64,2048]{1,0:T(8,128)(2,1)S(1)} collective-permute-done((bf16[64,2048]{1,0:T(8,128)(2,1)S(1)}, bf16[64,2048]{1,0:T(8,128)(2,1)S(1)}, u32[]{:S(2)}, u32[]{:S(2)}) %collective-permute-start.6) | collective-permute-done | bytes 262176 | tf_op jit(solution)/shard_map/ppermute | solution.py:394
  159.1 5.1 %collective-permute-done.8.refs_3_ = bf16[64,2048]{1,0:T(8,128)(2,1)S(1)} collective-permute-done((bf16[64,2048]{1,0:T(8,128)(2,1)S(1)}, bf16[64,2048]{1,0:T(8,128)(2,1)S(1)}, u32[]{:S(2)}, u32[]{:S(2)}) %collective-permute-start.8) | collective-permute-done | bytes 262176 | tf_op jit(solution)/shard_map/ppermute | solution.py:394
  164.2 2.9 %expert_rows.4 = (bf16[32,2048]{1,0:T(8,128)(2,1)S(1)}, bf16[32,2048]{1,0:T(8,128)(2,1)S(1)}, bf16[32,2048]{1,0:T(8,128)(2,1)S(1)}, bf16[32,2048]{1,0:T(8,128)(2...) custom-call(bf16[64,2048]{1,0:T(8,128)(2,1)S(1)} %get-tuple-element., ...), custom_call_target="tpu_custom_call" | custom-call | flops 1610612736 | bytes 6291456 | tf_op jit(solution)/shard_map/expert_rows/pallas_call | solution.py:275
  169.7 3.3 %collective-permute-done.10.refs_2_ = bf16[32,2048]{1,0:T(8,128)(2,1)S(1)} collective-permute-done((bf16[32,2048]{1,0:T(8,128)(2,1)S(1)}, bf16[32,2048]{1,0:T(8,128)(2,1)S(1)}, u32[]{:S(2)}, u32[]{:S(2)}) %collective-permute-start.10) | collective-permute-done | bytes 131104 | tf_op jit(solution)/shard_map/ppermute | solution.py:394
  179.4 2.0 %shared_rows.1 = f32[128,2048]{1,0:T(8,128)S(1)} custom-call(bf16[128,2048]{1,0:T(8,128)(2,1)S(1)} %get-tuple-element.84.rows_ref.own_ref, f32[128,2048]{1,0:T(8,128)S(1)} %copy-done.7, bf16[2048,512]{1,0:T(8,128)(2,1)S(1)} %copy-done.4, bf16[2048,512]{1,0:T(8,128)(2,1)S(1)} %copy-done.5, bf16[512,2048]{1,0:T(8,128)(2,1)S(1)} %copy-done.6), custom_call_target="tpu_custom_call" | custom-call | flops 805306368 | bytes 6291456 | tf_op jit(solution)/shard_map/shared_rows/pallas_call | solution.py:313
  181.4 2.8 %collective-permute-done.15.refs_7_ = bf16[32,2048]{1,0:T(8,128)(2,1)S(1)} collective-permute-done((bf16[32,2048]{1,0:T(8,128)(2,1)S(1)}, bf16[32,2048]{1,0:T(8,128)(2,1)S(1)}, u32[]{:S(2)}, u32[]{:S(2)}) %collective-permute-start.15) | collective-permute-done | bytes 131104 | tf_op jit(solution)/shard_map/ppermute | solution.py:394
  (147 shorter events, 56.3 us)
Async XLA Ops:
  18.4 15.0 %collective-permute-start.16 = (bf16[128,2048]{1,0:T(8,128)(2,1)S(1)}, bf16[128,2048]{1,0:T(8,128)(2,1)S(1)}, u32[]{:S(2)}, u32[]{:S(2)}) collective-permute-start(bf16[128,2048]{1,0:T(8,128)(2,1)S(1)} %get-tuple-element.84.rows_ref.own_ref), channel_id=1, source_target_pairs={{0,8},{8,24},{24,16},{16,0},{1,9},{9,25},{25,17},{17,1},{2,10},{10... | collective-permute-start | bytes 1572872 | tf_op jit(solution)/shard_map/ppermute | solution.py:386
  33.4 25.5 %collective-permute-start.30 = (bf16[128,2048]{1,0:T(8,128)(2,1)S(1)}, bf16[128,2048]{1,0:T(8,128)(2,1)}, u32[]{:S(2)}, u32[]{:S(2)}) collective-permute-start(bf16[128,2048]{1,0:T(8,128)(2,1)S(1)} %collective-permute-done.16.own_ref), channel_id=1, source_target_pairs={{0,8},{8,24},{24,16},{16,0},{1,9},{9,25},{25,17},{17,1},{2,10},{10... | collective-permute-start | bytes 1572872 | tf_op jit(solution)/shard_map/ppermute | solution.py:387
  33.4 33.2 %collective-permute-start.44 = (bf16[128,2048]{1,0:T(8,128)(2,1)S(1)}, bf16[128,2048]{1,0:T(8,128)(2,1)S(1)}, u32[]{:S(2)}, u32[]{:S(2)}) collective-permute-start(bf16[128,2048]{1,0:T(8,128)(2,1)S(1)} %get-tuple-element.84.rows_ref.own_ref), channel_id=1, source_target_pairs={{0,16},{8,0},{24,8},{16,24},{1,17},{9,1},{25,9},{17,25},{2,18},{10... | collective-permute-start | bytes 1572872 | tf_op jit(solution)/shard_map/ppermute | solution.py:388
  36.3 34.1 %collective-permute-start.17 = (bf16[128,2048]{1,0:T(8,128)(2,1)S(1)}, bf16[128,2048]{1,0:T(8,128)(2,1)S(1)}, u32[]{:S(2)}, u32[]{:S(2)}) collective-permute-start(bf16[128,2048]{1,0:T(8,128)(2,1)S(1)} %collective-permute-done.16.own_ref), channel_id=1, source_target_pairs={{0,1},{1,0},{2,3},{3,2},{4,5},{5,4},{6,7},{7,6},{8,9},{9,8},{10,11... | collective-permute-start | bytes 1572872 | tf_op jit(solution)/shard_map/ppermute | solution.py:467
  66.6 25.8 %collective-permute-start.4 = (bf16[128,2048]{1,0:T(8,128)(2,1)S(1)}, bf16[128,2048]{1,0:T(8,128)(2,1)S(1)}, u32[]{:S(2)}, u32[]{:S(2)}) collective-permute-start(bf16[128,2048]{1,0:T(8,128)(2,1)S(1)} %get-tuple-element.84.rows_ref.own_ref), channel_id=1, source_target_pairs={{0,1},{1,0},{2,3},{3,2},{4,5},{5,4},{6,7},{7,6},{8,9},{9,8},{10,11... | collective-permute-start | bytes 1572872 | tf_op jit(solution)/shard_map/ppermute | solution.py:467
  66.6 25.9 %collective-permute-start.45 = (bf16[128,2048]{1,0:T(8,128)(2,1)S(1)}, bf16[128,2048]{1,0:T(8,128)(2,1)S(1)}, u32[]{:S(2)}, u32[]{:S(2)}) collective-permute-start(bf16[128,2048]{1,0:T(8,128)(2,1)S(1)} %collective-permute-done.44.own_ref), channel_id=1, source_target_pairs={{0,1},{1,0},{2,3},{3,2},{4,5},{5,4},{6,7},{7,6},{8,9},{9,8},{10,11... | collective-permute-start | bytes 1572872 | tf_op jit(solution)/shard_map/ppermute | solution.py:467
  68.6 9.6 %collective-permute-start.33 = (bf16[64,2048]{1,0:T(8,128)(2,1)S(1)}, bf16[64,2048]{1,0:T(8,128)(2,1)S(1)}, u32[]{:S(2)}, u32[]{:S(2)}) collective-permute-start(bf16[64,2048]{1,0:T(8,128)(2,1)S(1)} %get-tuple-element.114), channel_id=1, source_target_pairs={{0,2},{2,0},{4,6},{6,4},{1,3},{3,1},{5,7},{7,5},{8,10},{10,8},{12,... | collective-permute-start | bytes 786440 | tf_op jit(solution)/shard_map/ppermute | solution.py:394
  70.5 9.2 %collective-permute-start.34 = (bf16[64,2048]{1,0:T(8,128)(2,1)S(1)}, bf16[64,2048]{1,0:T(8,128)(2,1)S(1)}, u32[]{:S(2)}, u32[]{:S(2)}) collective-permute-start(bf16[64,2048]{1,0:T(8,128)(2,1)S(1)} %get-tuple-element.115), channel_id=1, source_target_pairs={{0,4},{2,6},{4,0},{6,2},{1,5},{3,7},{5,1},{7,3},{8,12},{10,14},{12... | collective-permute-start | bytes 786440 | tf_op jit(solution)/shard_map/ppermute | solution.py:394
  70.5 15.9 %collective-permute-start.35 = (bf16[64,2048]{1,0:T(8,128)(2,1)S(1)}, bf16[64,2048]{1,0:T(8,128)(2,1)S(1)}, u32[]{:S(2)}, u32[]{:S(2)}) collective-permute-start(bf16[64,2048]{1,0:T(8,128)(2,1)S(1)} %get-tuple-element.116), channel_id=1, source_target_pairs={{0,6},{2,4},{4,2},{6,0},{1,7},{3,5},{5,3},{7,1},{8,14},{10,12},{12... | collective-permute-start | bytes 786440 | tf_op jit(solution)/shard_map/ppermute | solution.py:394
  78.2 15.9 %collective-permute-start.19 = (bf16[64,2048]{1,0:T(8,128)(2,1)S(1)}, bf16[64,2048]{1,0:T(8,128)(2,1)S(1)}, u32[]{:S(2)}, u32[]{:S(2)}) collective-permute-start(bf16[64,2048]{1,0:T(8,128)(2,1)S(1)} %get-tuple-element.101), channel_id=1, source_target_pairs={{0,2},{2,0},{4,6},{6,4},{1,3},{3,1},{5,7},{7,5},{8,10},{10,8},{12,... | collective-permute-start | bytes 786440 | tf_op jit(solution)/shard_map/ppermute | solution.py:394
  79.6 14.7 %collective-permute-start.20 = (bf16[64,2048]{1,0:T(8,128)(2,1)S(1)}, bf16[64,2048]{1,0:T(8,128)(2,1)S(1)}, u32[]{:S(2)}, u32[]{:S(2)}) collective-permute-start(bf16[64,2048]{1,0:T(8,128)(2,1)S(1)} %get-tuple-element.102), channel_id=1, source_target_pairs={{0,4},{2,6},{4,0},{6,2},{1,5},{3,7},{5,1},{7,3},{8,12},{10,14},{12... | collective-permute-start | bytes 786440 | tf_op jit(solution)/shard_map/ppermute | solution.py:394
  86.3 9.9 %collective-permute-start.21 = (bf16[64,2048]{1,0:T(8,128)(2,1)S(1)}, bf16[64,2048]{1,0:T(8,128)(2,1)S(1)}, u32[]{:S(2)}, u32[]{:S(2)}) collective-permute-start(bf16[64,2048]{1,0:T(8,128)(2,1)S(1)} %get-tuple-element.103), channel_id=1, source_target_pairs={{0,6},{2,4},{4,2},{6,0},{1,7},{3,5},{5,3},{7,1},{8,14},{10,12},{12... | collective-permute-start | bytes 786440 | tf_op jit(solution)/shard_map/ppermute | solution.py:394
  94.3 9.2 %collective-permute-start.39 = (bf16[32,2048]{1,0:T(8,128)(2,1)S(1)}, bf16[32,2048]{1,0:T(8,128)(2,1)S(1)}, u32[]{:S(2)}, u32[]{:S(2)}) collective-permute-start(bf16[32,2048]{1,0:T(8,128)(2,1)S(1)} %get-tuple-element.121), channel_id=1, source_target_pairs={{0,4},{1,5},{2,6},{3,7},{4,0},{5,1},{6,2},{7,3},{8,12},{9,13},{10,... | collective-permute-start | bytes 393224 | tf_op jit(solution)/shard_map/ppermute | solution.py:394
  96.7 25.7 %collective-permute-start.47 = (bf16[64,2048]{1,0:T(8,128)(2,1)S(1)}, bf16[64,2048]{1,0:T(8,128)(2,1)S(1)}, u32[]{:S(2)}, u32[]{:S(2)}) collective-permute-start(bf16[64,2048]{1,0:T(8,128)(2,1)S(1)} %get-tuple-element.127), channel_id=1, source_target_pairs={{0,2},{2,0},{4,6},{6,4},{1,3},{3,1},{5,7},{7,5},{8,10},{10,8},{12,... | collective-permute-start | bytes 786440 | tf_op jit(solution)/shard_map/ppermute | solution.py:394
  98.9 24.7 %collective-permute-start.48 = (bf16[64,2048]{1,0:T(8,128)(2,1)S(1)}, bf16[64,2048]{1,0:T(8,128)(2,1)S(1)}, u32[]{:S(2)}, u32[]{:S(2)}) collective-permute-start(bf16[64,2048]{1,0:T(8,128)(2,1)S(1)} %get-tuple-element.128), channel_id=1, source_target_pairs={{0,4},{2,6},{4,0},{6,2},{1,5},{3,7},{5,1},{7,3},{8,12},{10,14},{12... | collective-permute-start | bytes 786440 | tf_op jit(solution)/shard_map/ppermute | solution.py:394
  100.8 24.5 %collective-permute-start.49 = (bf16[64,2048]{1,0:T(8,128)(2,1)S(1)}, bf16[64,2048]{1,0:T(8,128)(2,1)S(1)}, u32[]{:S(2)}, u32[]{:S(2)}) collective-permute-start(bf16[64,2048]{1,0:T(8,128)(2,1)S(1)} %get-tuple-element.129), channel_id=1, source_target_pairs={{0,6},{2,4},{4,2},{6,0},{1,7},{3,5},{5,3},{7,1},{8,14},{10,12},{12... | collective-permute-start | bytes 786440 | tf_op jit(solution)/shard_map/ppermute | solution.py:394
  103.6 14.9 %collective-permute-start.41 = (bf16[32,2048]{1,0:T(8,128)(2,1)S(1)}, bf16[32,2048]{1,0:T(8,128)(2,1)S(1)}, u32[]{:S(2)}, u32[]{:S(2)}) collective-permute-start(bf16[32,2048]{1,0:T(8,128)(2,1)S(1)} %get-tuple-element.123), channel_id=1, source_target_pairs={{0,6},{1,7},{2,4},{3,5},{4,2},{5,3},{6,0},{7,1},{8,14},{9,15},{10,... | collective-permute-start | bytes 393224 | tf_op jit(solution)/shard_map/ppermute | solution.py:394
  103.8 16.8 %collective-permute-start.42 = (bf16[32,2048]{1,0:T(8,128)(2,1)S(1)}, bf16[32,2048]{1,0:T(8,128)(2,1)S(1)}, u32[]{:S(2)}, u32[]{:S(2)}) collective-permute-start(bf16[32,2048]{1,0:T(8,128)(2,1)S(1)} %get-tuple-element.124), channel_id=1, source_target_pairs={{0,7},{1,6},{2,5},{3,4},{4,3},{5,2},{6,1},{7,0},{8,15},{9,14},{10,... | collective-permute-start | bytes 393224 | tf_op jit(solution)/shard_map/ppermute | solution.py:394
  122.4 9.4 %collective-permute-start.24 = (bf16[32,2048]{1,0:T(8,128)(2,1)S(1)}, bf16[32,2048]{1,0:T(8,128)(2,1)S(1)}, u32[]{:S(2)}, u32[]{:S(2)}) collective-permute-start(bf16[32,2048]{1,0:T(8,128)(2,1)S(1)} %get-tuple-element.107), channel_id=1, source_target_pairs={{0,3},{1,2},{2,1},{3,0},{4,7},{5,6},{6,5},{7,4},{8,11},{9,10},{10,... | collective-permute-start | bytes 393224 | tf_op jit(solution)/shard_map/ppermute | solution.py:394
  123.6 8.3 %collective-permute-start.25 = (bf16[32,2048]{1,0:T(8,128)(2,1)S(1)}, bf16[32,2048]{1,0:T(8,128)(2,1)S(1)}, u32[]{:S(2)}, u32[]{:S(2)}) collective-permute-start(bf16[32,2048]{1,0:T(8,128)(2,1)S(1)} %get-tuple-element.108), channel_id=1, source_target_pairs={{0,4},{1,5},{2,6},{3,7},{4,0},{5,1},{6,2},{7,3},{8,12},{9,13},{10,... | collective-permute-start | bytes 393224 | tf_op jit(solution)/shard_map/ppermute | solution.py:394
  125.5 9.5 %collective-permute-start.27 = (bf16[32,2048]{1,0:T(8,128)(2,1)S(1)}, bf16[32,2048]{1,0:T(8,128)(2,1)S(1)}, u32[]{:S(2)}, u32[]{:S(2)}) collective-permute-start(bf16[32,2048]{1,0:T(8,128)(2,1)S(1)} %get-tuple-element.110), channel_id=1, source_target_pairs={{0,6},{1,7},{2,4},{3,5},{4,2},{5,3},{6,0},{7,1},{8,14},{9,15},{10,... | collective-permute-start | bytes 393224 | tf_op jit(solution)/shard_map/ppermute | solution.py:394
  127.0 28.7 %collective-permute-start.43 = (bf16[128,2048]{1,0:T(8,128)(2,1)S(1)}, bf16[128,2048]{1,0:T(8,128)(2,1)S(1)}, u32[]{:S(2)}, u32[]{:S(2)}) collective-permute-start(bf16[128,2048]{1,0:T(8,128)(2,1)S(1)} %get-tuple-element.125), channel_id=1, source_target_pairs={{0,8},{8,24},{24,16},{16,0},{1,9},{9,25},{25,17},{17,1},{2,10},{10... | collective-permute-start | bytes 1572872 | tf_op jit(solution)/shard_map/ppermute | solution.py:486
  135.0 9.1 %collective-permute-start.52 = (bf16[32,2048]{1,0:T(8,128)(2,1)S(1)}, bf16[32,2048]{1,0:T(8,128)(2,1)S(1)}, u32[]{:S(2)}, u32[]{:S(2)}) collective-permute-start(bf16[32,2048]{1,0:T(8,128)(2,1)S(1)} %get-tuple-element.133), channel_id=1, source_target_pairs={{0,3},{1,2},{2,1},{3,0},{4,7},{5,6},{6,5},{7,4},{8,11},{9,10},{10,... | collective-permute-start | bytes 393224 | tf_op jit(solution)/shard_map/ppermute | solution.py:394
  138.6 9.0 %collective-permute-start.53 = (bf16[32,2048]{1,0:T(8,128)(2,1)S(1)}, bf16[32,2048]{1,0:T(8,128)(2,1)S(1)}, u32[]{:S(2)}, u32[]{:S(2)}) collective-permute-start(bf16[32,2048]{1,0:T(8,128)(2,1)S(1)} %get-tuple-element.134), channel_id=1, source_target_pairs={{0,4},{1,5},{2,6},{3,7},{4,0},{5,1},{6,2},{7,3},{8,12},{9,13},{10,... | collective-permute-start | bytes 393224 | tf_op jit(solution)/shard_map/ppermute | solution.py:394
  139.3 8.8 %collective-permute-start.54 = (bf16[32,2048]{1,0:T(8,128)(2,1)S(1)}, bf16[32,2048]{1,0:T(8,128)(2,1)S(1)}, u32[]{:S(2)}, u32[]{:S(2)}) collective-permute-start(bf16[32,2048]{1,0:T(8,128)(2,1)S(1)} %get-tuple-element.135), channel_id=1, source_target_pairs={{0,5},{1,4},{2,7},{3,6},{4,1},{5,0},{6,3},{7,2},{8,13},{9,12},{10,... | collective-permute-start | bytes 393224 | tf_op jit(solution)/shard_map/ppermute | solution.py:394
  141.5 9.1 %collective-permute-start.55 = (bf16[32,2048]{1,0:T(8,128)(2,1)S(1)}, bf16[32,2048]{1,0:T(8,128)(2,1)S(1)}, u32[]{:S(2)}, u32[]{:S(2)}) collective-permute-start(bf16[32,2048]{1,0:T(8,128)(2,1)S(1)} %get-tuple-element.136), channel_id=1, source_target_pairs={{0,6},{1,7},{2,4},{3,5},{4,2},{5,3},{6,0},{7,1},{8,14},{9,15},{10,... | collective-permute-start | bytes 393224 | tf_op jit(solution)/shard_map/ppermute | solution.py:394
  144.1 8.3 %collective-permute-start.56 = (bf16[32,2048]{1,0:T(8,128)(2,1)S(1)}, bf16[32,2048]{1,0:T(8,128)(2,1)S(1)}, u32[]{:S(2)}, u32[]{:S(2)}) collective-permute-start(bf16[32,2048]{1,0:T(8,128)(2,1)S(1)} %get-tuple-element.137), channel_id=1, source_target_pairs={{0,7},{1,6},{2,5},{3,4},{4,3},{5,2},{6,1},{7,0},{8,15},{9,14},{10,... | collective-permute-start | bytes 393224 | tf_op jit(solution)/shard_map/ppermute | solution.py:394
  147.7 11.3 %collective-permute-start.6 = (bf16[64,2048]{1,0:T(8,128)(2,1)S(1)}, bf16[64,2048]{1,0:T(8,128)(2,1)S(1)}, u32[]{:S(2)}, u32[]{:S(2)}) collective-permute-start(bf16[64,2048]{1,0:T(8,128)(2,1)S(1)} %get-tuple-element.88), channel_id=1, source_target_pairs={{0,2},{2,0},{4,6},{6,4},{1,3},{3,1},{5,7},{7,5},{8,10},{10,8},{12,... | collective-permute-start | bytes 786440 | tf_op jit(solution)/shard_map/ppermute | solution.py:394
  148.1 11.0 %collective-permute-start.7 = (bf16[64,2048]{1,0:T(8,128)(2,1)S(1)}, bf16[64,2048]{1,0:T(8,128)(2,1)S(1)}, u32[]{:S(2)}, u32[]{:S(2)}) collective-permute-start(bf16[64,2048]{1,0:T(8,128)(2,1)S(1)} %get-tuple-element.89), channel_id=1, source_target_pairs={{0,4},{2,6},{4,0},{6,2},{1,5},{3,7},{5,1},{7,3},{8,12},{10,14},{12... | collective-permute-start | bytes 786440 | tf_op jit(solution)/shard_map/ppermute | solution.py:394
  150.6 13.5 %collective-permute-start.8 = (bf16[64,2048]{1,0:T(8,128)(2,1)S(1)}, bf16[64,2048]{1,0:T(8,128)(2,1)S(1)}, u32[]{:S(2)}, u32[]{:S(2)}) collective-permute-start(bf16[64,2048]{1,0:T(8,128)(2,1)S(1)} %get-tuple-element.90), channel_id=1, source_target_pairs={{0,6},{2,4},{4,2},{6,0},{1,7},{3,5},{5,3},{7,1},{8,14},{10,12},{12... | collective-permute-start | bytes 786440 | tf_op jit(solution)/shard_map/ppermute | solution.py:394
  152.5 33.0 %collective-permute-start.29 = (bf16[128,2048]{1,0:T(8,128)(2,1)S(1)}, bf16[128,2048]{1,0:T(8,128)(2,1)S(1)}, u32[]{:S(2)}, u32[]{:S(2)}) collective-permute-start(bf16[128,2048]{1,0:T(8,128)(2,1)S(1)} %get-tuple-element.112), channel_id=1, source_target_pairs={{0,16},{8,0},{24,8},{16,24},{1,17},{9,1},{25,9},{17,25},{2,18},{10... | collective-permute-start | bytes 1572872 | tf_op jit(solution)/shard_map/ppermute | solution.py:486
  155.8 29.7 %collective-permute-start.57 = (bf16[128,2048]{1,0:T(8,128)(2,1)S(1)}, bf16[128,2048]{1,0:T(8,128)(2,1)S(1)}, u32[]{:S(2)}, u32[]{:S(2)}) collective-permute-start(bf16[128,2048]{1,0:T(8,128)(2,1)S(1)} %add_convert_fusion.1), channel_id=1, source_target_pairs={{0,8},{8,24},{24,16},{16,0},{1,9},{9,25},{25,17},{17,1},{2,10},{10... | collective-permute-start | bytes 1572872 | tf_op jit(solution)/shard_map/ppermute | solution.py:486
  (39 other events, 391.1 us)
